TPU v7x, 32 devices: a whole 2x2x4 slice. The times are simulated.
32 devices in a mesh: sp: 8 (over z, x), tp: 4 (over y, core).
Axes of the slice: x: 2, y: 2, z: 4, core: 2. Of those that a mesh axis runs over, the one named last changes fastest.
Arguments:
- tokens: bfloat16 [8192, 2048], P('sp'), may hold values from -8 to 8
- norm_gain: float32 [2048], replicated, may hold values from 0.1 to 1.9
- query_weight: bfloat16 [2048, 512], P(None, 'tp'), may hold values from -40 to 40
- key_weight: bfloat16 [2048, 256], P(None, 'tp'), may hold values from -1 to 1
- value_weight: bfloat16 [2048, 256], P(None, 'tp'), may hold values from -0.125 to 0.125
- sink_logits: float32 [8], P('tp'), may hold values from 1 to 6
- conv_in_weight: bfloat16 [2048, 512], P(None, 'tp'), may hold values from -0.125 to 0.125
- conv_gate_weight: bfloat16 [2048, 512], P(None, 'tp'), may hold values from -0.125 to 0.125
- conv_taps: bfloat16 [31, 512], replicated, may hold values from -1 to 1
- conv_gain: float32 [512], replicated, may hold values from 0.1 to 1.9
- point_weight: bfloat16 [512, 512], replicated, may hold values from -0.25 to 0.25
- output_gain: float32 [1024], replicated, may hold values from 0.1 to 1.9
- output_weight: bfloat16 [1024, 2048], P('sp'), may hold values from -0.1875 to 0.1875
Outputs:
- mixed_output: bfloat16 [8192, 2048], P(('sp', 'tp'))
All inputs are finite; a program needn't handle non-finite values.
Results may differ from a plain program's by a relative error of at most 0.0087.
Values may be sent and summed in bfloat16 or wider, within the bound.
No kernel may reach another device: no remote copies, remote signals or barrier semaphores. Data moves between devices by JAX's collectives and lax.ppermute only.
A program may use at most 64 MiB of HBM per device.

v0:
```python
import jax
import jax.numpy as jnp
from jax import lax
from jax.experimental import pallas as pl
from jax.experimental.pallas import tpu as pltpu
from jax.sharding import PartitionSpec as P


HEAD_DIM = 64
WINDOW = 128
CONV_WIDTH = 31


NORM_EPSILON = 1e-06
MASKED_SCORE = -1e30
HALO = 32


PLACE = ("sp", "tp")


def from_behind(block, axis, distance):
    devices = range(lax.axis_size(axis))
    route = [(i - distance, i) for i in devices if i - distance in devices]
    return lax.ppermute(block, axis, route)


def project_inputs(tokens, norm_gain, query_weight, key_weight, value_weight, in_weight, gate_weight):
    rows, width = tokens.shape
    heads_width, pair_width = query_weight.shape[1], key_weight.shape[1] + value_weight.shape[1]
    key_width, channels = key_weight.shape[1], in_weight.shape[1]
    block = 256
    blocks = rows // block
    tail = WINDOW + HALO
    starts = [0, heads_width + pair_width, heads_width + pair_width + channels]

    def body(
        gain_hbm, tokens_hbm, query_hbm, key_hbm, value_hbm, in_hbm, gate_hbm,
        queries_ref, pairs_ref, gated_ref, tail_ref,
        fetched, normed, joined, pairs_rows, gain_ref, arrived, fetched_sem,
    ):
        fetches = [
            pltpu.make_async_copy(
                tokens_hbm.at[pl.ds(i * block, block)], fetched.at[i], fetched_sem.at[i]
            )
            for i in range(blocks)
        ]
        copies = [
            pltpu.make_async_copy(key_hbm, pairs_rows.at[pl.ds(0, key_width)], arrived.at[3]),
            pltpu.make_async_copy(
                value_hbm, pairs_rows.at[pl.ds(key_width, pair_width - key_width)], arrived.at[4]
            ),
        ] + [
            pltpu.make_async_copy(
                source, joined.at[:, pl.ds(start, source.shape[1])], arrived.at[i]
            )
            for i, (source, start) in enumerate(zip([query_hbm, in_hbm, gate_hbm], starts))
        ]
        gain_copy = pltpu.make_async_copy(gain_hbm, gain_ref, arrived.at[5])
        gain_copy.start()
        fetches[0].start()
        for copy in copies:
            copy.start()
        for fetch in fetches[1:]:
            fetch.start()

        def norm(i):
            widened = fetched[i].astype(jnp.float32)
            scale = lax.rsqrt(jnp.mean(widened * widened, axis=-1, keepdims=True) + NORM_EPSILON)
            normed[i] = (widened * scale * gain_ref[...]).astype(jnp.bfloat16)

        gain_copy.wait()
        fetches[0].wait()
        norm(0)
        for copy in copies[:2]:
            copy.wait()
        joined[:, heads_width : heads_width + pair_width] = pairs_rows[...].T
        for copy in copies[2:]:
            copy.wait()
        for i in range(blocks):
            if i + 1 < blocks:
                fetches[i + 1].wait()
            here = pl.ds(i * block, block)
            result = jnp.dot(normed[i], joined[...], preferred_element_type=jnp.float32)
            if i + 1 < blocks:
                norm(i + 1)
            queries_ref[here] = result[:, :heads_width].astype(jnp.bfloat16)
            pairs = result[:, heads_width : heads_width + pair_width].astype(jnp.bfloat16)
            pairs_ref[here] = pairs
            conv_in = result[:, starts[1] : starts[2]]
            conv_gate = result[:, starts[2] :]
            gated = (conv_in * jax.nn.sigmoid(conv_gate)).astype(jnp.bfloat16)
            gated_ref[here] = gated
            if i + 1 == blocks:
                tail_ref[:WINDOW] = pairs[block - WINDOW :]
                tail_ref[WINDOW:] = gated[block - HALO :]

    vmem = pl.BlockSpec(memory_space=pltpu.VMEM)
    in_hbm = [
        pltpu.with_memory_space_constraint(operand, pltpu.HBM)
        for operand in (
            norm_gain[None], tokens, query_weight, key_weight.T, value_weight.T, in_weight, gate_weight
        )
    ]
    return pl.pallas_call(
        body,
        in_specs=[pl.BlockSpec(memory_space=pl.ANY)] * 7,
        out_specs=[vmem] * 4,
        out_shape=[
            jax.ShapeDtypeStruct((rows, heads_width), jnp.bfloat16),
            jax.ShapeDtypeStruct((rows, pair_width), jnp.bfloat16),
            jax.ShapeDtypeStruct((rows, channels), jnp.bfloat16),
            jax.ShapeDtypeStruct((tail, channels), jnp.bfloat16),
        ],
        scratch_shapes=[
            pltpu.VMEM((blocks, block, width), jnp.bfloat16),
            pltpu.VMEM((blocks, block, width), jnp.bfloat16),
            pltpu.VMEM((width, heads_width + pair_width + 2 * channels), jnp.bfloat16),
            pltpu.VMEM((pair_width, width), jnp.bfloat16),
            pltpu.VMEM((1, width), jnp.float32),
            pltpu.SemaphoreType.DMA((6,)),
            pltpu.SemaphoreType.DMA((blocks,)),
        ],
        compiler_params=pltpu.CompilerParams(vmem_limit_bytes=24 << 20),
        name="project_inputs",
    )(*in_hbm)


def mix_rows(queries, pairs, gated, earlier, sinks, taps, shares):
    rows, heads_width = queries.shape
    channels = gated.shape[1]
    head_count = heads_width // HEAD_DIM
    share_rows = rows // shares

    def body(
        sinks_ref, queries_ref, pairs_ref, gated_ref, earlier_ref, taps_ref,
        out_ref, band, extended,
    ):
        band[:WINDOW] = earlier_ref[:WINDOW]
        band[WINDOW:] = pairs_ref[...]
        extended[:HALO] = earlier_ref[WINDOW:].astype(jnp.float32)
        extended[HALO:] = gated_ref[...].astype(jnp.float32)
        query_index = lax.broadcasted_iota(jnp.int32, (WINDOW, 2 * WINDOW), 0)
        key_index = lax.broadcasted_iota(jnp.int32, (WINDOW, 2 * WINDOW), 1)
        distance = WINDOW + query_index - key_index
        in_window = (distance >= 0) & (distance < WINDOW)
        not_before = in_window & ((lax.axis_index("sp") > 0) | (key_index >= WINDOW))
        own = pl.multiple_of(lax.axis_index("tp") * channels, channels)
        tap_rows = taps_ref[:, pl.ds(own, channels)].astype(jnp.float32)
        for block in range(rows // WINDOW):
            start = block * WINDOW
            share, inner = start // share_rows, start % share_rows
            keys = band[start : start + 2 * WINDOW, :HEAD_DIM]
            values = band[start : start + 2 * WINDOW, HEAD_DIM : 2 * HEAD_DIM]
            allowed = not_before if block == 0 else in_window
            found = []
            for head in range(head_count):
                here = queries_ref[start : start + WINDOW, head * HEAD_DIM : (head + 1) * HEAD_DIM]
                scores = lax.dot_general(
                    here, keys, (((1,), (1,)), ((), ())), preferred_element_type=jnp.float32
                ) * HEAD_DIM ** (-0.5)
                scores = jnp.where(allowed, scores, MASKED_SCORE)
                sink = sinks_ref[head]
                peak = jnp.maximum(jnp.max(scores, axis=-1, keepdims=True), sink)
                raised = jnp.exp(scores - peak)
                denominator = jnp.sum(raised, axis=-1, keepdims=True) + jnp.exp(sink - peak)
                weights = (raised * (1.0 / denominator)).astype(jnp.bfloat16)
                found.append(
                    jnp.dot(weights, values, preferred_element_type=jnp.float32).astype(jnp.bfloat16)
                )
            out_ref[share, inner : inner + WINDOW, :heads_width] = jnp.concatenate(found, axis=1)
            total = jnp.zeros((WINDOW, channels), jnp.float32)
            for tap in range(CONV_WIDTH):
                from_row = start + HALO - (CONV_WIDTH - 1) + tap
                total = total + tap_rows[tap : tap + 1] * extended[from_row : from_row + WINDOW]
            out_ref[share, inner : inner + WINDOW, heads_width:] = total.astype(jnp.bfloat16)

    whole = pl.BlockSpec(memory_space=pltpu.VMEM)
    scalars = pl.BlockSpec(memory_space=pltpu.SMEM)
    return pl.pallas_call(
        body,
        in_specs=[scalars] + [whole] * 5,
        out_specs=whole,
        out_shape=jax.ShapeDtypeStruct((shares, share_rows, heads_width + channels), jnp.bfloat16),
        scratch_shapes=[
            pltpu.VMEM((WINDOW + rows, pairs.shape[1]), jnp.bfloat16),
            pltpu.VMEM((HALO + rows, channels), jnp.float32),
        ],
        compiler_params=pltpu.CompilerParams(vmem_limit_bytes=12 << 20),
        name="mix_rows",
    )(sinks, queries, pairs, gated, earlier, taps)


def merge_mixers(exchanged, conv_gain, point_weight, output_gain):
    shares, rows, joint = exchanged.shape
    heads_width = joint // 2
    width = shares * heads_width

    def body(exchanged_ref, conv_gain_ref, point_ref, gain_ref, out_ref):
        attended = jnp.concatenate(
            [exchanged_ref[i, :, :heads_width] for i in range(shares)], axis=1
        ).astype(jnp.float32)
        convolved = jnp.concatenate(
            [exchanged_ref[i, :, heads_width:] for i in range(shares)], axis=1
        ).astype(jnp.float32)
        centered = convolved - jnp.mean(convolved, axis=-1, keepdims=True)
        scaled = (
            centered
            * lax.rsqrt(jnp.mean(centered * centered, axis=-1, keepdims=True) + NORM_EPSILON)
            * conv_gain_ref[...]
        )
        activated = (scaled * jax.nn.sigmoid(scaled)).astype(jnp.bfloat16)
        pointwise = jnp.dot(activated, point_ref[...], preferred_element_type=jnp.float32)
        out_ref[:, :width] = (
            attended
            * lax.rsqrt(jnp.mean(attended * attended, axis=-1, keepdims=True) + NORM_EPSILON)
            * gain_ref[:, :width]
        ).astype(jnp.bfloat16)
        out_ref[:, width:] = (
            pointwise
            * lax.rsqrt(jnp.mean(pointwise * pointwise, axis=-1, keepdims=True) + NORM_EPSILON)
            * gain_ref[:, width:]
        ).astype(jnp.bfloat16)

    return pl.pallas_call(
        body,
        out_shape=jax.ShapeDtypeStruct((rows, output_gain.shape[0]), jnp.bfloat16),
        compiler_params=pltpu.CompilerParams(vmem_limit_bytes=12 << 20),
        name="merge_mixers",
    )(exchanged, conv_gain[None], point_weight, output_gain[None])


def gather_shares(share, lines, tp_size):
    def number(line, side, lane):
        return (line * 2 + side) * tp_size + lane

    def send(block, target):
        found = []
        for line in range(lines):
            for side in range(2):
                for lane in range(tp_size):
                    to_line, to_side, to_lane = target(line, side, lane)
                    if 0 <= to_line < lines:
                        found.append((number(line, side, lane), number(to_line, to_side, to_lane)))
        return lax.ppermute(block, PLACE, found)

    def beside(line, side, lane):
        return (line + 1 if lane % 2 == 0 else line - 1), side, lane

    def beyond(line, side, lane):
        targets = far_lines(line, lines)
        if lane % 2 >= len(targets):
            return -1, side, lane
        to_line = targets[lane % 2]
        return to_line, side, lane - lane % 2 + far_lines(to_line, lines).index(line)

    def across(line, side, lane):
        return line, 1 - side, lane

    def lanes(line, side, lane):
        return line, side, lane ^ 1

    near = send(share, beside)
    far = send(share, beyond)
    half_rows = share.shape[0] // 2
    half = lax.dynamic_slice_in_dim(share, lax.axis_index("tp") % 2 * half_rows, half_rows, axis=0)
    traded = send(jnp.concatenate([near, half], axis=0), across)
    far_across = send(far, across)
    near_here = jnp.concatenate([near, traded], axis=0)
    near_there = send(near_here, lanes)
    far_there = send(far, lanes)
    far_across_there = send(far_across, lanes)
    return near_here, near_there, (far, far_there, far_across, far_across_there)


def far_lines(line, lines):
    return [other for other in range(lines) if abs(other - line) > 1]


def place_of_device():
    position, lane = lax.axis_index("sp"), lax.axis_index("tp") % 2
    return position // 2, position % 2, lane


def columns_of(merged_ref, from_line, sides, share_rows):
    found = []
    for at_side in sides:
        start = pl.multiple_of((from_line * 2 + at_side) * share_rows, share_rows)
        found.append(merged_ref[:, pl.ds(start, share_rows)])
    return jnp.concatenate(found, axis=1)


def near_product(merged, share, near_here, near_there, lines):
    rows, _ = merged.shape
    share_rows, columns = share.shape
    half_rows = share_rows // 2

    def body(merged_ref, share_ref, here_ref, there_ref, out_ref, pair):
        line, side, lane = place_of_device()

        def product(from_line, left):
            return jnp.dot(
                columns_of(merged_ref, from_line, (side, 1 - side), share_rows),
                left,
                preferred_element_type=jnp.float32,
            )

        pair[:share_rows] = share_ref[...]
        for ref, at_lane in ((here_ref, lane), (there_ref, 1 - lane)):
            start = pl.multiple_of(share_rows + at_lane * half_rows, half_rows)
            pair[pl.ds(start, half_rows)] = ref[2 * share_rows :]
        out_ref[...] = product(line, pair[...])

        for ref, at_lane in ((here_ref, lane), (there_ref, 1 - lane)):
            from_line = line - 1 + 2 * at_lane

            @pl.when((from_line >= 0) & (from_line < lines))
            def _():
                out_ref[...] += product(from_line, ref[: 2 * share_rows])

    vmem = pl.BlockSpec(memory_space=pltpu.VMEM)
    return pl.pallas_call(
        body,
        in_specs=[vmem] * 4,
        out_specs=vmem,
        out_shape=jax.ShapeDtypeStruct((rows, columns), jnp.float32),
        scratch_shapes=[pltpu.VMEM((2 * share_rows, columns), jnp.bfloat16)],
        compiler_params=pltpu.CompilerParams(vmem_limit_bytes=16 << 20),
        name="near_product",
    )(merged, share, near_here, near_there)


def far_product(merged, near_sum, far_pieces, lines):
    rows, _ = merged.shape
    share_rows, columns = far_pieces[0].shape
    chunk = 512

    def body(merged_ref, near_ref, *refs):
        piece_refs, out_hbm, rounded, sent = refs[:4], refs[4], refs[5], refs[6]
        line, side, lane = place_of_device()
        before = jnp.maximum(line - 1, 0)

        def other_line(index):
            found = jnp.where(index < before, index, line + 2 + index - before)
            return jnp.where(found < lines, found, -1)

        sources = [other_line(lane), other_line(1 - lane)]

        def finish(slots):
            left = [
                columns_of(merged_ref, sources[slot], (side, 1 - side), share_rows)
                for slot in slots
            ]
            left = jnp.concatenate(left, axis=1) if left else None
            copies = []
            for first in range(0, columns, chunk):
                here = slice(first, first + chunk)
                total = near_ref[:, here]
                if slots:
                    right = [piece_refs[2 * i + slot][:, here] for slot in slots for i in range(2)]
                    total = total + jnp.dot(
                        left, jnp.concatenate(right, axis=0), preferred_element_type=jnp.float32
                    )
                rounded[:, here] = total.astype(rounded.dtype)
                copies.append(
                    pltpu.make_async_copy(
                        rounded.at[:, pl.ds(first, chunk)],
                        out_hbm.at[:, pl.ds(first, chunk)],
                        sent.at[first // chunk],
                    )
                )
                copies[-1].start()
            for copy in copies:
                copy.wait()

        for slots in ((0, 1), (0,), (1,), ()):
            wanted = [(sources[slot] >= 0) == (slot in slots) for slot in range(2)]

            @pl.when(wanted[0] & wanted[1])
            def _():
                finish(slots)

    vmem = pl.BlockSpec(memory_space=pltpu.VMEM)
    return pl.pallas_call(
        body,
        in_specs=[vmem] * 6,
        out_specs=pl.BlockSpec(memory_space=pl.ANY),
        out_shape=pltpu.HBM((rows, columns), jnp.bfloat16),
        scratch_shapes=[
            pltpu.VMEM((rows, columns), jnp.bfloat16),
            pltpu.SemaphoreType.DMA((columns // chunk,)),
        ],
        compiler_params=pltpu.CompilerParams(vmem_limit_bytes=16 << 20),
        name="far_product",
    )(merged, near_sum, *far_pieces)


def on_device(
    tokens,
    norm_gain,
    query_weight,
    key_weight,
    value_weight,
    sink_logits,
    conv_in_weight,
    conv_gate_weight,
    conv_taps,
    conv_gain,
    point_weight,
    output_gain,
    output_weight,
):
    sp_size, tp_size = lax.axis_size("sp"), lax.axis_size("tp")
    lines = sp_size // 2
    by_shares = sends_shares(sp_size, tp_size)
    if by_shares:
        near_here, near_there, far_pieces = gather_shares(output_weight, lines, tp_size)
    queries, pairs, gated, tail = project_inputs(
        tokens, norm_gain, query_weight, key_weight, value_weight, conv_in_weight, conv_gate_weight
    )
    earlier = from_behind(tail, "sp", 1)
    mixed = mix_rows(queries, pairs, gated, earlier, sink_logits, conv_taps, tp_size)
    exchanged = lax.all_to_all(mixed, "tp", split_axis=0, concat_axis=0, tiled=True)
    merged = merge_mixers(exchanged, conv_gain, point_weight, output_gain)
    if by_shares:
        near_sum = near_product(merged, output_weight, near_here, near_there, lines)
        return far_product(merged, near_sum, far_pieces, lines)
    projected = jnp.dot(
        merged,
        lax.all_gather(output_weight, "sp", axis=0, tiled=True),
        preferred_element_type=jnp.float32,
    )
    return projected.astype(jnp.bfloat16)


def sends_shares(sp_size, tp_size):
    return sp_size % 2 == 0 and tp_size % 2 == 0 and 3 <= sp_size // 2 <= 4


def solution(mesh):
    in_specs = (
        P("sp", None),
        P(),
        P(None, "tp"),
        P(None, "tp"),
        P(None, "tp"),
        P("tp"),
        P(None, "tp"),
        P(None, "tp"),
        P(),
        P(),
        P(),
        P(),
        P("sp", None),
    )
    out_specs = P(("sp", "tp"), None)
    return jax.shard_map(
        on_device, mesh=mesh, in_specs=in_specs, out_specs=out_specs, check_vma=False
    )
```

profile of v0, /device:TPU:24, one launch (start us, length us, event | category | flops | bytes accessed | tf_op | source)
XLA Modules:
  0.0 76.5 jit_solution(16438123992292349861)
XLA Ops:
  0.0 1.4 %collective-permute-start.1 = (bf16[128,2048]{1,0:T(8,128)(2,1)}, bf16[128,2048]{1,0:T(8,128)(2,1)S(1)}, u32[]{:S(2)}, u32[]{:S(2)}) collective-permute-start(bf16[128,2048]{1,0:T(8,128)(2,1)} %share_ref.1), channel_id=1, source_target_pairs={{0,8},{2,10},{4,12},{6,14},{8,16},{9,1},{10,18},{11,3},{12,20},{13... | collective-permute-start | bytes 1572872 | tf_op jit(solution)/shard_map/ppermute | solution.py:245
  1.4 1.0 %constant_dynamic-slice_fusion = bf16[64,2048]{1,0:T(8,128)(2,1)S(1)} fusion(bf16[128,2048]{1,0:T(8,128)(2,1)} %share_ref.1, s32[]{:T(128)S(6)} %select_n.11), kind=kLoop, calls=%fused_computation.3 | loop fusion | bytes 524292 | tf_op jit(solution)/shard_map/dynamic_slice | solution.py:266
  2.4 9.0 %collective-permute-done.1 = bf16[128,2048]{1,0:T(8,128)(2,1)S(1)} collective-permute-done((bf16[128,2048]{1,0:T(8,128)(2,1)}, bf16[128,2048]{1,0:T(8,128)(2,1)S(1)}, u32[]{:S(2)}, u32[]{:S(2)}) %collective-permute-start.1) | collective-permute-done | bytes 524320 | tf_op jit(solution)/shard_map/ppermute | solution.py:245
  11.4 0.1 pad_maximum_fusion
  11.5 1.6 %collective-permute-start.2 = (bf16[192,2048]{1,0:T(8,128)(2,1)S(1)}, bf16[192,2048]{1,0:T(8,128)(2,1)S(1)}, u32[]{:S(2)}, u32[]{:S(2)}) collective-permute-start(bf16[192,2048]{1,0:T(8,128)(2,1)S(1)} %pad_maximum_fusion), channel_id=1, source_target_pairs={{0,4},{1,5},{2,6},{3,7},{4,0},{5,1},{6,2},{7,3},{8,12},{9,13},{10,... | collective-permute-start | bytes 2359304 | tf_op jit(solution)/shard_map/ppermute | solution.py:245
  13.0 1.9 %collective-permute-start.4 = (bf16[128,2048]{1,0:T(8,128)(2,1)S(1)}, bf16[128,2048]{1,0:T(8,128)(2,1)S(1)}, u32[]{:S(2)}, u32[]{:S(2)}) collective-permute-start(bf16[128,2048]{1,0:T(8,128)(2,1)S(1)} %copy-done), channel_id=1, source_target_pairs={{0,16},{1,24},{2,18},{3,26},{4,20},{5,28},{6,22},{7,30},{8,25},{10... | collective-permute-start | bytes 1572872 | tf_op jit(solution)/shard_map/ppermute | solution.py:245
  15.0 13.0 %collective-permute-done.2 = bf16[192,2048]{1,0:T(8,128)(2,1)S(1)} collective-permute-done((bf16[192,2048]{1,0:T(8,128)(2,1)S(1)}, bf16[192,2048]{1,0:T(8,128)(2,1)S(1)}, u32[]{:S(2)}, u32[]{:S(2)}) %collective-permute-start.2) | collective-permute-done | bytes 786464 | tf_op jit(solution)/shard_map/ppermute | solution.py:245
  28.0 0.1 constant_dynamic-update-slice_fusion.here_ref
  28.1 0.1 collective-permute-start.3
  28.2 2.4 %collective-permute-done.4.refs_0_ = bf16[128,2048]{1,0:T(8,128)(2,1)S(1)} collective-permute-done((bf16[128,2048]{1,0:T(8,128)(2,1)S(1)}, bf16[128,2048]{1,0:T(8,128)(2,1)S(1)}, u32[]{:S(2)}, u32[]{:S(2)}) %collective-permute-start.4) | collective-permute-done | bytes 524320 | tf_op jit(solution)/shard_map/ppermute | solution.py:245
  30.6 0.5 collective-permute-start.6
  31.1 2.6 %collective-permute-start.5 = (bf16[128,2048]{1,0:T(8,128)(2,1)S(1)}, bf16[128,2048]{1,0:T(8,128)(2,1)S(1)}, u32[]{:S(2)}, u32[]{:S(2)}) collective-permute-start(bf16[128,2048]{1,0:T(8,128)(2,1)S(1)} %collective-permute-done.4.refs_0_), channel_id=1, source_target_pairs={{0,1},{1,0},{2,3},{3,2},{4,5},{5,4},{6,7},{7,6},{8,9},{9,8},{10,11... | collective-permute-start | bytes 1572872 | tf_op jit(solution)/shard_map/ppermute | solution.py:245
  33.7 9.8 %collective-permute-done.6.refs_2_ = bf16[128,2048]{1,0:T(8,128)(2,1)S(1)} collective-permute-done((bf16[128,2048]{1,0:T(8,128)(2,1)S(1)}, bf16[128,2048]{1,0:T(8,128)(2,1)S(1)}, u32[]{:S(2)}, u32[]{:S(2)}) %collective-permute-start.6) | collective-permute-done | bytes 524320 | tf_op jit(solution)/shard_map/ppermute | solution.py:245
  43.5 1.7 %collective-permute-start.7 = (bf16[128,2048]{1,0:T(8,128)(2,1)S(1)}, bf16[128,2048]{1,0:T(8,128)(2,1)S(1)}, u32[]{:S(2)}, u32[]{:S(2)}) collective-permute-start(bf16[128,2048]{1,0:T(8,128)(2,1)S(1)} %collective-permute-done.6.refs_2_), channel_id=1, source_target_pairs={{0,1},{1,0},{2,3},{3,2},{4,5},{5,4},{6,7},{7,6},{8,9},{9,8},{10,11... | collective-permute-start | bytes 1572872 | tf_op jit(solution)/shard_map/ppermute | solution.py:245
  45.2 5.8 %project_inputs.1 = (bf16[1024,128]{1,0:T(8,128)(2,1)S(1)}, bf16[1024,128]{1,0:T(8,128)(2,1)S(1)}, bf16[1024,128]{1,0:T(8,128)(2,1)S(1)}, bf16[160,128]{1,0:T(8,128)(2,1)S(1)}) custom-call(f32[1,2048]{1,0:T(1,128)} %bitcast.9, bf16[1024,2048]{1,0:T(8,128)(2,1)} %tokens_hbm.1, bf16[2048,128]{1,0:T(8,128)(2,1)} %query_hbm.1, bf16[64,2048]{1,0:T(8,128)(2,1)} %bitcast.7, ...), custom_call_target="tpu_custom_call" | custom-call | tf_op jit(solution)/shard_map/project_inputs/pallas_call | solution.py:105
  51.0 0.0 copy-start.1
  51.0 0.0 copy-start.3
  51.1 2.6 %collective-permute-start = (bf16[160,128]{1,0:T(8,128)(2,1)S(1)}, bf16[160,128]{1,0:T(8,128)(2,1)S(1)}, u32[]{:S(2)}, u32[]{:S(2)}) collective-permute-start(bf16[160,128]{1,0:T(8,128)(2,1)S(1)} %get-tuple-element.12), channel_id=1, source_target_pairs={{0,4},{4,8},{8,12},{12,16},{16,20},{20,24},{24,28},{1,5},{5,9},{9,... | collective-permute-start | bytes 122888 | tf_op jit(solution)/shard_map/ppermute | solution.py:25
  53.6 4.3 %collective-permute-done.earlier_ref = bf16[160,128]{1,0:T(8,128)(2,1)S(1)} collective-permute-done((bf16[160,128]{1,0:T(8,128)(2,1)S(1)}, bf16[160,128]{1,0:T(8,128)(2,1)S(1)}, u32[]{:S(2)}, u32[]{:S(2)}) %collective-permute-start) | collective-permute-done | bytes 40992 | tf_op jit(solution)/shard_map/ppermute | solution.py:25
  58.0 3.9 %mix_rows.1 = bf16[4,256,256]{2,1,0:T(8,128)(2,1)S(1)} custom-call(f32[2]{0:T(128)S(1)} %copy-done.5, bf16[1024,128]{1,0:T(8,128)(2,1)S(1)} %get-tuple-element.9.queries_ref, bf16[1024,128]{1,0:T(8,128)(2,1)S(1)} %get-tuple-element.10.pairs_ref, bf16[1024,128]{1,0:T(8,128)(2,1)S(1)} %get-tuple-element.11.gated_ref, ...), custom_call_target="tpu_custom_call" | custom-call | tf_op jit(solution)/shard_map/mix_rows/pallas_call | solution.py:180
  61.9 11.4 %all_to_all.5.exchanged_ref = bf16[4,256,256]{2,1,0:T(8,128)(2,1)S(1)} all-to-all(bf16[4,256,256]{2,1,0:T(8,128)(2,1)S(1)} %mix_rows.1), channel_id=1, replica_groups=mesh['sp'=8,'tp'=4] {'tp'}, dimensions={0} | all-to-all | bytes 1048576 | tf_op jit(solution)/shard_map/all_to_all | solution.py:423
  73.3 0.6 merge_mixers.1.merged_ref
  74.0 1.0 %near_product.1.near_ref = f32[256,2048]{1,0:T(8,128)S(1)} custom-call(bf16[256,1024]{1,0:T(8,128)(2,1)S(1)} %merge_mixers.1.merged_ref, bf16[128,2048]{1,0:T(8,128)(2,1)S(1)} %copy-done, bf16[320,2048]{1,0:T(8,128)(2,1)S(1)} %constant_dynamic-update-slice_fusion.here_ref, bf16[320,2048]{1,0:T(8,128)(2,1)S(1)} %collective-permute-done.3.there_ref), custom_call_target="tpu_custom_call" | custom-call | tf_op jit(solution)/shard_map/near_product/pallas_call | solution.py:322
  75.0 1.5 %far_product.1 = bf16[256,2048]{1,0:T(8,128)(2,1)} custom-call(bf16[256,1024]{1,0:T(8,128)(2,1)S(1)} %merge_mixers.1.merged_ref, f32[256,2048]{1,0:T(8,128)S(1)} %near_product.1.near_ref, bf16[128,2048]{1,0:T(8,128)(2,1)S(1)} %collective-permute-done.4.refs_0_, bf16[128,2048]{1,0:T(8,128)(2,1)S(1)} %collective-permute-done.5.refs_1_, ...), custom_call_target="tpu_custom_call" | custom-call | tf_op jit(solution)/shard_map/far_product/pallas_call | solution.py:384
  (14 shorter events, 0.1 us)
Async XLA Ops:
  0.0 13.0 %copy-start = (bf16[128,2048]{1,0:T(8,128)(2,1)S(1)}, bf16[128,2048]{1,0:T(8,128)(2,1)}, u32[]{:S(2)}) copy-start(bf16[128,2048]{1,0:T(8,128)(2,1)} %share_ref.1) | copy-start | bytes 1572868
  0.0 11.4 %collective-permute-start.1 = (bf16[128,2048]{1,0:T(8,128)(2,1)}, bf16[128,2048]{1,0:T(8,128)(2,1)S(1)}, u32[]{:S(2)}, u32[]{:S(2)}) collective-permute-start(bf16[128,2048]{1,0:T(8,128)(2,1)} %share_ref.1), channel_id=1, source_target_pairs={{0,8},{2,10},{4,12},{6,14},{8,16},{9,1},{10,18},{11,3},{12,20},{13... | collective-permute-start | bytes 1572872 | tf_op jit(solution)/shard_map/ppermute | solution.py:245
  11.5 16.6 %collective-permute-start.2 = (bf16[192,2048]{1,0:T(8,128)(2,1)S(1)}, bf16[192,2048]{1,0:T(8,128)(2,1)S(1)}, u32[]{:S(2)}, u32[]{:S(2)}) collective-permute-start(bf16[192,2048]{1,0:T(8,128)(2,1)S(1)} %pad_maximum_fusion), channel_id=1, source_target_pairs={{0,4},{1,5},{2,6},{3,7},{4,0},{5,1},{6,2},{7,3},{8,12},{9,13},{10,... | collective-permute-start | bytes 2359304 | tf_op jit(solution)/shard_map/ppermute | solution.py:245
  13.0 17.6 %collective-permute-start.4 = (bf16[128,2048]{1,0:T(8,128)(2,1)S(1)}, bf16[128,2048]{1,0:T(8,128)(2,1)S(1)}, u32[]{:S(2)}, u32[]{:S(2)}) collective-permute-start(bf16[128,2048]{1,0:T(8,128)(2,1)S(1)} %copy-done), channel_id=1, source_target_pairs={{0,16},{1,24},{2,18},{3,26},{4,20},{5,28},{6,22},{7,30},{8,25},{10... | collective-permute-start | bytes 1572872 | tf_op jit(solution)/shard_map/ppermute | solution.py:245
  28.1 45.9 %collective-permute-start.3 = (bf16[320,2048]{1,0:T(8,128)(2,1)S(1)}, bf16[320,2048]{1,0:T(8,128)(2,1)S(1)}, u32[]{:S(2)}, u32[]{:S(2)}) collective-permute-start(bf16[320,2048]{1,0:T(8,128)(2,1)S(1)} %constant_dynamic-update-slice_fusion.here_ref), channel_id=1, source_target_pairs={{0,1},{1,0},{2,3},{3,2},{4,5},{5,4},{6,7},{7,6},{8,9},{9,8},{10,11... | collective-permute-start | bytes 3932168 | tf_op jit(solution)/shard_map/ppermute | solution.py:245
  30.6 12.9 %collective-permute-start.6 = (bf16[128,2048]{1,0:T(8,128)(2,1)S(1)}, bf16[128,2048]{1,0:T(8,128)(2,1)S(1)}, u32[]{:S(2)}, u32[]{:S(2)}) collective-permute-start(bf16[128,2048]{1,0:T(8,128)(2,1)S(1)} %collective-permute-done.4.refs_0_), channel_id=1, source_target_pairs={{0,4},{1,5},{2,6},{3,7},{4,0},{5,1},{6,2},{7,3},{8,12},{9,13},{10,... | collective-permute-start | bytes 1572872 | tf_op jit(solution)/shard_map/ppermute | solution.py:245
  31.1 43.8 %collective-permute-start.5 = (bf16[128,2048]{1,0:T(8,128)(2,1)S(1)}, bf16[128,2048]{1,0:T(8,128)(2,1)S(1)}, u32[]{:S(2)}, u32[]{:S(2)}) collective-permute-start(bf16[128,2048]{1,0:T(8,128)(2,1)S(1)} %collective-permute-done.4.refs_0_), channel_id=1, source_target_pairs={{0,1},{1,0},{2,3},{3,2},{4,5},{5,4},{6,7},{7,6},{8,9},{9,8},{10,11... | collective-permute-start | bytes 1572872 | tf_op jit(solution)/shard_map/ppermute | solution.py:245
  43.5 31.5 %collective-permute-start.7 = (bf16[128,2048]{1,0:T(8,128)(2,1)S(1)}, bf16[128,2048]{1,0:T(8,128)(2,1)S(1)}, u32[]{:S(2)}, u32[]{:S(2)}) collective-permute-start(bf16[128,2048]{1,0:T(8,128)(2,1)S(1)} %collective-permute-done.6.refs_2_), channel_id=1, source_target_pairs={{0,1},{1,0},{2,3},{3,2},{4,5},{5,4},{6,7},{7,6},{8,9},{9,8},{10,11... | collective-permute-start | bytes 1572872 | tf_op jit(solution)/shard_map/ppermute | solution.py:245
  45.2 12.8 %copy-start.2 = (bf16[31,512]{1,0:T(8,128)(2,1)S(1)}, bf16[31,512]{1,0:T(8,128)(2,1)}, u32[]{:S(2)}) copy-start(bf16[31,512]{1,0:T(8,128)(2,1)} %taps_ref.1) | copy-start | bytes 95236
  45.2 12.8 %copy-start.5 = (f32[2]{0:T(128)S(1)}, f32[2]{0:T(128)}, u32[]{:S(2)}) copy-start(f32[2]{0:T(128)} %sinks_ref.1) | copy-start | bytes 28
  51.0 22.3 %copy-start.1 = (bf16[512,512]{1,0:T(8,128)(2,1)S(1)}, bf16[512,512]{1,0:T(8,128)(2,1)}, u32[]{:S(2)}) copy-start(bf16[512,512]{1,0:T(8,128)(2,1)} %point_ref.1) | copy-start | bytes 1572868
  51.0 22.3 %copy-start.3 = (f32[1024]{0:T(1024)S(1)}, f32[1024]{0:T(1024)}, u32[]{:S(2)}) copy-start(f32[1024]{0:T(1024)} %param.24) | copy-start | bytes 12292
  51.1 22.3 %copy-start.4 = (f32[512]{0:T(512)S(1)}, f32[512]{0:T(512)}, u32[]{:S(2)}) copy-start(f32[512]{0:T(512)} %param.22) | copy-start | bytes 6148
  51.1 6.9 %collective-permute-start = (bf16[160,128]{1,0:T(8,128)(2,1)S(1)}, bf16[160,128]{1,0:T(8,128)(2,1)S(1)}, u32[]{:S(2)}, u32[]{:S(2)}) collective-permute-start(bf16[160,128]{1,0:T(8,128)(2,1)S(1)} %get-tuple-element.12), channel_id=1, source_target_pairs={{0,4},{4,8},{8,12},{12,16},{16,20},{20,24},{24,28},{1,5},{5,9},{9,... | collective-permute-start | bytes 122888 | tf_op jit(solution)/shard_map/ppermute | solution.py:25
where the time goes:
time: 76.7 us; the launch traced here: 76.5 us
  waiting for transfers between devices  38.6 us (50%)
  Pallas kernels  12.8 us (17%)
  starting transfers between devices  12.4 us (16%)
  blocking collectives  11.4 us (15%)
  local copies, waits for them, and re-layouts  1.09 us (1%)
    ppermute x7, waiting for transfers between devices, send(): return lax.ppermute(block, PLACE, found)  34.2 us
    all_to_all x1, blocking collectives, on_device(): lax.all_to_all(mixed, 'tp', split_axis=0, concat_axis=0, tiled=True)  11.4 us
    ppermute x7, starting transfers between devices, send(): return lax.ppermute(block, PLACE, found)  9.81 us
    pallas_call x1, Pallas kernels, project_inputs(): pl.pallas_call(body, in_specs=[pl.BlockSpec(memory_space=pl.ANY)] * 7, ou...  5.81 us
    ppermute x1, waiting for transfers between devices, from_behind(): return lax.ppermute(block, axis, route)  4.34 us
    pallas_call x1, Pallas kernels, mix_rows(): pl.pallas_call(body, in_specs=[scalars] + [whole] * 5, out_specs=whole, o...  3.93 us
    ppermute x1, starting transfers between devices, from_behind(): return lax.ppermute(block, axis, route)  2.58 us
  transfers between devices with their start and end apart: 8, of which 5 were waited for; matrix products, arithmetic and copies ran while one was open for 1% of the time, Pallas kernels for 15%

commit v1 on v0

--- a/solution.py
+++ b/solution.py
@@ -252,25 +252,34 @@
         if lane % 2 >= len(targets):
             return -1, side, lane
         to_line = targets[lane % 2]
-        return to_line, side, lane - lane % 2 + far_lines(to_line, lines).index(line)
-
-    def across(line, side, lane):
-        return line, 1 - side, lane
+        to_side = 1 - side if lane // 2 % 2 else side
+        return to_line, to_side, lane - lane % 2 + far_lines(to_line, lines).index(line)
+
+    def lower_lane_across(line, side, lane):
+        return (line if lane % 2 == 0 else -1), 1 - side, lane
+
+    def holders_across(line, side, lane):
+        from_line = line - 1 if lane % 2 == 0 else line + 1
+        return (line if 0 <= from_line < lines else -1), 1 - side, lane
+
+    def holders_to_neighbours(line, side, lane):
+        held = lane % 2 < len(far_lines(line, lines))
+        to = (1 - side, lane) if lane % 2 == 0 else (side, lane ^ 2)
+        return (line if held else -1), *to
 
     def lanes(line, side, lane):
         return line, side, lane ^ 1
 
     near = send(share, beside)
+    opposite = send(share, lower_lane_across)
+    near_across = send(near, holders_across)
     far = send(share, beyond)
-    half_rows = share.shape[0] // 2
-    half = lax.dynamic_slice_in_dim(share, lax.axis_index("tp") % 2 * half_rows, half_rows, axis=0)
-    traded = send(jnp.concatenate([near, half], axis=0), across)
-    far_across = send(far, across)
-    near_here = jnp.concatenate([near, traded], axis=0)
+    far_other = send(far, holders_to_neighbours)
+    near_here = jnp.concatenate([near, near_across, opposite], axis=0)
     near_there = send(near_here, lanes)
     far_there = send(far, lanes)
-    far_across_there = send(far_across, lanes)
-    return near_here, near_there, (far, far_there, far_across, far_across_there)
+    far_other_there = send(far_other, lanes)
+    return near_here, near_there, (far, far_there, far_other, far_other_there)
 
 
 def far_lines(line, lines):
@@ -293,9 +302,8 @@
 def near_product(merged, share, near_here, near_there, lines):
     rows, _ = merged.shape
     share_rows, columns = share.shape
-    half_rows = share_rows // 2
-
-    def body(merged_ref, share_ref, here_ref, there_ref, out_ref, pair):
+
+    def body(merged_ref, share_ref, here_ref, there_ref, out_ref):
         line, side, lane = place_of_device()
 
         def product(from_line, left):
@@ -305,11 +313,12 @@
                 preferred_element_type=jnp.float32,
             )
 
-        pair[:share_rows] = share_ref[...]
-        for ref, at_lane in ((here_ref, lane), (there_ref, 1 - lane)):
-            start = pl.multiple_of(share_rows + at_lane * half_rows, half_rows)
-            pair[pl.ds(start, half_rows)] = ref[2 * share_rows :]
-        out_ref[...] = product(line, pair[...])
+        for ref, holds in ((here_ref, lane == 0), (there_ref, lane == 1)):
+
+            @pl.when(holds)
+            def _():
+                pair = jnp.concatenate([share_ref[...], ref[2 * share_rows :]], axis=0)
+                out_ref[...] = product(line, pair)
 
         for ref, at_lane in ((here_ref, lane), (there_ref, 1 - lane)):
             from_line = line - 1 + 2 * at_lane
@@ -324,7 +333,6 @@
         in_specs=[vmem] * 4,
         out_specs=vmem,
         out_shape=jax.ShapeDtypeStruct((rows, columns), jnp.float32),
-        scratch_shapes=[pltpu.VMEM((2 * share_rows, columns), jnp.bfloat16)],
         compiler_params=pltpu.CompilerParams(vmem_limit_bytes=16 << 20),
         name="near_product",
     )(merged, share, near_here, near_there)
@@ -338,6 +346,7 @@
     def body(merged_ref, near_ref, *refs):
         piece_refs, out_hbm, rounded, sent = refs[:4], refs[4], refs[5], refs[6]
         line, side, lane = place_of_device()
+        first_side = jnp.where(lax.axis_index("tp") // 2 % 2 == 1, 1 - side, side)
         before = jnp.maximum(line - 1, 0)
 
         def other_line(index):
@@ -348,7 +357,7 @@
 
         def finish(slots):
             left = [
-                columns_of(merged_ref, sources[slot], (side, 1 - side), share_rows)
+                columns_of(merged_ref, sources[slot], (first_side, 1 - first_side), share_rows)
                 for slot in slots
             ]
             left = jnp.concatenate(left, axis=1) if left else None
@@ -434,7 +443,7 @@
 
 
 def sends_shares(sp_size, tp_size):
-    return sp_size % 2 == 0 and tp_size % 2 == 0 and 3 <= sp_size // 2 <= 4
+    return sp_size % 2 == 0 and tp_size % 4 == 0 and 3 <= sp_size // 2 <= 4
 
 
 def solution(mesh):

time: 76.7 us -> 94.5 us (1.23)
  the two profiles are of different devices: /device:TPU:24 before, /device:TPU:0 now
where the time goes in v1:
time: 94.5 us; the launch traced here: 94.1 us
  waiting for transfers between devices  42.8 us (45%)
  starting transfers between devices  26.8 us (28%)
  Pallas kernels  12.8 us (14%)
  blocking collectives  11.4 us (12%)
    ppermute x8, waiting for transfers between devices, send(): return lax.ppermute(block, PLACE, found)  41.2 us
    ppermute x8, starting transfers between devices, send(): return lax.ppermute(block, PLACE, found)  23.3 us
    all_to_all x1, blocking collectives, on_device(): lax.all_to_all(mixed, 'tp', split_axis=0, concat_axis=0, tiled=True)  11.4 us
    pallas_call x1, Pallas kernels, project_inputs(): pl.pallas_call(body, in_specs=[pl.BlockSpec(memory_space=pl.ANY)] * 7, ou...  5.82 us
    pallas_call x1, Pallas kernels, mix_rows(): pl.pallas_call(body, in_specs=[scalars] + [whole] * 5, out_specs=whole, o...  3.93 us
    ppermute x1, starting transfers between devices, from_behind(): return lax.ppermute(block, axis, route)  3.53 us
  transfers between devices with their start and end apart: 9, of which 5 were waited for; matrix products, arithmetic and copies ran while one was open for 0% of the time, Pallas kernels for 12%

profile of v1, /device:TPU:0, one launch (start us, length us, event | category | flops | bytes accessed | tf_op | source)
XLA Modules:
  0.0 94.1 jit_solution(6735031587954836741)
XLA Ops:
  0.0 5.1 %collective-permute-start.1 = (bf16[128,2048]{1,0:T(8,128)(2,1)}, bf16[128,2048]{1,0:T(8,128)(2,1)S(1)}, u32[]{:S(2)}, u32[]{:S(2)}) collective-permute-start(bf16[128,2048]{1,0:T(8,128)(2,1)} %share_ref.1), channel_id=1, source_target_pairs={{0,8},{2,10},{4,12},{6,14},{8,16},{9,1},{10,18},{11,3},{12,20},{13... | collective-permute-start | bytes 1572872 | tf_op jit(solution)/shard_map/ppermute | solution.py:245
  5.1 7.0 %collective-permute-done.1 = bf16[128,2048]{1,0:T(8,128)(2,1)S(1)} collective-permute-done((bf16[128,2048]{1,0:T(8,128)(2,1)}, bf16[128,2048]{1,0:T(8,128)(2,1)S(1)}, u32[]{:S(2)}, u32[]{:S(2)}) %collective-permute-start.1) | collective-permute-done | bytes 524320 | tf_op jit(solution)/shard_map/ppermute | solution.py:245
  12.1 0.7 collective-permute-start.2
  12.8 3.4 %collective-permute-start.3 = (bf16[128,2048]{1,0:T(8,128)(2,1)}, bf16[128,2048]{1,0:T(8,128)(2,1)S(1)}, u32[]{:S(2)}, u32[]{:S(2)}) collective-permute-start(bf16[128,2048]{1,0:T(8,128)(2,1)} %share_ref.1), channel_id=1, source_target_pairs={{0,4},{2,6},{4,0},{6,2},{8,12},{10,14},{12,8},{14,10},{16,20},{18,... | collective-permute-start | bytes 1572872 | tf_op jit(solution)/shard_map/ppermute | solution.py:245
  16.2 0.0 collective-permute-done.2
  16.3 10.8 %collective-permute-done.3 = bf16[128,2048]{1,0:T(8,128)(2,1)S(1)} collective-permute-done((bf16[128,2048]{1,0:T(8,128)(2,1)}, bf16[128,2048]{1,0:T(8,128)(2,1)S(1)}, u32[]{:S(2)}, u32[]{:S(2)}) %collective-permute-start.3) | collective-permute-done | bytes 524320 | tf_op jit(solution)/shard_map/ppermute | solution.py:245
  27.2 0.1 collective-permute-start.4
  27.3 10.6 %collective-permute-start.5 = (bf16[128,2048]{1,0:T(8,128)(2,1)S(1)}, bf16[128,2048]{1,0:T(8,128)(2,1)S(1)}, u32[]{:S(2)}, u32[]{:S(2)}) collective-permute-start(bf16[128,2048]{1,0:T(8,128)(2,1)S(1)} %copy-done), channel_id=1, source_target_pairs={{0,16},{1,24},{2,22},{3,30},{4,20},{5,28},{6,18},{7,26},{8,25},{10... | collective-permute-start | bytes 1572872 | tf_op jit(solution)/shard_map/ppermute | solution.py:245
  37.8 15.8 %collective-permute-done.5.refs_0_ = bf16[128,2048]{1,0:T(8,128)(2,1)S(1)} collective-permute-done((bf16[128,2048]{1,0:T(8,128)(2,1)S(1)}, bf16[128,2048]{1,0:T(8,128)(2,1)S(1)}, u32[]{:S(2)}, u32[]{:S(2)}) %collective-permute-start.5) | collective-permute-done | bytes 524320 | tf_op jit(solution)/shard_map/ppermute | solution.py:245
  53.6 3.4 %collective-permute-start.7 = (bf16[128,2048]{1,0:T(8,128)(2,1)S(1)}, bf16[128,2048]{1,0:T(8,128)(2,1)S(1)}, u32[]{:S(2)}, u32[]{:S(2)}) collective-permute-start(bf16[128,2048]{1,0:T(8,128)(2,1)S(1)} %collective-permute-done.5.refs_0_), channel_id=1, source_target_pairs={{0,4},{1,3},{2,6},{3,1},{4,0},{5,7},{6,2},{7,5},{8,12},{10,14},{12... | collective-permute-start | bytes 1572872 | tf_op jit(solution)/shard_map/ppermute | solution.py:245
  57.0 0.1 collective-permute-start.6
  57.1 7.6 %collective-permute-done.7.refs_2_ = bf16[128,2048]{1,0:T(8,128)(2,1)S(1)} collective-permute-done((bf16[128,2048]{1,0:T(8,128)(2,1)S(1)}, bf16[128,2048]{1,0:T(8,128)(2,1)S(1)}, u32[]{:S(2)}, u32[]{:S(2)}) %collective-permute-start.7) | collective-permute-done | bytes 524320 | tf_op jit(solution)/shard_map/ppermute | solution.py:245
  64.7 5.8 %project_inputs.1 = (bf16[1024,128]{1,0:T(8,128)(2,1)S(1)}, bf16[1024,128]{1,0:T(8,128)(2,1)S(1)}, bf16[1024,128]{1,0:T(8,128)(2,1)S(1)}, bf16[160,128]{1,0:T(8,128)(2,1)S(1)}) custom-call(f32[1,2048]{1,0:T(1,128)} %bitcast.9, bf16[1024,2048]{1,0:T(8,128)(2,1)} %tokens_hbm.1, bf16[2048,128]{1,0:T(8,128)(2,1)} %query_hbm.1, bf16[64,2048]{1,0:T(8,128)(2,1)} %bitcast.7, ...), custom_call_target="tpu_custom_call" | custom-call | tf_op jit(solution)/shard_map/project_inputs/pallas_call | solution.py:105
  70.5 0.0 copy-start.1
  70.5 0.0 copy-start.3
  70.5 0.0 copy-start.4
  70.5 3.5 %collective-permute-start = (bf16[160,128]{1,0:T(8,128)(2,1)S(1)}, bf16[160,128]{1,0:T(8,128)(2,1)S(1)}, u32[]{:S(2)}, u32[]{:S(2)}) collective-permute-start(bf16[160,128]{1,0:T(8,128)(2,1)S(1)} %get-tuple-element.12), channel_id=1, source_target_pairs={{0,4},{4,8},{8,12},{12,16},{16,20},{20,24},{24,28},{1,5},{5,9},{9,... | collective-permute-start | bytes 122888 | tf_op jit(solution)/shard_map/ppermute | solution.py:25
  74.1 1.7 %collective-permute-done.earlier_ref = bf16[160,128]{1,0:T(8,128)(2,1)S(1)} collective-permute-done((bf16[160,128]{1,0:T(8,128)(2,1)S(1)}, bf16[160,128]{1,0:T(8,128)(2,1)S(1)}, u32[]{:S(2)}, u32[]{:S(2)}) %collective-permute-start) | collective-permute-done | bytes 40992 | tf_op jit(solution)/shard_map/ppermute | solution.py:25
  75.7 3.9 %mix_rows.1 = bf16[4,256,256]{2,1,0:T(8,128)(2,1)S(1)} custom-call(f32[2]{0:T(128)S(1)} %copy-done.5, bf16[1024,128]{1,0:T(8,128)(2,1)S(1)} %get-tuple-element.9.queries_ref, bf16[1024,128]{1,0:T(8,128)(2,1)S(1)} %get-tuple-element.10.pairs_ref, bf16[1024,128]{1,0:T(8,128)(2,1)S(1)} %get-tuple-element.11.gated_ref, ...), custom_call_target="tpu_custom_call" | custom-call | tf_op jit(solution)/shard_map/mix_rows/pallas_call | solution.py:180
  79.7 11.4 %all_to_all.5.exchanged_ref = bf16[4,256,256]{2,1,0:T(8,128)(2,1)S(1)} all-to-all(bf16[4,256,256]{2,1,0:T(8,128)(2,1)S(1)} %mix_rows.1), channel_id=1, replica_groups=mesh['sp'=8,'tp'=4] {'tp'}, dimensions={0} | all-to-all | bytes 1048576 | tf_op jit(solution)/shard_map/all_to_all | solution.py:432
  91.0 0.6 merge_mixers.1.merged_ref
  91.7 0.9 near_product.1.near_ref
  92.6 0.0 collective-permute-done.6.refs_1_
  92.6 1.5 %far_product.1 = bf16[256,2048]{1,0:T(8,128)(2,1)} custom-call(bf16[256,1024]{1,0:T(8,128)(2,1)S(1)} %merge_mixers.1.merged_ref, f32[256,2048]{1,0:T(8,128)S(1)} %near_product.1.near_ref, bf16[128,2048]{1,0:T(8,128)(2,1)S(1)} %collective-permute-done.5.refs_0_, bf16[128,2048]{1,0:T(8,128)(2,1)S(1)} %collective-permute-done.6.refs_1_, ...), custom_call_target="tpu_custom_call" | custom-call | tf_op jit(solution)/shard_map/far_product/pallas_call | solution.py:393
  (15 shorter events, 0.1 us)
Async XLA Ops:
  0.0 27.3 %copy-start = (bf16[128,2048]{1,0:T(8,128)(2,1)S(1)}, bf16[128,2048]{1,0:T(8,128)(2,1)}, u32[]{:S(2)}) copy-start(bf16[128,2048]{1,0:T(8,128)(2,1)} %share_ref.1) | copy-start | bytes 1572868
  0.0 12.1 %collective-permute-start.1 = (bf16[128,2048]{1,0:T(8,128)(2,1)}, bf16[128,2048]{1,0:T(8,128)(2,1)S(1)}, u32[]{:S(2)}, u32[]{:S(2)}) collective-permute-start(bf16[128,2048]{1,0:T(8,128)(2,1)} %share_ref.1), channel_id=1, source_target_pairs={{0,8},{2,10},{4,12},{6,14},{8,16},{9,1},{10,18},{11,3},{12,20},{13... | collective-permute-start | bytes 1572872 | tf_op jit(solution)/shard_map/ppermute | solution.py:245
  12.1 4.1 %collective-permute-start.2 = (bf16[128,2048]{1,0:T(8,128)(2,1)S(1)}, bf16[128,2048]{1,0:T(8,128)(2,1)S(1)}, u32[]{:S(2)}, u32[]{:S(2)}) collective-permute-start(bf16[128,2048]{1,0:T(8,128)(2,1)S(1)} %collective-permute-done.1), channel_id=1, source_target_pairs={{1,5},{3,7},{5,1},{7,3},{8,12},{9,13},{10,14},{11,15},{12,8},{13,9... | collective-permute-start | bytes 1572872 | tf_op jit(solution)/shard_map/ppermute | solution.py:245
  12.8 14.3 %collective-permute-start.3 = (bf16[128,2048]{1,0:T(8,128)(2,1)}, bf16[128,2048]{1,0:T(8,128)(2,1)S(1)}, u32[]{:S(2)}, u32[]{:S(2)}) collective-permute-start(bf16[128,2048]{1,0:T(8,128)(2,1)} %share_ref.1), channel_id=1, source_target_pairs={{0,4},{2,6},{4,0},{6,2},{8,12},{10,14},{12,8},{14,10},{16,20},{18,... | collective-permute-start | bytes 1572872 | tf_op jit(solution)/shard_map/ppermute | solution.py:245
  27.2 64.5 %collective-permute-start.4 = (bf16[384,2048]{1,0:T(8,128)(2,1)S(1)}, bf16[384,2048]{1,0:T(8,128)(2,1)S(1)}, u32[]{:S(2)}, u32[]{:S(2)}) collective-permute-start(bf16[384,2048]{1,0:T(8,128)(2,1)S(1)} %constant_dynamic-update-slice_fusion.here_ref), channel_id=1, source_target_pairs={{0,1},{1,0},{2,3},{3,2},{4,5},{5,4},{6,7},{7,6},{8,9},{9,8},{10,11... | collective-permute-start | bytes 4718600 | tf_op jit(solution)/shard_map/ppermute | solution.py:245
  27.3 26.3 %collective-permute-start.5 = (bf16[128,2048]{1,0:T(8,128)(2,1)S(1)}, bf16[128,2048]{1,0:T(8,128)(2,1)S(1)}, u32[]{:S(2)}, u32[]{:S(2)}) collective-permute-start(bf16[128,2048]{1,0:T(8,128)(2,1)S(1)} %copy-done), channel_id=1, source_target_pairs={{0,16},{1,24},{2,22},{3,30},{4,20},{5,28},{6,18},{7,26},{8,25},{10... | collective-permute-start | bytes 1572872 | tf_op jit(solution)/shard_map/ppermute | solution.py:245
  53.6 11.1 %collective-permute-start.7 = (bf16[128,2048]{1,0:T(8,128)(2,1)S(1)}, bf16[128,2048]{1,0:T(8,128)(2,1)S(1)}, u32[]{:S(2)}, u32[]{:S(2)}) collective-permute-start(bf16[128,2048]{1,0:T(8,128)(2,1)S(1)} %collective-permute-done.5.refs_0_), channel_id=1, source_target_pairs={{0,4},{1,3},{2,6},{3,1},{4,0},{5,7},{6,2},{7,5},{8,12},{10,14},{12... | collective-permute-start | bytes 1572872 | tf_op jit(solution)/shard_map/ppermute | solution.py:245
  57.0 35.6 %collective-permute-start.6 = (bf16[128,2048]{1,0:T(8,128)(2,1)S(1)}, bf16[128,2048]{1,0:T(8,128)(2,1)S(1)}, u32[]{:S(2)}, u32[]{:S(2)}) collective-permute-start(bf16[128,2048]{1,0:T(8,128)(2,1)S(1)} %collective-permute-done.5.refs_0_), channel_id=1, source_target_pairs={{0,1},{1,0},{2,3},{3,2},{4,5},{5,4},{6,7},{7,6},{8,9},{9,8},{10,11... | collective-permute-start | bytes 1572872 | tf_op jit(solution)/shard_map/ppermute | solution.py:245
  64.7 28.0 %collective-permute-start.8 = (bf16[128,2048]{1,0:T(8,128)(2,1)S(1)}, bf16[128,2048]{1,0:T(8,128)(2,1)S(1)}, u32[]{:S(2)}, u32[]{:S(2)}) collective-permute-start(bf16[128,2048]{1,0:T(8,128)(2,1)S(1)} %collective-permute-done.7.refs_2_), channel_id=1, source_target_pairs={{0,1},{1,0},{2,3},{3,2},{4,5},{5,4},{6,7},{7,6},{8,9},{9,8},{10,11... | collective-permute-start | bytes 1572872 | tf_op jit(solution)/shard_map/ppermute | solution.py:245
  64.7 11.1 %copy-start.2 = (bf16[31,512]{1,0:T(8,128)(2,1)S(1)}, bf16[31,512]{1,0:T(8,128)(2,1)}, u32[]{:S(2)}) copy-start(bf16[31,512]{1,0:T(8,128)(2,1)} %taps_ref.1) | copy-start | bytes 95236
  64.7 11.1 %copy-start.5 = (f32[2]{0:T(128)S(1)}, f32[2]{0:T(128)}, u32[]{:S(2)}) copy-start(f32[2]{0:T(128)} %sinks_ref.1) | copy-start | bytes 28
  70.5 20.5 %copy-start.1 = (bf16[512,512]{1,0:T(8,128)(2,1)S(1)}, bf16[512,512]{1,0:T(8,128)(2,1)}, u32[]{:S(2)}) copy-start(bf16[512,512]{1,0:T(8,128)(2,1)} %point_ref.1) | copy-start | bytes 1572868
  70.5 20.5 %copy-start.3 = (f32[1024]{0:T(1024)S(1)}, f32[1024]{0:T(1024)}, u32[]{:S(2)}) copy-start(f32[1024]{0:T(1024)} %param.24) | copy-start | bytes 12292
  70.5 20.5 %copy-start.4 = (f32[512]{0:T(512)S(1)}, f32[512]{0:T(512)}, u32[]{:S(2)}) copy-start(f32[512]{0:T(512)} %param.22) | copy-start | bytes 6148
  70.5 5.2 %collective-permute-start = (bf16[160,128]{1,0:T(8,128)(2,1)S(1)}, bf16[160,128]{1,0:T(8,128)(2,1)S(1)}, u32[]{:S(2)}, u32[]{:S(2)}) collective-permute-start(bf16[160,128]{1,0:T(8,128)(2,1)S(1)} %get-tuple-element.12), channel_id=1, source_target_pairs={{0,4},{4,8},{8,12},{12,16},{16,20},{20,24},{24,28},{1,5},{5,9},{9,... | collective-permute-start | bytes 122888 | tf_op jit(solution)/shard_map/ppermute | solution.py:25

commit v2 on v1

--- a/solution.py
+++ b/solution.py
@@ -25,121 +25,154 @@
     return lax.ppermute(block, axis, route)
 
 
-def project_inputs(tokens, norm_gain, query_weight, key_weight, value_weight, in_weight, gate_weight):
+BLOCK = 256
+
+
+def normed_rows(token_rows, gain):
+    widened = token_rows.astype(jnp.float32)
+    scale = lax.rsqrt(jnp.mean(widened * widened, axis=-1, keepdims=True) + NORM_EPSILON)
+    return (widened * scale * gain).astype(jnp.bfloat16)
+
+
+def split_product(normed, joined, heads_width, pair_width, channels):
+    result = jnp.dot(normed, joined, preferred_element_type=jnp.float32)
+    pairs_end = heads_width + pair_width
+    conv_in = result[:, pairs_end : pairs_end + channels]
+    gated = conv_in * jax.nn.sigmoid(result[:, pairs_end + channels :])
+    return [
+        part.astype(jnp.bfloat16)
+        for part in (result[:, :heads_width], result[:, heads_width:pairs_end], gated)
+    ]
+
+
+def project_last(tokens, norm_gain, query_weight, key_weight, value_weight, in_weight, gate_weight):
     rows, width = tokens.shape
-    heads_width, pair_width = query_weight.shape[1], key_weight.shape[1] + value_weight.shape[1]
-    key_width, channels = key_weight.shape[1], in_weight.shape[1]
-    block = 256
-    blocks = rows // block
+    heads_width, key_width, channels = query_weight.shape[1], key_weight.shape[1], in_weight.shape[1]
+    pair_width = key_width + value_weight.shape[1]
     tail = WINDOW + HALO
+    others = rows - BLOCK
     starts = [0, heads_width + pair_width, heads_width + pair_width + channels]
 
     def body(
         gain_hbm, tokens_hbm, query_hbm, key_hbm, value_hbm, in_hbm, gate_hbm,
-        queries_ref, pairs_ref, gated_ref, tail_ref,
-        fetched, normed, joined, pairs_rows, gain_ref, arrived, fetched_sem,
+        queries_ref, pairs_ref, gated_ref, tail_ref, joined, rest_ref,
+        last_ref, pairs_rows, gain_ref, arrived,
     ):
-        fetches = [
-            pltpu.make_async_copy(
-                tokens_hbm.at[pl.ds(i * block, block)], fetched.at[i], fetched_sem.at[i]
+        copies = [
+            pltpu.make_async_copy(source, target, arrived.at[i])
+            for i, (source, target) in enumerate(
+                [
+                    (gain_hbm, gain_ref),
+                    (tokens_hbm.at[pl.ds(others, BLOCK)], last_ref),
+                    (key_hbm, pairs_rows.at[pl.ds(0, key_width)]),
+                    (value_hbm, pairs_rows.at[pl.ds(key_width, pair_width - key_width)]),
+                ]
+                + [
+                    (source, joined.at[:, pl.ds(start, source.shape[1])])
+                    for source, start in zip([query_hbm, in_hbm, gate_hbm], starts)
+                ]
+                + [(tokens_hbm.at[pl.ds(0, others)], rest_ref)]
             )
-            for i in range(blocks)
         ]
-        copies = [
-            pltpu.make_async_copy(key_hbm, pairs_rows.at[pl.ds(0, key_width)], arrived.at[3]),
-            pltpu.make_async_copy(
-                value_hbm, pairs_rows.at[pl.ds(key_width, pair_width - key_width)], arrived.at[4]
-            ),
-        ] + [
-            pltpu.make_async_copy(
-                source, joined.at[:, pl.ds(start, source.shape[1])], arrived.at[i]
-            )
-            for i, (source, start) in enumerate(zip([query_hbm, in_hbm, gate_hbm], starts))
-        ]
-        gain_copy = pltpu.make_async_copy(gain_hbm, gain_ref, arrived.at[5])
-        gain_copy.start()
-        fetches[0].start()
         for copy in copies:
             copy.start()
-        for fetch in fetches[1:]:
-            fetch.start()
-
-        def norm(i):
-            widened = fetched[i].astype(jnp.float32)
-            scale = lax.rsqrt(jnp.mean(widened * widened, axis=-1, keepdims=True) + NORM_EPSILON)
-            normed[i] = (widened * scale * gain_ref[...]).astype(jnp.bfloat16)
-
-        gain_copy.wait()
-        fetches[0].wait()
-        norm(0)
         for copy in copies[:2]:
             copy.wait()
+        normed = normed_rows(last_ref[...], gain_ref[...])
+        for copy in copies[2:4]:
+            copy.wait()
         joined[:, heads_width : heads_width + pair_width] = pairs_rows[...].T
-        for copy in copies[2:]:
+        for copy in copies[4:7]:
             copy.wait()
-        for i in range(blocks):
-            if i + 1 < blocks:
-                fetches[i + 1].wait()
-            here = pl.ds(i * block, block)
-            result = jnp.dot(normed[i], joined[...], preferred_element_type=jnp.float32)
-            if i + 1 < blocks:
-                norm(i + 1)
-            queries_ref[here] = result[:, :heads_width].astype(jnp.bfloat16)
-            pairs = result[:, heads_width : heads_width + pair_width].astype(jnp.bfloat16)
-            pairs_ref[here] = pairs
-            conv_in = result[:, starts[1] : starts[2]]
-            conv_gate = result[:, starts[2] :]
-            gated = (conv_in * jax.nn.sigmoid(conv_gate)).astype(jnp.bfloat16)
-            gated_ref[here] = gated
-            if i + 1 == blocks:
-                tail_ref[:WINDOW] = pairs[block - WINDOW :]
-                tail_ref[WINDOW:] = gated[block - HALO :]
+        queries, pairs, gated = split_product(
+            normed, joined[...], heads_width, pair_width, channels
+        )
+        queries_ref[...] = queries
+        pairs_ref[...] = pairs
+        gated_ref[...] = gated
+        tail_ref[:WINDOW] = pairs[BLOCK - WINDOW :]
+        tail_ref[WINDOW:] = gated[BLOCK - HALO :]
+        copies[7].wait()
 
     vmem = pl.BlockSpec(memory_space=pltpu.VMEM)
     in_hbm = [
         pltpu.with_memory_space_constraint(operand, pltpu.HBM)
         for operand in (
-            norm_gain[None], tokens, query_weight, key_weight.T, value_weight.T, in_weight, gate_weight
+            norm_gain[None], tokens, query_weight, key_weight.T, value_weight.T, in_weight,
+            gate_weight,
         )
+    ]
+    shapes = [
+        (BLOCK, heads_width), (BLOCK, pair_width), (BLOCK, channels), (tail, channels),
+        (width, heads_width + pair_width + 2 * channels), (others, width),
     ]
     return pl.pallas_call(
         body,
         in_specs=[pl.BlockSpec(memory_space=pl.ANY)] * 7,
-        out_specs=[vmem] * 4,
-        out_shape=[
-            jax.ShapeDtypeStruct((rows, heads_width), jnp.bfloat16),
-            jax.ShapeDtypeStruct((rows, pair_width), jnp.bfloat16),
-            jax.ShapeDtypeStruct((rows, channels), jnp.bfloat16),
-            jax.ShapeDtypeStruct((tail, channels), jnp.bfloat16),
-        ],
+        out_specs=[vmem] * len(shapes),
+        out_shape=[jax.ShapeDtypeStruct(shape, jnp.bfloat16) for shape in shapes],
         scratch_shapes=[
-            pltpu.VMEM((blocks, block, width), jnp.bfloat16),
-            pltpu.VMEM((blocks, block, width), jnp.bfloat16),
-            pltpu.VMEM((width, heads_width + pair_width + 2 * channels), jnp.bfloat16),
+            pltpu.VMEM((BLOCK, width), jnp.bfloat16),
             pltpu.VMEM((pair_width, width), jnp.bfloat16),
             pltpu.VMEM((1, width), jnp.float32),
-            pltpu.SemaphoreType.DMA((6,)),
-            pltpu.SemaphoreType.DMA((blocks,)),
+            pltpu.SemaphoreType.DMA((8,)),
         ],
+        compiler_params=pltpu.CompilerParams(vmem_limit_bytes=20 << 20),
+        name="project_last",
+    )(*in_hbm)
+
+
+def project_rest(tokens, norm_gain, joined, heads_width, pair_width):
+    rows, width = tokens.shape
+    channels = (joined.shape[1] - heads_width - pair_width) // 2
+    blocks = rows // BLOCK
+
+    def body(gain_ref, tokens_ref, joined_ref, queries_ref, pairs_ref, gated_ref, normed):
+        normed[0] = normed_rows(tokens_ref[:BLOCK], gain_ref[...])
+        for i in range(blocks):
+            here = slice(i * BLOCK, (i + 1) * BLOCK)
+            queries, pairs, gated = split_product(
+                normed[i], joined_ref[...], heads_width, pair_width, channels
+            )
+            if i + 1 < blocks:
+                following = tokens_ref[(i + 1) * BLOCK : (i + 2) * BLOCK]
+                normed[i + 1] = normed_rows(following, gain_ref[...])
+            queries_ref[here] = queries
+            pairs_ref[here] = pairs
+            gated_ref[here] = gated
+
+    vmem = pl.BlockSpec(memory_space=pltpu.VMEM)
+    return pl.pallas_call(
+        body,
+        in_specs=[vmem] * 3,
+        out_specs=[vmem] * 3,
+        out_shape=[
+            jax.ShapeDtypeStruct((rows, columns), jnp.bfloat16)
+            for columns in (heads_width, pair_width, channels)
+        ],
+        scratch_shapes=[pltpu.VMEM((blocks, BLOCK, width), jnp.bfloat16)],
         compiler_params=pltpu.CompilerParams(vmem_limit_bytes=24 << 20),
-        name="project_inputs",
-    )(*in_hbm)
-
-
-def mix_rows(queries, pairs, gated, earlier, sinks, taps, shares):
-    rows, heads_width = queries.shape
-    channels = gated.shape[1]
+        name="project_rest",
+    )(norm_gain[None], tokens, joined)
+
+
+def mix_rows(first_rows, last_rows, earlier, sinks, taps, shares):
+    rest, heads_width = first_rows[0].shape
+    rows = rest + last_rows[0].shape[0]
+    pair_width, channels = first_rows[1].shape[1], first_rows[2].shape[1]
     head_count = heads_width // HEAD_DIM
     share_rows = rows // shares
 
     def body(
-        sinks_ref, queries_ref, pairs_ref, gated_ref, earlier_ref, taps_ref,
-        out_ref, band, extended,
+        sinks_ref, queries_ref, pairs_ref, gated_ref, last_queries, last_pairs, last_gated,
+        earlier_ref, taps_ref, out_ref, band, extended,
     ):
         band[:WINDOW] = earlier_ref[:WINDOW]
-        band[WINDOW:] = pairs_ref[...]
+        band[WINDOW : WINDOW + rest] = pairs_ref[...]
+        band[WINDOW + rest :] = last_pairs[...]
         extended[:HALO] = earlier_ref[WINDOW:].astype(jnp.float32)
-        extended[HALO:] = gated_ref[...].astype(jnp.float32)
+        extended[HALO : HALO + rest] = gated_ref[...].astype(jnp.float32)
+        extended[HALO + rest :] = last_gated[...].astype(jnp.float32)
         query_index = lax.broadcasted_iota(jnp.int32, (WINDOW, 2 * WINDOW), 0)
         key_index = lax.broadcasted_iota(jnp.int32, (WINDOW, 2 * WINDOW), 1)
         distance = WINDOW + query_index - key_index
@@ -155,7 +188,8 @@
             allowed = not_before if block == 0 else in_window
             found = []
             for head in range(head_count):
-                here = queries_ref[start : start + WINDOW, head * HEAD_DIM : (head + 1) * HEAD_DIM]
+                source, at = (queries_ref, start) if start < rest else (last_queries, start - rest)
+                here = source[at : at + WINDOW, head * HEAD_DIM : (head + 1) * HEAD_DIM]
                 scores = lax.dot_general(
                     here, keys, (((1,), (1,)), ((), ())), preferred_element_type=jnp.float32
                 ) * HEAD_DIM ** (-0.5)
@@ -179,16 +213,16 @@
     scalars = pl.BlockSpec(memory_space=pltpu.SMEM)
     return pl.pallas_call(
         body,
-        in_specs=[scalars] + [whole] * 5,
+        in_specs=[scalars] + [whole] * 8,
         out_specs=whole,
         out_shape=jax.ShapeDtypeStruct((shares, share_rows, heads_width + channels), jnp.bfloat16),
         scratch_shapes=[
-            pltpu.VMEM((WINDOW + rows, pairs.shape[1]), jnp.bfloat16),
+            pltpu.VMEM((WINDOW + rows, pair_width), jnp.bfloat16),
             pltpu.VMEM((HALO + rows, channels), jnp.float32),
         ],
         compiler_params=pltpu.CompilerParams(vmem_limit_bytes=12 << 20),
         name="mix_rows",
-    )(sinks, queries, pairs, gated, earlier, taps)
+    )(sinks, *first_rows, *last_rows, earlier, taps)
 
 
 def merge_mixers(exchanged, conv_gain, point_weight, output_gain):
@@ -230,56 +264,52 @@
     )(exchanged, conv_gain[None], point_weight, output_gain[None])
 
 
-def gather_shares(share, lines, tp_size):
-    def number(line, side, lane):
-        return (line * 2 + side) * tp_size + lane
-
-    def send(block, target):
+class ShareRoutes:
+    def __init__(self, lines, tp_size):
+        self.lines, self.tp_size = lines, tp_size
+
+    def number(self, line, side, lane):
+        return (line * 2 + side) * self.tp_size + lane
+
+    def send(self, block, target):
         found = []
-        for line in range(lines):
+        for line in range(self.lines):
             for side in range(2):
-                for lane in range(tp_size):
-                    to_line, to_side, to_lane = target(line, side, lane)
-                    if 0 <= to_line < lines:
-                        found.append((number(line, side, lane), number(to_line, to_side, to_lane)))
+                for lane in range(self.tp_size):
+                    to = target(line, side, lane)
+                    if 0 <= to[0] < self.lines:
+                        found.append((self.number(line, side, lane), self.number(*to)))
         return lax.ppermute(block, PLACE, found)
 
-    def beside(line, side, lane):
+    def beside(self, line, side, lane):
         return (line + 1 if lane % 2 == 0 else line - 1), side, lane
 
-    def beyond(line, side, lane):
-        targets = far_lines(line, lines)
+    def beyond(self, line, side, lane):
+        targets = far_lines(line, self.lines)
         if lane % 2 >= len(targets):
             return -1, side, lane
         to_line = targets[lane % 2]
         to_side = 1 - side if lane // 2 % 2 else side
-        return to_line, to_side, lane - lane % 2 + far_lines(to_line, lines).index(line)
-
-    def lower_lane_across(line, side, lane):
+        to_lane = lane - lane % 2 + far_lines(to_line, self.lines).index(line)
+        return to_line, to_side, to_lane
+
+    def holders_across(self, line, side, lane):
+        from_line = line - 1 if lane % 2 == 0 else line + 1
+        return (line if 0 <= from_line < self.lines else -1), 1 - side, lane
+
+    def lower_lane_across(self, line, side, lane):
         return (line if lane % 2 == 0 else -1), 1 - side, lane
 
-    def holders_across(line, side, lane):
-        from_line = line - 1 if lane % 2 == 0 else line + 1
-        return (line if 0 <= from_line < lines else -1), 1 - side, lane
-
-    def holders_to_neighbours(line, side, lane):
-        held = lane % 2 < len(far_lines(line, lines))
+    def upper_lane_from_lower(self, line, side, lane):
+        return (line if lane % 2 == 0 else -1), side, lane ^ 1
+
+    def to_neighbours(self, line, side, lane):
+        held = lane % 2 < len(far_lines(line, self.lines))
         to = (1 - side, lane) if lane % 2 == 0 else (side, lane ^ 2)
         return (line if held else -1), *to
 
-    def lanes(line, side, lane):
+    def lanes(self, line, side, lane):
         return line, side, lane ^ 1
-
-    near = send(share, beside)
-    opposite = send(share, lower_lane_across)
-    near_across = send(near, holders_across)
-    far = send(share, beyond)
-    far_other = send(far, holders_to_neighbours)
-    near_here = jnp.concatenate([near, near_across, opposite], axis=0)
-    near_there = send(near_here, lanes)
-    far_there = send(far, lanes)
-    far_other_there = send(far_other, lanes)
-    return near_here, near_there, (far, far_there, far_other, far_other_there)
 
 
 def far_lines(line, lines):
@@ -299,43 +329,44 @@
     return jnp.concatenate(found, axis=1)
 
 
-def near_product(merged, share, near_here, near_there, lines):
+def near_product(merged, share, near_pieces, opposite_pieces, lines):
     rows, _ = merged.shape
     share_rows, columns = share.shape
 
-    def body(merged_ref, share_ref, here_ref, there_ref, out_ref):
+    def body(merged_ref, share_ref, *refs):
+        near_refs, opposite_refs, out_ref = refs[:4], refs[4:6], refs[6]
         line, side, lane = place_of_device()
 
-        def product(from_line, left):
+        def product(from_line, *parts):
             return jnp.dot(
                 columns_of(merged_ref, from_line, (side, 1 - side), share_rows),
-                left,
+                jnp.concatenate(parts, axis=0),
                 preferred_element_type=jnp.float32,
             )
 
-        for ref, holds in ((here_ref, lane == 0), (there_ref, lane == 1)):
-
-            @pl.when(holds)
+        for which in range(2):
+
+            @pl.when(lane == which)
             def _():
-                pair = jnp.concatenate([share_ref[...], ref[2 * share_rows :]], axis=0)
-                out_ref[...] = product(line, pair)
-
-        for ref, at_lane in ((here_ref, lane), (there_ref, 1 - lane)):
+                out_ref[...] = product(line, share_ref[...], opposite_refs[which][...])
+
+        for which in range(2):
+            at_lane = (lane, 1 - lane)[which]
             from_line = line - 1 + 2 * at_lane
 
             @pl.when((from_line >= 0) & (from_line < lines))
             def _():
-                out_ref[...] += product(from_line, ref[: 2 * share_rows])
+                out_ref[...] += product(from_line, near_refs[which][...], near_refs[2 + which][...])
 
     vmem = pl.BlockSpec(memory_space=pltpu.VMEM)
     return pl.pallas_call(
         body,
-        in_specs=[vmem] * 4,
+        in_specs=[vmem] * 8,
         out_specs=vmem,
         out_shape=jax.ShapeDtypeStruct((rows, columns), jnp.float32),
         compiler_params=pltpu.CompilerParams(vmem_limit_bytes=16 << 20),
         name="near_product",
-    )(merged, share, near_here, near_there)
+    )(merged, share, *near_pieces, *opposite_pieces)
 
 
 def far_product(merged, near_sum, far_pieces, lines):
@@ -423,16 +454,28 @@
     lines = sp_size // 2
     by_shares = sends_shares(sp_size, tp_size)
     if by_shares:
-        near_here, near_there, far_pieces = gather_shares(output_weight, lines, tp_size)
-    queries, pairs, gated, tail = project_inputs(
+        routes = ShareRoutes(lines, tp_size)
+        near = routes.send(output_weight, routes.beside)
+        far = routes.send(output_weight, routes.beyond)
+    *last_rows, tail, joined, other_tokens = project_last(
         tokens, norm_gain, query_weight, key_weight, value_weight, conv_in_weight, conv_gate_weight
     )
     earlier = from_behind(tail, "sp", 1)
-    mixed = mix_rows(queries, pairs, gated, earlier, sink_logits, conv_taps, tp_size)
+    pair_width = key_weight.shape[1] + value_weight.shape[1]
+    first_rows = project_rest(other_tokens, norm_gain, joined, query_weight.shape[1], pair_width)
+    mixed = mix_rows(first_rows, last_rows, earlier, sink_logits, conv_taps, tp_size)
     exchanged = lax.all_to_all(mixed, "tp", split_axis=0, concat_axis=0, tiled=True)
     merged = merge_mixers(exchanged, conv_gain, point_weight, output_gain)
     if by_shares:
-        near_sum = near_product(merged, output_weight, near_here, near_there, lines)
+        opposite = routes.send(output_weight, routes.lower_lane_across)
+        near_across = routes.send(near, routes.holders_across)
+        far_other = routes.send(far, routes.to_neighbours)
+        near_pieces = near, routes.send(near, routes.lanes)
+        near_pieces += near_across, routes.send(near_across, routes.lanes)
+        opposite_pieces = opposite, routes.send(opposite, routes.upper_lane_from_lower)
+        far_pieces = far, routes.send(far, routes.lanes)
+        far_pieces += far_other, routes.send(far_other, routes.lanes)
+        near_sum = near_product(merged, output_weight, near_pieces, opposite_pieces, lines)
         return far_product(merged, near_sum, far_pieces, lines)
     projected = jnp.dot(
         merged,

time: 94.5 us -> 65.4 us (0.69)
  the two profiles are of different devices: /device:TPU:0 before, /device:TPU:18 now
where the time goes in v2:
time: 65.4 us; the launch traced here: 65.1 us
  starting transfers between devices  23.3 us (36%)
  waiting for transfers between devices  17.6 us (27%)
  Pallas kernels  12.4 us (19%)
  blocking collectives  11.4 us (17%)
    ppermute x10, starting transfers between devices, send(): return lax.ppermute(block, PLACE, found)  21.4 us
    ppermute x10, waiting for transfers between devices, send(): return lax.ppermute(block, PLACE, found)  14.4 us
    all_to_all x1, blocking collectives, on_device(): lax.all_to_all(mixed, 'tp', split_axis=0, concat_axis=0, tiled=True)  11.4 us
    pallas_call x1, Pallas kernels, mix_rows(): pl.pallas_call(body, in_specs=[scalars] + [whole] * 8, out_specs=whole, o...  3.94 us
    ppermute x1, waiting for transfers between devices, from_behind(): return lax.ppermute(block, axis, route)  3.17 us
    pallas_call x1, Pallas kernels, project_last(): pl.pallas_call(body, in_specs=[pl.BlockSpec(memory_space=pl.ANY)] * 7, ou...  2.94 us
    pallas_call x1, Pallas kernels, project_rest(): pl.pallas_call(body, in_specs=[vmem] * 3, out_specs=[vmem] * 3, out_shape...  2.29 us
    ppermute x1, starting transfers between devices, from_behind(): return lax.ppermute(block, axis, route)  1.92 us
  transfers between devices with their start and end apart: 11, of which 3 were waited for; matrix products, arithmetic and copies ran while one was open for 0% of the time, Pallas kernels for 17%

profile of v2, /device:TPU:18, one launch (start us, length us, event | category | flops | bytes accessed | tf_op | source)
XLA Modules:
  0.0 65.1 jit_solution(8573055596376104505)
XLA Ops:
  0.0 3.5 %collective-permute-start.1 = (bf16[128,2048]{1,0:T(8,128)(2,1)}, bf16[128,2048]{1,0:T(8,128)(2,1)S(1)}, u32[]{:S(2)}, u32[]{:S(2)}) collective-permute-start(bf16[128,2048]{1,0:T(8,128)(2,1)} %share_ref.1), channel_id=1, source_target_pairs={{0,8},{2,10},{4,12},{6,14},{8,16},{9,1},{10,18},{11,3},{12,20},{13... | collective-permute-start | bytes 1572872 | tf_op jit(solution)/shard_map/ppermute | solution.py:282
  3.5 2.3 %collective-permute-start.7 = (bf16[128,2048]{1,0:T(8,128)(2,1)}, bf16[128,2048]{1,0:T(8,128)(2,1)S(1)}, u32[]{:S(2)}, u32[]{:S(2)}) collective-permute-start(bf16[128,2048]{1,0:T(8,128)(2,1)} %share_ref.1), channel_id=1, source_target_pairs={{0,16},{1,24},{2,22},{3,30},{4,20},{5,28},{6,18},{7,26},{8,25},{10... | collective-permute-start | bytes 1572872 | tf_op jit(solution)/shard_map/ppermute | solution.py:282
  5.8 2.4 %collective-permute-start.5 = (bf16[128,2048]{1,0:T(8,128)(2,1)}, bf16[128,2048]{1,0:T(8,128)(2,1)S(1)}, u32[]{:S(2)}, u32[]{:S(2)}) collective-permute-start(bf16[128,2048]{1,0:T(8,128)(2,1)} %share_ref.1), channel_id=1, source_target_pairs={{0,4},{2,6},{4,0},{6,2},{8,12},{10,14},{12,8},{14,10},{16,20},{18,... | collective-permute-start | bytes 1572872 | tf_op jit(solution)/shard_map/ppermute | solution.py:282
  8.2 14.3 %collective-permute-done.1.refs_0_ = bf16[128,2048]{1,0:T(8,128)(2,1)S(1)} collective-permute-done((bf16[128,2048]{1,0:T(8,128)(2,1)}, bf16[128,2048]{1,0:T(8,128)(2,1)S(1)}, u32[]{:S(2)}, u32[]{:S(2)}) %collective-permute-start.1) | collective-permute-done | bytes 524320 | tf_op jit(solution)/shard_map/ppermute | solution.py:282
  22.5 2.4 %collective-permute-start.3 = (bf16[128,2048]{1,0:T(8,128)(2,1)S(1)}, bf16[128,2048]{1,0:T(8,128)(2,1)S(1)}, u32[]{:S(2)}, u32[]{:S(2)}) collective-permute-start(bf16[128,2048]{1,0:T(8,128)(2,1)S(1)} %collective-permute-done.1.refs_0_), channel_id=1, source_target_pairs={{1,5},{3,7},{5,1},{7,3},{8,12},{9,13},{10,14},{11,15},{12,8},{13,9... | collective-permute-start | bytes 1572872 | tf_op jit(solution)/shard_map/ppermute | solution.py:282
  25.0 0.1 collective-permute-done.7.refs_0_
  25.1 3.3 %collective-permute-start.9 = (bf16[128,2048]{1,0:T(8,128)(2,1)S(1)}, bf16[128,2048]{1,0:T(8,128)(2,1)S(1)}, u32[]{:S(2)}, u32[]{:S(2)}) collective-permute-start(bf16[128,2048]{1,0:T(8,128)(2,1)S(1)} %collective-permute-done.7.refs_0_), channel_id=1, source_target_pairs={{0,4},{1,3},{2,6},{3,1},{4,0},{5,7},{6,2},{7,5},{8,12},{10,14},{12... | collective-permute-start | bytes 1572872 | tf_op jit(solution)/shard_map/ppermute | solution.py:282
  28.4 2.9 %project_last.1 = (bf16[256,128]{1,0:T(8,128)(2,1)S(1)}, bf16[256,128]{1,0:T(8,128)(2,1)S(1)}, bf16[256,128]{1,0:T(8,128)(2,1)S(1)}, bf16[160,128]{1,0:T(8,128)(...) custom-call(f32[1,2048]{1,0:T(1,128)} %bitcast.5, bf16[1024,2048]{1,0:T(8,128)(2,1)} %tokens_hbm.1, ...), custom_call_target="tpu_custom_call" | custom-call | tf_op jit(solution)/shard_map/project_last/pallas_call | solution.py:109
  31.3 0.0 copy-start.3
  31.3 0.0 copy-start.6
  31.4 1.9 %collective-permute-start = (bf16[160,128]{1,0:T(8,128)(2,1)S(1)}, bf16[160,128]{1,0:T(8,128)(2,1)S(1)}, u32[]{:S(2)}, u32[]{:S(2)}) collective-permute-start(bf16[160,128]{1,0:T(8,128)(2,1)S(1)} %get-tuple-element.22), channel_id=1, source_target_pairs={{0,4},{4,8},{8,12},{12,16},{16,20},{20,24},{24,28},{1,5},{5,9},{9,... | collective-permute-start | bytes 122888 | tf_op jit(solution)/shard_map/ppermute | solution.py:25
  33.3 5.0 %collective-permute-start.2 = (bf16[128,2048]{1,0:T(8,128)(2,1)S(1)}, bf16[128,2048]{1,0:T(8,128)(2,1)S(1)}, u32[]{:S(2)}, u32[]{:S(2)}) collective-permute-start(bf16[128,2048]{1,0:T(8,128)(2,1)S(1)} %collective-permute-done.1.refs_0_), channel_id=1, source_target_pairs={{0,1},{1,0},{2,3},{3,2},{4,5},{5,4},{6,7},{7,6},{8,9},{9,8},{10,11... | collective-permute-start | bytes 1572872 | tf_op jit(solution)/shard_map/ppermute | solution.py:282
  38.2 2.0 %collective-permute-start.6 = (bf16[128,2048]{1,0:T(8,128)(2,1)S(1)}, bf16[128,2048]{1,0:T(8,128)(2,1)S(1)}, u32[]{:S(2)}, u32[]{:S(2)}) collective-permute-start(bf16[128,2048]{1,0:T(8,128)(2,1)S(1)} %collective-permute-done.5.refs_4_), channel_id=1, source_target_pairs={{0,1},{2,3},{4,5},{6,7},{8,9},{10,11},{12,13},{14,15},{16,17},{18,... | collective-permute-start | bytes 1572872 | tf_op jit(solution)/shard_map/ppermute | solution.py:282
  40.2 0.1 collective-permute-start.4
  40.3 3.2 %collective-permute-done.earlier_ref = bf16[160,128]{1,0:T(8,128)(2,1)S(1)} collective-permute-done((bf16[160,128]{1,0:T(8,128)(2,1)S(1)}, bf16[160,128]{1,0:T(8,128)(2,1)S(1)}, u32[]{:S(2)}, u32[]{:S(2)}) %collective-permute-start) | collective-permute-done | bytes 40992 | tf_op jit(solution)/shard_map/ppermute | solution.py:25
  43.5 0.5 collective-permute-start.10
  44.0 2.3 %project_rest.1 = (bf16[768,128]{1,0:T(8,128)(2,1)S(1)}, bf16[768,128]{1,0:T(8,128)(2,1)S(1)}, bf16[768,128]{1,0:T(8,128)(2,1)S(1)}) custom-call(f32[1,2048]{1,0:T(1,128)S(1)} %bitcast.6, bf16[768,2048]{1,0:T(8,128)(2,1)S(1)} %get-tuple-element.14.tokens_ref, bf16[2048,512]{1,0:T(8,128)(2,1)S(1)} %get-tuple-element.15.joined_ref), custom_call_target="tpu_custom_call" | custom-call | tf_op jit(solution)/shard_map/project_rest/pallas_call | solution.py:145
  46.3 0.0 copy-start
  46.3 3.9 %mix_rows.1 = bf16[4,256,256]{2,1,0:T(8,128)(2,1)S(1)} custom-call(f32[2]{0:T(128)S(1)} %copy-done.6, bf16[768,128]{1,0:T(8,128)(2,1)S(1)} %get-tuple-element.16.queries_ref, bf16[768,128]{1,0:T(8,128)(2,1)S(1)} %get-tuple-element.17.pairs_ref, bf16[768,128]{1,0:T(8,128)(2,1)S(1)} %get-tuple-element.18.gated_ref, ...), custom_call_target="tpu_custom_call" | custom-call | tf_op jit(solution)/shard_map/mix_rows/pallas_call | solution.py:214
  50.3 11.4 %all_to_all.5.exchanged_ref = bf16[4,256,256]{2,1,0:T(8,128)(2,1)S(1)} all-to-all(bf16[4,256,256]{2,1,0:T(8,128)(2,1)S(1)} %mix_rows.1), channel_id=1, replica_groups=mesh['sp'=8,'tp'=4] {'tp'}, dimensions={0} | all-to-all | bytes 1048576 | tf_op jit(solution)/shard_map/all_to_all | solution.py:467
  61.7 0.6 merge_mixers.1.merged_ref
  62.3 0.0 collective-permute-done.2.refs_1_
  62.4 1.4 %near_product.1.near_ref = f32[256,2048]{1,0:T(8,128)S(1)} custom-call(bf16[256,1024]{1,0:T(8,128)(2,1)S(1)} %merge_mixers.1.merged_ref, bf16[128,2048]{1,0:T(8,128)(2,1)S(1)} %copy-done, bf16[128,2048]{1,0:T(8,128)(2,1)S(1)} %collective-permute-done.1.refs_0_, bf16[128,2048]{1,0:T(8,128)(2,1)S(1)} %collective-permute-done.2.refs_1_, ...), custom_call_target="tpu_custom_call" | custom-call | tf_op jit(solution)/shard_map/near_product/pallas_call | solution.py:362
  63.8 1.3 %far_product.1 = bf16[256,2048]{1,0:T(8,128)(2,1)} custom-call(bf16[256,1024]{1,0:T(8,128)(2,1)S(1)} %merge_mixers.1.merged_ref, f32[256,2048]{1,0:T(8,128)S(1)} %near_product.1.near_ref, bf16[128,2048]{1,0:T(8,128)(2,1)S(1)} %collective-permute-done.7.refs_0_, bf16[128,2048]{1,0:T(8,128)(2,1)S(1)} %collective-permute-done.8.refs_1_, ...), custom_call_target="tpu_custom_call" | custom-call | tf_op jit(solution)/shard_map/far_product/pallas_call | solution.py:424
  (19 shorter events, 0.0 us)
Async XLA Ops:
  0.0 22.5 %collective-permute-start.1 = (bf16[128,2048]{1,0:T(8,128)(2,1)}, bf16[128,2048]{1,0:T(8,128)(2,1)S(1)}, u32[]{:S(2)}, u32[]{:S(2)}) collective-permute-start(bf16[128,2048]{1,0:T(8,128)(2,1)} %share_ref.1), channel_id=1, source_target_pairs={{0,8},{2,10},{4,12},{6,14},{8,16},{9,1},{10,18},{11,3},{12,20},{13... | collective-permute-start | bytes 1572872 | tf_op jit(solution)/shard_map/ppermute | solution.py:282
  3.5 21.6 %collective-permute-start.7 = (bf16[128,2048]{1,0:T(8,128)(2,1)}, bf16[128,2048]{1,0:T(8,128)(2,1)S(1)}, u32[]{:S(2)}, u32[]{:S(2)}) collective-permute-start(bf16[128,2048]{1,0:T(8,128)(2,1)} %share_ref.1), channel_id=1, source_target_pairs={{0,16},{1,24},{2,22},{3,30},{4,20},{5,28},{6,18},{7,26},{8,25},{10... | collective-permute-start | bytes 1572872 | tf_op jit(solution)/shard_map/ppermute | solution.py:282
  5.8 32.5 %collective-permute-start.5 = (bf16[128,2048]{1,0:T(8,128)(2,1)}, bf16[128,2048]{1,0:T(8,128)(2,1)S(1)}, u32[]{:S(2)}, u32[]{:S(2)}) collective-permute-start(bf16[128,2048]{1,0:T(8,128)(2,1)} %share_ref.1), channel_id=1, source_target_pairs={{0,4},{2,6},{4,0},{6,2},{8,12},{10,14},{12,8},{14,10},{16,20},{18,... | collective-permute-start | bytes 1572872 | tf_op jit(solution)/shard_map/ppermute | solution.py:282
  22.5 17.7 %collective-permute-start.3 = (bf16[128,2048]{1,0:T(8,128)(2,1)S(1)}, bf16[128,2048]{1,0:T(8,128)(2,1)S(1)}, u32[]{:S(2)}, u32[]{:S(2)}) collective-permute-start(bf16[128,2048]{1,0:T(8,128)(2,1)S(1)} %collective-permute-done.1.refs_0_), channel_id=1, source_target_pairs={{1,5},{3,7},{5,1},{7,3},{8,12},{9,13},{10,14},{11,15},{12,8},{13,9... | collective-permute-start | bytes 1572872 | tf_op jit(solution)/shard_map/ppermute | solution.py:282
  25.1 18.4 %collective-permute-start.9 = (bf16[128,2048]{1,0:T(8,128)(2,1)S(1)}, bf16[128,2048]{1,0:T(8,128)(2,1)S(1)}, u32[]{:S(2)}, u32[]{:S(2)}) collective-permute-start(bf16[128,2048]{1,0:T(8,128)(2,1)S(1)} %collective-permute-done.7.refs_0_), channel_id=1, source_target_pairs={{0,4},{1,3},{2,6},{3,1},{4,0},{5,7},{6,2},{7,5},{8,12},{10,14},{12... | collective-permute-start | bytes 1572872 | tf_op jit(solution)/shard_map/ppermute | solution.py:282
  28.4 15.6 %copy-start.2 = (f32[2048]{0:T(1024)S(1)}, f32[2048]{0:T(1024)}, u32[]{:S(2)}) copy-start(f32[2048]{0:T(1024)} %param.14) | copy-start | bytes 24580
  31.3 15.0 %copy-start.3 = (bf16[31,512]{1,0:T(8,128)(2,1)S(1)}, bf16[31,512]{1,0:T(8,128)(2,1)}, u32[]{:S(2)}) copy-start(bf16[31,512]{1,0:T(8,128)(2,1)} %taps_ref.1) | copy-start | bytes 95236
  31.3 15.0 %copy-start.6 = (f32[2]{0:T(128)S(1)}, f32[2]{0:T(128)}, u32[]{:S(2)}) copy-start(f32[2]{0:T(128)} %sinks_ref.1) | copy-start | bytes 28
  31.4 12.1 %collective-permute-start = (bf16[160,128]{1,0:T(8,128)(2,1)S(1)}, bf16[160,128]{1,0:T(8,128)(2,1)S(1)}, u32[]{:S(2)}, u32[]{:S(2)}) collective-permute-start(bf16[160,128]{1,0:T(8,128)(2,1)S(1)} %get-tuple-element.22), channel_id=1, source_target_pairs={{0,4},{4,8},{8,12},{12,16},{16,20},{20,24},{24,28},{1,5},{5,9},{9,... | collective-permute-start | bytes 122888 | tf_op jit(solution)/shard_map/ppermute | solution.py:25
  33.3 29.1 %collective-permute-start.2 = (bf16[128,2048]{1,0:T(8,128)(2,1)S(1)}, bf16[128,2048]{1,0:T(8,128)(2,1)S(1)}, u32[]{:S(2)}, u32[]{:S(2)}) collective-permute-start(bf16[128,2048]{1,0:T(8,128)(2,1)S(1)} %collective-permute-done.1.refs_0_), channel_id=1, source_target_pairs={{0,1},{1,0},{2,3},{3,2},{4,5},{5,4},{6,7},{7,6},{8,9},{9,8},{10,11... | collective-permute-start | bytes 1572872 | tf_op jit(solution)/shard_map/ppermute | solution.py:282
  38.2 24.1 %collective-permute-start.6 = (bf16[128,2048]{1,0:T(8,128)(2,1)S(1)}, bf16[128,2048]{1,0:T(8,128)(2,1)S(1)}, u32[]{:S(2)}, u32[]{:S(2)}) collective-permute-start(bf16[128,2048]{1,0:T(8,128)(2,1)S(1)} %collective-permute-done.5.refs_4_), channel_id=1, source_target_pairs={{0,1},{2,3},{4,5},{6,7},{8,9},{10,11},{12,13},{14,15},{16,17},{18,... | collective-permute-start | bytes 1572872 | tf_op jit(solution)/shard_map/ppermute | solution.py:282
  40.2 22.1 %collective-permute-start.4 = (bf16[128,2048]{1,0:T(8,128)(2,1)S(1)}, bf16[128,2048]{1,0:T(8,128)(2,1)S(1)}, u32[]{:S(2)}, u32[]{:S(2)}) collective-permute-start(bf16[128,2048]{1,0:T(8,128)(2,1)S(1)} %collective-permute-done.3.refs_2_), channel_id=1, source_target_pairs={{0,1},{1,0},{2,3},{3,2},{4,5},{5,4},{6,7},{7,6},{8,9},{9,8},{10,11... | collective-permute-start | bytes 1572872 | tf_op jit(solution)/shard_map/ppermute | solution.py:282
  43.5 20.3 %collective-permute-start.8 = (bf16[128,2048]{1,0:T(8,128)(2,1)S(1)}, bf16[128,2048]{1,0:T(8,128)(2,1)S(1)}, u32[]{:S(2)}, u32[]{:S(2)}) collective-permute-start(bf16[128,2048]{1,0:T(8,128)(2,1)S(1)} %collective-permute-done.7.refs_0_), channel_id=1, source_target_pairs={{0,1},{1,0},{2,3},{3,2},{4,5},{5,4},{6,7},{7,6},{8,9},{9,8},{10,11... | collective-permute-start | bytes 1572872 | tf_op jit(solution)/shard_map/ppermute | solution.py:282
  43.5 20.3 %collective-permute-start.10 = (bf16[128,2048]{1,0:T(8,128)(2,1)S(1)}, bf16[128,2048]{1,0:T(8,128)(2,1)S(1)}, u32[]{:S(2)}, u32[]{:S(2)}) collective-permute-start(bf16[128,2048]{1,0:T(8,128)(2,1)S(1)} %collective-permute-done.9.refs_2_), channel_id=1, source_target_pairs={{0,1},{1,0},{2,3},{3,2},{4,5},{5,4},{6,7},{7,6},{8,9},{9,8},{10,11... | collective-permute-start | bytes 1572872 | tf_op jit(solution)/shard_map/ppermute | solution.py:282
  44.0 17.7 %copy-start.1 = (bf16[512,512]{1,0:T(8,128)(2,1)S(1)}, bf16[512,512]{1,0:T(8,128)(2,1)}, u32[]{:S(2)}) copy-start(bf16[512,512]{1,0:T(8,128)(2,1)} %point_ref.1) | copy-start | bytes 1572868
  44.0 17.7 %copy-start.4 = (f32[1024]{0:T(1024)S(1)}, f32[1024]{0:T(1024)}, u32[]{:S(2)}) copy-start(f32[1024]{0:T(1024)} %param.24) | copy-start | bytes 12292
  44.0 17.7 %copy-start.5 = (f32[512]{0:T(512)S(1)}, f32[512]{0:T(512)}, u32[]{:S(2)}) copy-start(f32[512]{0:T(512)} %param.22) | copy-start | bytes 6148
  46.3 16.1 %copy-start = (bf16[128,2048]{1,0:T(8,128)(2,1)S(1)}, bf16[128,2048]{1,0:T(8,128)(2,1)}, u32[]{:S(2)}) copy-start(bf16[128,2048]{1,0:T(8,128)(2,1)} %share_ref.1) | copy-start | bytes 1572868

commit v3 on v2

--- a/solution.py
+++ b/solution.py
@@ -230,7 +230,9 @@
     heads_width = joint // 2
     width = shares * heads_width
 
-    def body(exchanged_ref, conv_gain_ref, point_ref, gain_ref, out_ref):
+    def body(exchanged_ref, conv_gain_ref, gain_ref, point_hbm, out_ref, point_ref, fetched):
+        fetch = pltpu.make_async_copy(point_hbm, point_ref, fetched)
+        fetch.start()
         attended = jnp.concatenate(
             [exchanged_ref[i, :, :heads_width] for i in range(shares)], axis=1
         ).astype(jnp.float32)
@@ -244,24 +246,35 @@
             * conv_gain_ref[...]
         )
         activated = (scaled * jax.nn.sigmoid(scaled)).astype(jnp.bfloat16)
-        pointwise = jnp.dot(activated, point_ref[...], preferred_element_type=jnp.float32)
         out_ref[:, :width] = (
             attended
             * lax.rsqrt(jnp.mean(attended * attended, axis=-1, keepdims=True) + NORM_EPSILON)
             * gain_ref[:, :width]
         ).astype(jnp.bfloat16)
+        fetch.wait()
+        pointwise = jnp.dot(activated, point_ref[...], preferred_element_type=jnp.float32)
         out_ref[:, width:] = (
             pointwise
             * lax.rsqrt(jnp.mean(pointwise * pointwise, axis=-1, keepdims=True) + NORM_EPSILON)
             * gain_ref[:, width:]
         ).astype(jnp.bfloat16)
 
+    vmem = pl.BlockSpec(memory_space=pltpu.VMEM)
     return pl.pallas_call(
         body,
+        in_specs=[vmem] * 3 + [pl.BlockSpec(memory_space=pl.ANY)],
+        out_specs=vmem,
         out_shape=jax.ShapeDtypeStruct((rows, output_gain.shape[0]), jnp.bfloat16),
+        scratch_shapes=[
+            pltpu.VMEM(point_weight.shape, point_weight.dtype),
+            pltpu.SemaphoreType.DMA(()),
+        ],
         compiler_params=pltpu.CompilerParams(vmem_limit_bytes=12 << 20),
         name="merge_mixers",
-    )(exchanged, conv_gain[None], point_weight, output_gain[None])
+    )(
+        exchanged, conv_gain[None], output_gain[None],
+        pltpu.with_memory_space_constraint(point_weight, pltpu.HBM),
+    )
 
 
 class ShareRoutes:
@@ -282,7 +295,10 @@
         return lax.ppermute(block, PLACE, found)
 
     def beside(self, line, side, lane):
-        return (line + 1 if lane % 2 == 0 else line - 1), side, lane
+        to_line = line + 1 if lane % 2 == 0 else line - 1
+        if 0 <= to_line < self.lines:
+            return to_line, side, lane
+        return line, 1 - side, lane ^ 1
 
     def beyond(self, line, side, lane):
         targets = far_lines(line, self.lines)
@@ -297,11 +313,14 @@
         from_line = line - 1 if lane % 2 == 0 else line + 1
         return (line if 0 <= from_line < self.lines else -1), 1 - side, lane
 
-    def lower_lane_across(self, line, side, lane):
-        return (line if lane % 2 == 0 else -1), 1 - side, lane
-
-    def upper_lane_from_lower(self, line, side, lane):
-        return (line if lane % 2 == 0 else -1), side, lane ^ 1
+    def inner(self, line, lane):
+        return line if 0 < line < self.lines - 1 and lane % 2 == 0 else -1
+
+    def inner_across(self, line, side, lane):
+        return self.inner(line, lane), 1 - side, lane
+
+    def inner_upper(self, line, side, lane):
+        return self.inner(line, lane), side, lane ^ 1
 
     def to_neighbours(self, line, side, lane):
         held = lane % 2 < len(far_lines(line, self.lines))
@@ -329,26 +348,41 @@
     return jnp.concatenate(found, axis=1)
 
 
-def near_product(merged, share, near_pieces, opposite_pieces, lines):
+def far_line(line, at_lane, lines):
+    before = jnp.maximum(line - 1, 0)
+    found = jnp.where(at_lane < before, at_lane, line + 2 + at_lane - before)
+    return jnp.where(found < lines, found, -1)
+
+
+def odd_row():
+    return lax.axis_index("tp") // 2 % 2
+
+
+def early_product(merged, share, near_pieces, opposite_pieces, far_pieces, lines):
     rows, _ = merged.shape
     share_rows, columns = share.shape
 
     def body(merged_ref, share_ref, *refs):
-        near_refs, opposite_refs, out_ref = refs[:4], refs[4:6], refs[6]
+        near_refs, opposite_refs, far_refs, out_ref = refs[:4], refs[4:6], refs[6:8], refs[8]
         line, side, lane = place_of_device()
 
-        def product(from_line, *parts):
+        def product(from_line, sides, *parts):
             return jnp.dot(
-                columns_of(merged_ref, from_line, (side, 1 - side), share_rows),
+                columns_of(merged_ref, from_line, sides, share_rows),
                 jnp.concatenate(parts, axis=0),
                 preferred_element_type=jnp.float32,
             )
 
+        both_sides = (side, 1 - side)
+        at_end = (line == 0) | (line == lines - 1)
+        holder = jnp.where(line == lines - 1, 1, 0)
         for which in range(2):
-
-            @pl.when(lane == which)
-            def _():
-                out_ref[...] = product(line, share_ref[...], opposite_refs[which][...])
+            held = holder == (lane, 1 - lane)[which]
+            for ends, ref in ((True, near_refs[which]), (False, opposite_refs[which])):
+
+                @pl.when(held & (at_end == ends))
+                def _():
+                    out_ref[...] = product(line, both_sides, share_ref[...], ref[...])
 
         for which in range(2):
             at_lane = (lane, 1 - lane)[which]
@@ -356,51 +390,54 @@
 
             @pl.when((from_line >= 0) & (from_line < lines))
             def _():
-                out_ref[...] += product(from_line, near_refs[which][...], near_refs[2 + which][...])
+                out_ref[...] += product(
+                    from_line, both_sides, near_refs[which][...], near_refs[2 + which][...]
+                )
+
+        first_side = jnp.where(odd_row() == 1, 1 - side, side)
+        for which in range(2):
+            from_line = far_line(line, (lane, 1 - lane)[which], lines)
+
+            @pl.when(from_line >= 0)
+            def _():
+                out_ref[...] += product(from_line, (first_side,), far_refs[which][...])
 
     vmem = pl.BlockSpec(memory_space=pltpu.VMEM)
     return pl.pallas_call(
         body,
-        in_specs=[vmem] * 8,
+        in_specs=[vmem] * 10,
         out_specs=vmem,
         out_shape=jax.ShapeDtypeStruct((rows, columns), jnp.float32),
         compiler_params=pltpu.CompilerParams(vmem_limit_bytes=16 << 20),
-        name="near_product",
-    )(merged, share, *near_pieces, *opposite_pieces)
-
-
-def far_product(merged, near_sum, far_pieces, lines):
+        name="early_product",
+    )(merged, share, *near_pieces, *opposite_pieces, *far_pieces)
+
+
+def late_product(merged, early_sum, far_pieces, lines):
     rows, _ = merged.shape
     share_rows, columns = far_pieces[0].shape
     chunk = 512
 
-    def body(merged_ref, near_ref, *refs):
-        piece_refs, out_hbm, rounded, sent = refs[:4], refs[4], refs[5], refs[6]
+    def body(merged_ref, early_ref, *refs):
+        far_refs, out_hbm, rounded, sent = refs[:2], refs[2], refs[3], refs[4]
         line, side, lane = place_of_device()
-        first_side = jnp.where(lax.axis_index("tp") // 2 % 2 == 1, 1 - side, side)
-        before = jnp.maximum(line - 1, 0)
-
-        def other_line(index):
-            found = jnp.where(index < before, index, line + 2 + index - before)
-            return jnp.where(found < lines, found, -1)
-
-        sources = [other_line(lane), other_line(1 - lane)]
+        last_side = jnp.where(odd_row() == 1, side, 1 - side)
+        sources = [far_line(line, lane, lines), far_line(line, 1 - lane, lines)]
 
         def finish(slots):
-            left = [
-                columns_of(merged_ref, sources[slot], (first_side, 1 - first_side), share_rows)
-                for slot in slots
-            ]
-            left = jnp.concatenate(left, axis=1) if left else None
+            if slots:
+                left = [
+                    columns_of(merged_ref, sources[slot], (last_side,), share_rows)
+                    for slot in slots
+                ]
+                left = jnp.concatenate(left, axis=1)
             copies = []
             for first in range(0, columns, chunk):
                 here = slice(first, first + chunk)
-                total = near_ref[:, here]
+                total = early_ref[:, here]
                 if slots:
-                    right = [piece_refs[2 * i + slot][:, here] for slot in slots for i in range(2)]
-                    total = total + jnp.dot(
-                        left, jnp.concatenate(right, axis=0), preferred_element_type=jnp.float32
-                    )
+                    right = jnp.concatenate([far_refs[slot][:, here] for slot in slots], axis=0)
+                    total = total + jnp.dot(left, right, preferred_element_type=jnp.float32)
                 rounded[:, here] = total.astype(rounded.dtype)
                 copies.append(
                     pltpu.make_async_copy(
@@ -423,7 +460,7 @@
     vmem = pl.BlockSpec(memory_space=pltpu.VMEM)
     return pl.pallas_call(
         body,
-        in_specs=[vmem] * 6,
+        in_specs=[vmem] * 4,
         out_specs=pl.BlockSpec(memory_space=pl.ANY),
         out_shape=pltpu.HBM((rows, columns), jnp.bfloat16),
         scratch_shapes=[
@@ -431,8 +468,8 @@
             pltpu.SemaphoreType.DMA((columns // chunk,)),
         ],
         compiler_params=pltpu.CompilerParams(vmem_limit_bytes=16 << 20),
-        name="far_product",
-    )(merged, near_sum, *far_pieces)
+        name="late_product",
+    )(merged, early_sum, *far_pieces)
 
 
 def on_device(
@@ -467,16 +504,18 @@
     exchanged = lax.all_to_all(mixed, "tp", split_axis=0, concat_axis=0, tiled=True)
     merged = merge_mixers(exchanged, conv_gain, point_weight, output_gain)
     if by_shares:
-        opposite = routes.send(output_weight, routes.lower_lane_across)
+        opposite = routes.send(output_weight, routes.inner_across)
         near_across = routes.send(near, routes.holders_across)
         far_other = routes.send(far, routes.to_neighbours)
         near_pieces = near, routes.send(near, routes.lanes)
         near_pieces += near_across, routes.send(near_across, routes.lanes)
-        opposite_pieces = opposite, routes.send(opposite, routes.upper_lane_from_lower)
+        opposite_pieces = opposite, routes.send(opposite, routes.inner_upper)
         far_pieces = far, routes.send(far, routes.lanes)
-        far_pieces += far_other, routes.send(far_other, routes.lanes)
-        near_sum = near_product(merged, output_weight, near_pieces, opposite_pieces, lines)
-        return far_product(merged, near_sum, far_pieces, lines)
+        last_pieces = far_other, routes.send(far_other, routes.lanes)
+        early_sum = early_product(
+            merged, output_weight, near_pieces, opposite_pieces, far_pieces, lines
+        )
+        return late_product(merged, early_sum, last_pieces, lines)
     projected = jnp.dot(
         merged,
         lax.all_gather(output_weight, "sp", axis=0, tiled=True),

time: 65.4 us -> 67.1 us (1.026)
  waiting for transfers between devices: 17.6 us -> 19.6 us
  Pallas kernels: 12.4 us -> 14 us
  starting transfers between devices: 23.3 us -> 21.8 us
    ppermute x1, waiting for transfers between devices: 3.17 us -> 5.06 us  [from_behind(): return lax.ppermute(block, axis, route)]
    ppermute x10, starting transfers between devices: 21.4 us -> 19.8 us  [send(): return lax.ppermute(block, PLACE, found)]
    pallas_call x3, Pallas kernels: 3.26 us -> 4.79 us  [the longest x1 1.82 us: early_product(): pl.pallas_call(body, in_specs=[vmem] * 10, out_specs=vmem, out_shape=jax....]
  transfers between devices with their start and end apart: 11 -> 11, of which waited for: 3 -> 3; matrix products, arithmetic and copies ran while one was open for 0% -> 0% of each run, Pallas kernels for 17% -> 19%
where the time goes in v3:
time: 67.1 us; the launch traced here: 66.7 us
  starting transfers between devices  21.8 us (32%)
  waiting for transfers between devices  19.6 us (29%)
  Pallas kernels  14 us (21%)
  blocking collectives  11.2 us (17%)
    ppermute x10, starting transfers between devices, send(): return lax.ppermute(block, PLACE, found)  19.8 us
    ppermute x10, waiting for transfers between devices, send(): return lax.ppermute(block, PLACE, found)  14.5 us
    all_to_all x1, blocking collectives, on_device(): lax.all_to_all(mixed, 'tp', split_axis=0, concat_axis=0, tiled=True)  11.2 us
    ppermute x1, waiting for transfers between devices, from_behind(): return lax.ppermute(block, axis, route)  5.06 us
    pallas_call x1, Pallas kernels, mix_rows(): pl.pallas_call(body, in_specs=[scalars] + [whole] * 8, out_specs=whole, o...  3.94 us
    pallas_call x1, Pallas kernels, project_last(): pl.pallas_call(body, in_specs=[pl.BlockSpec(memory_space=pl.ANY)] * 7, ou...  2.94 us
    pallas_call x1, Pallas kernels, project_rest(): pl.pallas_call(body, in_specs=[vmem] * 3, out_specs=[vmem] * 3, out_shape...  2.3 us
    ppermute x1, starting transfers between devices, from_behind(): return lax.ppermute(block, axis, route)  1.92 us
  transfers between devices with their start and end apart: 11, of which 3 were waited for; matrix products, arithmetic and copies ran while one was open for 0% of the time, Pallas kernels for 19%

profile of v3, /device:TPU:18, one launch (start us, length us, event | category | flops | bytes accessed | tf_op | source)
XLA Modules:
  0.0 66.7 jit_solution(8736379540469022965)
XLA Ops:
  0.0 1.6 %collective-permute-start.1 = (bf16[128,2048]{1,0:T(8,128)(2,1)}, bf16[128,2048]{1,0:T(8,128)(2,1)S(1)}, u32[]{:S(2)}, u32[]{:S(2)}) collective-permute-start(bf16[128,2048]{1,0:T(8,128)(2,1)} %share_ref.1), channel_id=1, source_target_pairs={{0,8},{1,4},{2,10},{3,6},{4,12},{5,0},{6,14},{7,2},{8,16},{9,1},{1... | collective-permute-start | bytes 1572872 | tf_op jit(solution)/shard_map/ppermute | solution.py:295
  1.6 2.2 %collective-permute-start.7 = (bf16[128,2048]{1,0:T(8,128)(2,1)}, bf16[128,2048]{1,0:T(8,128)(2,1)S(1)}, u32[]{:S(2)}, u32[]{:S(2)}) collective-permute-start(bf16[128,2048]{1,0:T(8,128)(2,1)} %share_ref.1), channel_id=1, source_target_pairs={{0,16},{1,24},{2,22},{3,30},{4,20},{5,28},{6,18},{7,26},{8,25},{10... | collective-permute-start | bytes 1572872 | tf_op jit(solution)/shard_map/ppermute | solution.py:295
  3.8 2.4 %collective-permute-start.5 = (bf16[128,2048]{1,0:T(8,128)(2,1)}, bf16[128,2048]{1,0:T(8,128)(2,1)S(1)}, u32[]{:S(2)}, u32[]{:S(2)}) collective-permute-start(bf16[128,2048]{1,0:T(8,128)(2,1)} %share_ref.1), channel_id=1, source_target_pairs={{8,12},{10,14},{12,8},{14,10},{16,20},{18,22},{20,16},{22,18}} | collective-permute-start | bytes 1572872 | tf_op jit(solution)/shard_map/ppermute | solution.py:295
  6.3 14.4 %collective-permute-done.1.refs_0_ = bf16[128,2048]{1,0:T(8,128)(2,1)S(1)} collective-permute-done((bf16[128,2048]{1,0:T(8,128)(2,1)}, bf16[128,2048]{1,0:T(8,128)(2,1)S(1)}, u32[]{:S(2)}, u32[]{:S(2)}) %collective-permute-start.1) | collective-permute-done | bytes 524320 | tf_op jit(solution)/shard_map/ppermute | solution.py:295
  20.6 2.4 %collective-permute-start.3 = (bf16[128,2048]{1,0:T(8,128)(2,1)S(1)}, bf16[128,2048]{1,0:T(8,128)(2,1)S(1)}, u32[]{:S(2)}, u32[]{:S(2)}) collective-permute-start(bf16[128,2048]{1,0:T(8,128)(2,1)S(1)} %collective-permute-done.1.refs_0_), channel_id=1, source_target_pairs={{1,5},{3,7},{5,1},{7,3},{8,12},{9,13},{10,14},{11,15},{12,8},{13,9... | collective-permute-start | bytes 1572872 | tf_op jit(solution)/shard_map/ppermute | solution.py:295
  23.1 0.1 collective-permute-done.7.refs_6_
  23.2 3.3 %collective-permute-start.9 = (bf16[128,2048]{1,0:T(8,128)(2,1)S(1)}, bf16[128,2048]{1,0:T(8,128)(2,1)S(1)}, u32[]{:S(2)}, u32[]{:S(2)}) collective-permute-start(bf16[128,2048]{1,0:T(8,128)(2,1)S(1)} %collective-permute-done.7.refs_6_), channel_id=1, source_target_pairs={{0,4},{1,3},{2,6},{3,1},{4,0},{5,7},{6,2},{7,5},{8,12},{10,14},{12... | collective-permute-start | bytes 1572872 | tf_op jit(solution)/shard_map/ppermute | solution.py:295
  26.5 2.9 %project_last.1 = (bf16[256,128]{1,0:T(8,128)(2,1)S(1)}, bf16[256,128]{1,0:T(8,128)(2,1)S(1)}, bf16[256,128]{1,0:T(8,128)(2,1)S(1)}, bf16[160,128]{1,0:T(8,128)(...) custom-call(f32[1,2048]{1,0:T(1,128)} %bitcast.5, bf16[1024,2048]{1,0:T(8,128)(2,1)} %tokens_hbm.1, ...), custom_call_target="tpu_custom_call" | custom-call | tf_op jit(solution)/shard_map/project_last/pallas_call | solution.py:109
  29.4 0.0 copy-start.2
  29.5 0.0 copy-start.5
  29.5 1.9 %collective-permute-start = (bf16[160,128]{1,0:T(8,128)(2,1)S(1)}, bf16[160,128]{1,0:T(8,128)(2,1)S(1)}, u32[]{:S(2)}, u32[]{:S(2)}) collective-permute-start(bf16[160,128]{1,0:T(8,128)(2,1)S(1)} %get-tuple-element.22), channel_id=1, source_target_pairs={{0,4},{4,8},{8,12},{12,16},{16,20},{20,24},{24,28},{1,5},{5,9},{9,... | collective-permute-start | bytes 122888 | tf_op jit(solution)/shard_map/ppermute | solution.py:25
  31.4 4.9 %collective-permute-start.2 = (bf16[128,2048]{1,0:T(8,128)(2,1)S(1)}, bf16[128,2048]{1,0:T(8,128)(2,1)S(1)}, u32[]{:S(2)}, u32[]{:S(2)}) collective-permute-start(bf16[128,2048]{1,0:T(8,128)(2,1)S(1)} %collective-permute-done.1.refs_0_), channel_id=1, source_target_pairs={{0,1},{1,0},{2,3},{3,2},{4,5},{5,4},{6,7},{7,6},{8,9},{9,8},{10,11... | collective-permute-start | bytes 1572872 | tf_op jit(solution)/shard_map/ppermute | solution.py:295
  36.3 5.1 %collective-permute-done.earlier_ref = bf16[160,128]{1,0:T(8,128)(2,1)S(1)} collective-permute-done((bf16[160,128]{1,0:T(8,128)(2,1)S(1)}, bf16[160,128]{1,0:T(8,128)(2,1)S(1)}, u32[]{:S(2)}, u32[]{:S(2)}) %collective-permute-start) | collective-permute-done | bytes 40992 | tf_op jit(solution)/shard_map/ppermute | solution.py:25
  41.3 2.4 %collective-permute-start.6 = (bf16[128,2048]{1,0:T(8,128)(2,1)S(1)}, bf16[128,2048]{1,0:T(8,128)(2,1)S(1)}, u32[]{:S(2)}, u32[]{:S(2)}) collective-permute-start(bf16[128,2048]{1,0:T(8,128)(2,1)S(1)} %collective-permute-done.5.refs_4_), channel_id=1, source_target_pairs={{8,9},{10,11},{12,13},{14,15},{16,17},{18,19},{20,21},{22,23}} | collective-permute-start | bytes 1572872 | tf_op jit(solution)/shard_map/ppermute | solution.py:295
  43.8 0.0 collective-permute-done.3.refs_2_
  43.8 0.1 collective-permute-start.4
  43.9 0.5 collective-permute-start.10
  44.4 2.3 %project_rest.1 = (bf16[768,128]{1,0:T(8,128)(2,1)S(1)}, bf16[768,128]{1,0:T(8,128)(2,1)S(1)}, bf16[768,128]{1,0:T(8,128)(2,1)S(1)}) custom-call(f32[1,2048]{1,0:T(1,128)S(1)} %bitcast.6, bf16[768,2048]{1,0:T(8,128)(2,1)S(1)} %get-tuple-element.14.tokens_ref, bf16[2048,512]{1,0:T(8,128)(2,1)S(1)} %get-tuple-element.15.joined_ref), custom_call_target="tpu_custom_call" | custom-call | tf_op jit(solution)/shard_map/project_rest/pallas_call | solution.py:145
  46.7 0.0 copy-start
  46.7 3.9 %mix_rows.1 = bf16[4,256,256]{2,1,0:T(8,128)(2,1)S(1)} custom-call(f32[2]{0:T(128)S(1)} %copy-done.5, bf16[768,128]{1,0:T(8,128)(2,1)S(1)} %get-tuple-element.16.queries_ref, bf16[768,128]{1,0:T(8,128)(2,1)S(1)} %get-tuple-element.17.pairs_ref, bf16[768,128]{1,0:T(8,128)(2,1)S(1)} %get-tuple-element.18.gated_ref, ...), custom_call_target="tpu_custom_call" | custom-call | tf_op jit(solution)/shard_map/mix_rows/pallas_call | solution.py:214
  50.6 11.2 %all_to_all.5.exchanged_ref = bf16[4,256,256]{2,1,0:T(8,128)(2,1)S(1)} all-to-all(bf16[4,256,256]{2,1,0:T(8,128)(2,1)S(1)} %mix_rows.1), channel_id=1, replica_groups=mesh['sp'=8,'tp'=4] {'tp'}, dimensions={0} | all-to-all | bytes 1048576 | tf_op jit(solution)/shard_map/all_to_all | solution.py:504
  61.9 1.7 %merge_mixers.1.merged_ref = bf16[256,1024]{1,0:T(8,128)(2,1)S(1)} custom-call(bf16[4,256,256]{2,1,0:T(8,128)(2,1)S(1)} %all_to_all.5.exchanged_ref, f32[1,512]{1,0:T(1,128)S(1)} %bitcast.8, f32[1,1024]{1,0:T(1,128)S(1)} %bitcast.7, bf16[512,512]{1,0:T(8,128)(2,1)} %point_hbm.1), custom_call_target="tpu_custom_call" | custom-call | tf_op jit(solution)/shard_map/merge_mixers/pallas_call | solution.py:263
  63.6 1.8 %early_product.1.early_ref = f32[256,2048]{1,0:T(8,128)S(1)} custom-call(bf16[256,1024]{1,0:T(8,128)(2,1)S(1)} %merge_mixers.1.merged_ref, bf16[128,2048]{1,0:T(8,128)(2,1)S(1)} %copy-done, bf16[128,2048]{1,0:T(8,128)(2,1)S(1)} %collective-permute-done.1.refs_0_, bf16[128,2048]{1,0:T(8,128)(2,1)S(1)} %collective-permute-done.2.refs_1_, ...), custom_call_target="tpu_custom_call" | custom-call | tf_op jit(solution)/shard_map/early_product/pallas_call | solution.py:406
  65.5 1.2 %late_product.1 = bf16[256,2048]{1,0:T(8,128)(2,1)} custom-call(bf16[256,1024]{1,0:T(8,128)(2,1)S(1)} %merge_mixers.1.merged_ref, f32[256,2048]{1,0:T(8,128)S(1)} %early_product.1.early_ref, bf16[128,2048]{1,0:T(8,128)(2,1)S(1)} %collective-permute-done.9.refs_0_, bf16[128,2048]{1,0:T(8,128)(2,1)S(1)} %collective-permute-done.10.refs_1_), custom_call_target="tpu_custom_call" | custom-call | tf_op jit(solution)/shard_map/late_product/pallas_call | solution.py:461
  (17 shorter events, 0.0 us)
Async XLA Ops:
  0.0 20.6 %collective-permute-start.1 = (bf16[128,2048]{1,0:T(8,128)(2,1)}, bf16[128,2048]{1,0:T(8,128)(2,1)S(1)}, u32[]{:S(2)}, u32[]{:S(2)}) collective-permute-start(bf16[128,2048]{1,0:T(8,128)(2,1)} %share_ref.1), channel_id=1, source_target_pairs={{0,8},{1,4},{2,10},{3,6},{4,12},{5,0},{6,14},{7,2},{8,16},{9,1},{1... | collective-permute-start | bytes 1572872 | tf_op jit(solution)/shard_map/ppermute | solution.py:295
  1.6 21.6 %collective-permute-start.7 = (bf16[128,2048]{1,0:T(8,128)(2,1)}, bf16[128,2048]{1,0:T(8,128)(2,1)S(1)}, u32[]{:S(2)}, u32[]{:S(2)}) collective-permute-start(bf16[128,2048]{1,0:T(8,128)(2,1)} %share_ref.1), channel_id=1, source_target_pairs={{0,16},{1,24},{2,22},{3,30},{4,20},{5,28},{6,18},{7,26},{8,25},{10... | collective-permute-start | bytes 1572872 | tf_op jit(solution)/shard_map/ppermute | solution.py:295
  3.8 37.5 %collective-permute-start.5 = (bf16[128,2048]{1,0:T(8,128)(2,1)}, bf16[128,2048]{1,0:T(8,128)(2,1)S(1)}, u32[]{:S(2)}, u32[]{:S(2)}) collective-permute-start(bf16[128,2048]{1,0:T(8,128)(2,1)} %share_ref.1), channel_id=1, source_target_pairs={{8,12},{10,14},{12,8},{14,10},{16,20},{18,22},{20,16},{22,18}} | collective-permute-start | bytes 1572872 | tf_op jit(solution)/shard_map/ppermute | solution.py:295
  20.6 23.1 %collective-permute-start.3 = (bf16[128,2048]{1,0:T(8,128)(2,1)S(1)}, bf16[128,2048]{1,0:T(8,128)(2,1)S(1)}, u32[]{:S(2)}, u32[]{:S(2)}) collective-permute-start(bf16[128,2048]{1,0:T(8,128)(2,1)S(1)} %collective-permute-done.1.refs_0_), channel_id=1, source_target_pairs={{1,5},{3,7},{5,1},{7,3},{8,12},{9,13},{10,14},{11,15},{12,8},{13,9... | collective-permute-start | bytes 1572872 | tf_op jit(solution)/shard_map/ppermute | solution.py:295
  23.2 20.7 %collective-permute-start.9 = (bf16[128,2048]{1,0:T(8,128)(2,1)S(1)}, bf16[128,2048]{1,0:T(8,128)(2,1)S(1)}, u32[]{:S(2)}, u32[]{:S(2)}) collective-permute-start(bf16[128,2048]{1,0:T(8,128)(2,1)S(1)} %collective-permute-done.7.refs_6_), channel_id=1, source_target_pairs={{0,4},{1,3},{2,6},{3,1},{4,0},{5,7},{6,2},{7,5},{8,12},{10,14},{12... | collective-permute-start | bytes 1572872 | tf_op jit(solution)/shard_map/ppermute | solution.py:295
  26.5 17.9 %copy-start.1 = (f32[2048]{0:T(1024)S(1)}, f32[2048]{0:T(1024)}, u32[]{:S(2)}) copy-start(f32[2048]{0:T(1024)} %param.14) | copy-start | bytes 24580
  29.4 17.2 %copy-start.2 = (bf16[31,512]{1,0:T(8,128)(2,1)S(1)}, bf16[31,512]{1,0:T(8,128)(2,1)}, u32[]{:S(2)}) copy-start(bf16[31,512]{1,0:T(8,128)(2,1)} %taps_ref.1) | copy-start | bytes 95236
  29.5 17.2 %copy-start.5 = (f32[2]{0:T(128)S(1)}, f32[2]{0:T(128)}, u32[]{:S(2)}) copy-start(f32[2]{0:T(128)} %sinks_ref.1) | copy-start | bytes 28
  29.5 11.9 %collective-permute-start = (bf16[160,128]{1,0:T(8,128)(2,1)S(1)}, bf16[160,128]{1,0:T(8,128)(2,1)S(1)}, u32[]{:S(2)}, u32[]{:S(2)}) collective-permute-start(bf16[160,128]{1,0:T(8,128)(2,1)S(1)} %get-tuple-element.22), channel_id=1, source_target_pairs={{0,4},{4,8},{8,12},{12,16},{16,20},{20,24},{24,28},{1,5},{5,9},{9,... | collective-permute-start | bytes 122888 | tf_op jit(solution)/shard_map/ppermute | solution.py:25
  31.4 32.2 %collective-permute-start.2 = (bf16[128,2048]{1,0:T(8,128)(2,1)S(1)}, bf16[128,2048]{1,0:T(8,128)(2,1)S(1)}, u32[]{:S(2)}, u32[]{:S(2)}) collective-permute-start(bf16[128,2048]{1,0:T(8,128)(2,1)S(1)} %collective-permute-done.1.refs_0_), channel_id=1, source_target_pairs={{0,1},{1,0},{2,3},{3,2},{4,5},{5,4},{6,7},{7,6},{8,9},{9,8},{10,11... | collective-permute-start | bytes 1572872 | tf_op jit(solution)/shard_map/ppermute | solution.py:295
  41.3 22.3 %collective-permute-start.8 = (bf16[128,2048]{1,0:T(8,128)(2,1)S(1)}, bf16[128,2048]{1,0:T(8,128)(2,1)S(1)}, u32[]{:S(2)}, u32[]{:S(2)}) collective-permute-start(bf16[128,2048]{1,0:T(8,128)(2,1)S(1)} %collective-permute-done.7.refs_6_), channel_id=1, source_target_pairs={{0,1},{1,0},{2,3},{3,2},{4,5},{5,4},{6,7},{7,6},{8,9},{9,8},{10,11... | collective-permute-start | bytes 1572872 | tf_op jit(solution)/shard_map/ppermute | solution.py:295
  41.3 22.3 %collective-permute-start.6 = (bf16[128,2048]{1,0:T(8,128)(2,1)S(1)}, bf16[128,2048]{1,0:T(8,128)(2,1)S(1)}, u32[]{:S(2)}, u32[]{:S(2)}) collective-permute-start(bf16[128,2048]{1,0:T(8,128)(2,1)S(1)} %collective-permute-done.5.refs_4_), channel_id=1, source_target_pairs={{8,9},{10,11},{12,13},{14,15},{16,17},{18,19},{20,21},{22,23}} | collective-permute-start | bytes 1572872 | tf_op jit(solution)/shard_map/ppermute | solution.py:295
  43.8 19.8 %collective-permute-start.4 = (bf16[128,2048]{1,0:T(8,128)(2,1)S(1)}, bf16[128,2048]{1,0:T(8,128)(2,1)S(1)}, u32[]{:S(2)}, u32[]{:S(2)}) collective-permute-start(bf16[128,2048]{1,0:T(8,128)(2,1)S(1)} %collective-permute-done.3.refs_2_), channel_id=1, source_target_pairs={{0,1},{1,0},{2,3},{3,2},{4,5},{5,4},{6,7},{7,6},{8,9},{9,8},{10,11... | collective-permute-start | bytes 1572872 | tf_op jit(solution)/shard_map/ppermute | solution.py:295
  43.9 21.6 %collective-permute-start.10 = (bf16[128,2048]{1,0:T(8,128)(2,1)S(1)}, bf16[128,2048]{1,0:T(8,128)(2,1)S(1)}, u32[]{:S(2)}, u32[]{:S(2)}) collective-permute-start(bf16[128,2048]{1,0:T(8,128)(2,1)S(1)} %collective-permute-done.9.refs_0_), channel_id=1, source_target_pairs={{0,1},{1,0},{2,3},{3,2},{4,5},{5,4},{6,7},{7,6},{8,9},{9,8},{10,11... | collective-permute-start | bytes 1572872 | tf_op jit(solution)/shard_map/ppermute | solution.py:295
  44.4 17.5 %copy-start.3 = (f32[1024]{0:T(1024)S(1)}, f32[1024]{0:T(1024)}, u32[]{:S(2)}) copy-start(f32[1024]{0:T(1024)} %param.24) | copy-start | bytes 12292
  44.4 17.5 %copy-start.4 = (f32[512]{0:T(512)S(1)}, f32[512]{0:T(512)}, u32[]{:S(2)}) copy-start(f32[512]{0:T(512)} %param.22) | copy-start | bytes 6148
  46.7 17.0 %copy-start = (bf16[128,2048]{1,0:T(8,128)(2,1)S(1)}, bf16[128,2048]{1,0:T(8,128)(2,1)}, u32[]{:S(2)}) copy-start(bf16[128,2048]{1,0:T(8,128)(2,1)} %share_ref.1) | copy-start | bytes 1572868

commit v4 on v3

--- a/solution.py
+++ b/solution.py
@@ -303,7 +303,7 @@
     def beyond(self, line, side, lane):
         targets = far_lines(line, self.lines)
         if lane % 2 >= len(targets):
-            return -1, side, lane
+            return (line if lane % 2 else -1), 1 - side, lane
         to_line = targets[lane % 2]
         to_side = 1 - side if lane // 2 % 2 else side
         to_lane = lane - lane % 2 + far_lines(to_line, self.lines).index(line)
@@ -312,15 +312,6 @@
     def holders_across(self, line, side, lane):
         from_line = line - 1 if lane % 2 == 0 else line + 1
         return (line if 0 <= from_line < self.lines else -1), 1 - side, lane
-
-    def inner(self, line, lane):
-        return line if 0 < line < self.lines - 1 and lane % 2 == 0 else -1
-
-    def inner_across(self, line, side, lane):
-        return self.inner(line, lane), 1 - side, lane
-
-    def inner_upper(self, line, side, lane):
-        return self.inner(line, lane), side, lane ^ 1
 
     def to_neighbours(self, line, side, lane):
         held = lane % 2 < len(far_lines(line, self.lines))
@@ -358,12 +349,12 @@
     return lax.axis_index("tp") // 2 % 2
 
 
-def early_product(merged, share, near_pieces, opposite_pieces, far_pieces, lines):
+def early_product(merged, share, near_pieces, far_pieces, lines):
     rows, _ = merged.shape
     share_rows, columns = share.shape
 
     def body(merged_ref, share_ref, *refs):
-        near_refs, opposite_refs, far_refs, out_ref = refs[:4], refs[4:6], refs[6:8], refs[8]
+        near_refs, far_refs, out_ref = refs[:4], refs[4:6], refs[6]
         line, side, lane = place_of_device()
 
         def product(from_line, sides, *parts):
@@ -375,10 +366,10 @@
 
         both_sides = (side, 1 - side)
         at_end = (line == 0) | (line == lines - 1)
-        holder = jnp.where(line == lines - 1, 1, 0)
+        holder = jnp.where(line == 0, 0, 1)
         for which in range(2):
             held = holder == (lane, 1 - lane)[which]
-            for ends, ref in ((True, near_refs[which]), (False, opposite_refs[which])):
+            for ends, ref in ((True, near_refs[which]), (False, far_refs[which])):
 
                 @pl.when(held & (at_end == ends))
                 def _():
@@ -405,12 +396,12 @@
     vmem = pl.BlockSpec(memory_space=pltpu.VMEM)
     return pl.pallas_call(
         body,
-        in_specs=[vmem] * 10,
+        in_specs=[vmem] * 8,
         out_specs=vmem,
         out_shape=jax.ShapeDtypeStruct((rows, columns), jnp.float32),
         compiler_params=pltpu.CompilerParams(vmem_limit_bytes=16 << 20),
         name="early_product",
-    )(merged, share, *near_pieces, *opposite_pieces, *far_pieces)
+    )(merged, share, *near_pieces, *far_pieces)
 
 
 def late_product(merged, early_sum, far_pieces, lines):
@@ -504,17 +495,13 @@
     exchanged = lax.all_to_all(mixed, "tp", split_axis=0, concat_axis=0, tiled=True)
     merged = merge_mixers(exchanged, conv_gain, point_weight, output_gain)
     if by_shares:
-        opposite = routes.send(output_weight, routes.inner_across)
         near_across = routes.send(near, routes.holders_across)
         far_other = routes.send(far, routes.to_neighbours)
         near_pieces = near, routes.send(near, routes.lanes)
         near_pieces += near_across, routes.send(near_across, routes.lanes)
-        opposite_pieces = opposite, routes.send(opposite, routes.inner_upper)
         far_pieces = far, routes.send(far, routes.lanes)
         last_pieces = far_other, routes.send(far_other, routes.lanes)
-        early_sum = early_product(
-            merged, output_weight, near_pieces, opposite_pieces, far_pieces, lines
-        )
+        early_sum = early_product(merged, output_weight, near_pieces, far_pieces, lines)
         return late_product(merged, early_sum, last_pieces, lines)
     projected = jnp.dot(
         merged,

time: 67.1 us -> 72.3 us (1.077)
  the two profiles are of different devices: /device:TPU:18 before, /device:TPU:16 now
where the time goes in v4:
time: 72.3 us; the launch traced here: 72 us
  waiting for transfers between devices  34.5 us (48%)
  Pallas kernels  14 us (19%)
  starting transfers between devices  12.1 us (17%)
  blocking collectives  11.2 us (15%)
    ppermute x8, waiting for transfers between devices, send(): return lax.ppermute(block, PLACE, found)  33.8 us
    all_to_all x1, blocking collectives, on_device(): lax.all_to_all(mixed, 'tp', split_axis=0, concat_axis=0, tiled=True)  11.2 us
    ppermute x8, starting transfers between devices, send(): return lax.ppermute(block, PLACE, found)  8.41 us
    pallas_call x1, Pallas kernels, mix_rows(): pl.pallas_call(body, in_specs=[scalars] + [whole] * 8, out_specs=whole, o...  3.93 us
    ppermute x1, starting transfers between devices, from_behind(): return lax.ppermute(block, axis, route)  3.64 us
    pallas_call x1, Pallas kernels, project_last(): pl.pallas_call(body, in_specs=[pl.BlockSpec(memory_space=pl.ANY)] * 7, ou...  2.95 us
    pallas_call x1, Pallas kernels, project_rest(): pl.pallas_call(body, in_specs=[vmem] * 3, out_specs=[vmem] * 3, out_shape...  2.33 us
    pallas_call x1, Pallas kernels, early_product(): pl.pallas_call(body, in_specs=[vmem] * 8, out_specs=vmem, out_shape=jax.S...  1.82 us
  transfers between devices with their start and end apart: 9, of which 4 were waited for; matrix products, arithmetic and copies ran while one was open for 0% of the time, Pallas kernels for 18%

profile of v4, /device:TPU:16, one launch (start us, length us, event | category | flops | bytes accessed | tf_op | source)
XLA Modules:
  0.0 72.0 jit_solution(12168808850376093079)
XLA Ops:
  0.0 1.6 %collective-permute-start.1 = (bf16[128,2048]{1,0:T(8,128)(2,1)}, bf16[128,2048]{1,0:T(8,128)(2,1)S(1)}, u32[]{:S(2)}, u32[]{:S(2)}) collective-permute-start(bf16[128,2048]{1,0:T(8,128)(2,1)} %share_ref.1), channel_id=1, source_target_pairs={{0,8},{1,4},{2,10},{3,6},{4,12},{5,0},{6,14},{7,2},{8,16},{9,1},{1... | collective-permute-start | bytes 1572872 | tf_op jit(solution)/shard_map/ppermute | solution.py:295
  1.6 0.3 collective-permute-start.5
  1.9 18.7 %collective-permute-done.1.refs_0_ = bf16[128,2048]{1,0:T(8,128)(2,1)S(1)} collective-permute-done((bf16[128,2048]{1,0:T(8,128)(2,1)}, bf16[128,2048]{1,0:T(8,128)(2,1)S(1)}, u32[]{:S(2)}, u32[]{:S(2)}) %collective-permute-start.1) | collective-permute-done | bytes 524320 | tf_op jit(solution)/shard_map/ppermute | solution.py:295
  20.6 3.4 %collective-permute-start.3 = (bf16[128,2048]{1,0:T(8,128)(2,1)S(1)}, bf16[128,2048]{1,0:T(8,128)(2,1)S(1)}, u32[]{:S(2)}, u32[]{:S(2)}) collective-permute-start(bf16[128,2048]{1,0:T(8,128)(2,1)S(1)} %collective-permute-done.1.refs_0_), channel_id=1, source_target_pairs={{1,5},{3,7},{5,1},{7,3},{8,12},{9,13},{10,14},{11,15},{12,8},{13,9... | collective-permute-start | bytes 1572872 | tf_op jit(solution)/shard_map/ppermute | solution.py:295
  24.0 2.5 %collective-permute-start.7 = (bf16[128,2048]{1,0:T(8,128)(2,1)S(1)}, bf16[128,2048]{1,0:T(8,128)(2,1)S(1)}, u32[]{:S(2)}, u32[]{:S(2)}) collective-permute-start(bf16[128,2048]{1,0:T(8,128)(2,1)S(1)} %collective-permute-done.5.refs_4_), channel_id=1, source_target_pairs={{0,4},{1,3},{2,6},{3,1},{4,0},{5,7},{6,2},{7,5},{8,12},{10,14},{12... | collective-permute-start | bytes 1572872 | tf_op jit(solution)/shard_map/ppermute | solution.py:295
  26.6 0.1 collective-permute-start.2
  26.7 0.5 collective-permute-start.6
  27.2 9.4 %collective-permute-done.3.refs_2_ = bf16[128,2048]{1,0:T(8,128)(2,1)S(1)} collective-permute-done((bf16[128,2048]{1,0:T(8,128)(2,1)S(1)}, bf16[128,2048]{1,0:T(8,128)(2,1)S(1)}, u32[]{:S(2)}, u32[]{:S(2)}) %collective-permute-start.3) | collective-permute-done | bytes 524320 | tf_op jit(solution)/shard_map/ppermute | solution.py:295
  36.6 0.0 collective-permute-start.4
  36.6 5.6 %collective-permute-done.7.refs_0_ = bf16[128,2048]{1,0:T(8,128)(2,1)S(1)} collective-permute-done((bf16[128,2048]{1,0:T(8,128)(2,1)S(1)}, bf16[128,2048]{1,0:T(8,128)(2,1)S(1)}, u32[]{:S(2)}, u32[]{:S(2)}) %collective-permute-start.7) | collective-permute-done | bytes 524320 | tf_op jit(solution)/shard_map/ppermute | solution.py:295
  42.2 2.9 %project_last.1 = (bf16[256,128]{1,0:T(8,128)(2,1)S(1)}, bf16[256,128]{1,0:T(8,128)(2,1)S(1)}, bf16[256,128]{1,0:T(8,128)(2,1)S(1)}, bf16[160,128]{1,0:T(8,128)(...) custom-call(f32[1,2048]{1,0:T(1,128)} %bitcast.5, bf16[1024,2048]{1,0:T(8,128)(2,1)} %tokens_hbm.1, ...), custom_call_target="tpu_custom_call" | custom-call | tf_op jit(solution)/shard_map/project_last/pallas_call | solution.py:109
  45.2 0.0 copy-start.2
  45.2 0.0 copy-start.5
  45.2 3.6 %collective-permute-start = (bf16[160,128]{1,0:T(8,128)(2,1)S(1)}, bf16[160,128]{1,0:T(8,128)(2,1)S(1)}, u32[]{:S(2)}, u32[]{:S(2)}) collective-permute-start(bf16[160,128]{1,0:T(8,128)(2,1)S(1)} %get-tuple-element.22), channel_id=1, source_target_pairs={{0,4},{4,8},{8,12},{12,16},{16,20},{20,24},{24,28},{1,5},{5,9},{9,... | collective-permute-start | bytes 122888 | tf_op jit(solution)/shard_map/ppermute | solution.py:25
  48.9 0.0 copy-start.3
  48.9 0.0 copy-start.4
  48.9 2.3 %project_rest.1 = (bf16[768,128]{1,0:T(8,128)(2,1)S(1)}, bf16[768,128]{1,0:T(8,128)(2,1)S(1)}, bf16[768,128]{1,0:T(8,128)(2,1)S(1)}) custom-call(f32[1,2048]{1,0:T(1,128)S(1)} %bitcast.6, bf16[768,2048]{1,0:T(8,128)(2,1)S(1)} %get-tuple-element.14.tokens_ref, bf16[2048,512]{1,0:T(8,128)(2,1)S(1)} %get-tuple-element.15.joined_ref), custom_call_target="tpu_custom_call" | custom-call | tf_op jit(solution)/shard_map/project_rest/pallas_call | solution.py:145
  51.2 0.0 copy-start
  51.2 0.8 %collective-permute-done.earlier_ref = bf16[160,128]{1,0:T(8,128)(2,1)S(1)} collective-permute-done((bf16[160,128]{1,0:T(8,128)(2,1)S(1)}, bf16[160,128]{1,0:T(8,128)(2,1)S(1)}, u32[]{:S(2)}, u32[]{:S(2)}) %collective-permute-start) | collective-permute-done | bytes 40992 | tf_op jit(solution)/shard_map/ppermute | solution.py:25
  52.0 3.9 %mix_rows.1 = bf16[4,256,256]{2,1,0:T(8,128)(2,1)S(1)} custom-call(f32[2]{0:T(128)S(1)} %copy-done.5, bf16[768,128]{1,0:T(8,128)(2,1)S(1)} %get-tuple-element.16.queries_ref, bf16[768,128]{1,0:T(8,128)(2,1)S(1)} %get-tuple-element.17.pairs_ref, bf16[768,128]{1,0:T(8,128)(2,1)S(1)} %get-tuple-element.18.gated_ref, ...), custom_call_target="tpu_custom_call" | custom-call | tf_op jit(solution)/shard_map/mix_rows/pallas_call | solution.py:214
  55.9 11.2 %all_to_all.5.exchanged_ref = bf16[4,256,256]{2,1,0:T(8,128)(2,1)S(1)} all-to-all(bf16[4,256,256]{2,1,0:T(8,128)(2,1)S(1)} %mix_rows.1), channel_id=1, replica_groups=mesh['sp'=8,'tp'=4] {'tp'}, dimensions={0} | all-to-all | bytes 1048576 | tf_op jit(solution)/shard_map/all_to_all | solution.py:495
  67.2 1.7 %merge_mixers.1.merged_ref = bf16[256,1024]{1,0:T(8,128)(2,1)S(1)} custom-call(bf16[4,256,256]{2,1,0:T(8,128)(2,1)S(1)} %all_to_all.5.exchanged_ref, f32[1,512]{1,0:T(1,128)S(1)} %bitcast.8, f32[1,1024]{1,0:T(1,128)S(1)} %bitcast.7, bf16[512,512]{1,0:T(8,128)(2,1)} %point_hbm.1), custom_call_target="tpu_custom_call" | custom-call | tf_op jit(solution)/shard_map/merge_mixers/pallas_call | solution.py:263
  68.9 1.8 %early_product.1.early_ref = f32[256,2048]{1,0:T(8,128)S(1)} custom-call(bf16[256,1024]{1,0:T(8,128)(2,1)S(1)} %merge_mixers.1.merged_ref, bf16[128,2048]{1,0:T(8,128)(2,1)S(1)} %copy-done, bf16[128,2048]{1,0:T(8,128)(2,1)S(1)} %collective-permute-done.1.refs_0_, bf16[128,2048]{1,0:T(8,128)(2,1)S(1)} %collective-permute-done.2.refs_1_, ...), custom_call_target="tpu_custom_call" | custom-call | tf_op jit(solution)/shard_map/early_product/pallas_call | solution.py:397
  70.7 1.2 %late_product.1 = bf16[256,2048]{1,0:T(8,128)(2,1)} custom-call(bf16[256,1024]{1,0:T(8,128)(2,1)S(1)} %merge_mixers.1.merged_ref, f32[256,2048]{1,0:T(8,128)S(1)} %early_product.1.early_ref, bf16[128,2048]{1,0:T(8,128)(2,1)S(1)} %collective-permute-done.7.refs_0_, bf16[128,2048]{1,0:T(8,128)(2,1)S(1)} %collective-permute-done.8.refs_1_), custom_call_target="tpu_custom_call" | custom-call | tf_op jit(solution)/shard_map/late_product/pallas_call | solution.py:452
  (13 shorter events, 0.0 us)
Async XLA Ops:
  0.0 20.6 %collective-permute-start.1 = (bf16[128,2048]{1,0:T(8,128)(2,1)}, bf16[128,2048]{1,0:T(8,128)(2,1)S(1)}, u32[]{:S(2)}, u32[]{:S(2)}) collective-permute-start(bf16[128,2048]{1,0:T(8,128)(2,1)} %share_ref.1), channel_id=1, source_target_pairs={{0,8},{1,4},{2,10},{3,6},{4,12},{5,0},{6,14},{7,2},{8,16},{9,1},{1... | collective-permute-start | bytes 1572872 | tf_op jit(solution)/shard_map/ppermute | solution.py:295
  1.6 22.4 %collective-permute-start.5 = (bf16[128,2048]{1,0:T(8,128)(2,1)}, bf16[128,2048]{1,0:T(8,128)(2,1)S(1)}, u32[]{:S(2)}, u32[]{:S(2)}) collective-permute-start(bf16[128,2048]{1,0:T(8,128)(2,1)} %share_ref.1), channel_id=1, source_target_pairs={{0,16},{1,24},{2,22},{3,30},{4,20},{5,28},{6,18},{7,26},{8,25},{9,... | collective-permute-start | bytes 1572872 | tf_op jit(solution)/shard_map/ppermute | solution.py:295
  20.6 16.0 %collective-permute-start.3 = (bf16[128,2048]{1,0:T(8,128)(2,1)S(1)}, bf16[128,2048]{1,0:T(8,128)(2,1)S(1)}, u32[]{:S(2)}, u32[]{:S(2)}) collective-permute-start(bf16[128,2048]{1,0:T(8,128)(2,1)S(1)} %collective-permute-done.1.refs_0_), channel_id=1, source_target_pairs={{1,5},{3,7},{5,1},{7,3},{8,12},{9,13},{10,14},{11,15},{12,8},{13,9... | collective-permute-start | bytes 1572872 | tf_op jit(solution)/shard_map/ppermute | solution.py:295
  24.0 18.2 %collective-permute-start.7 = (bf16[128,2048]{1,0:T(8,128)(2,1)S(1)}, bf16[128,2048]{1,0:T(8,128)(2,1)S(1)}, u32[]{:S(2)}, u32[]{:S(2)}) collective-permute-start(bf16[128,2048]{1,0:T(8,128)(2,1)S(1)} %collective-permute-done.5.refs_4_), channel_id=1, source_target_pairs={{0,4},{1,3},{2,6},{3,1},{4,0},{5,7},{6,2},{7,5},{8,12},{10,14},{12... | collective-permute-start | bytes 1572872 | tf_op jit(solution)/shard_map/ppermute | solution.py:295
  26.6 42.3 %collective-permute-start.2 = (bf16[128,2048]{1,0:T(8,128)(2,1)S(1)}, bf16[128,2048]{1,0:T(8,128)(2,1)S(1)}, u32[]{:S(2)}, u32[]{:S(2)}) collective-permute-start(bf16[128,2048]{1,0:T(8,128)(2,1)S(1)} %collective-permute-done.1.refs_0_), channel_id=1, source_target_pairs={{0,1},{1,0},{2,3},{3,2},{4,5},{5,4},{6,7},{7,6},{8,9},{9,8},{10,11... | collective-permute-start | bytes 1572872 | tf_op jit(solution)/shard_map/ppermute | solution.py:295
  26.7 42.2 %collective-permute-start.6 = (bf16[128,2048]{1,0:T(8,128)(2,1)S(1)}, bf16[128,2048]{1,0:T(8,128)(2,1)S(1)}, u32[]{:S(2)}, u32[]{:S(2)}) collective-permute-start(bf16[128,2048]{1,0:T(8,128)(2,1)S(1)} %collective-permute-done.5.refs_4_), channel_id=1, source_target_pairs={{0,1},{1,0},{2,3},{3,2},{4,5},{5,4},{6,7},{7,6},{8,9},{9,8},{10,11... | collective-permute-start | bytes 1572872 | tf_op jit(solution)/shard_map/ppermute | solution.py:295
  36.6 32.3 %collective-permute-start.4 = (bf16[128,2048]{1,0:T(8,128)(2,1)S(1)}, bf16[128,2048]{1,0:T(8,128)(2,1)S(1)}, u32[]{:S(2)}, u32[]{:S(2)}) collective-permute-start(bf16[128,2048]{1,0:T(8,128)(2,1)S(1)} %collective-permute-done.3.refs_2_), channel_id=1, source_target_pairs={{0,1},{1,0},{2,3},{3,2},{4,5},{5,4},{6,7},{7,6},{8,9},{9,8},{10,11... | collective-permute-start | bytes 1572872 | tf_op jit(solution)/shard_map/ppermute | solution.py:295
  42.2 28.5 %collective-permute-start.8 = (bf16[128,2048]{1,0:T(8,128)(2,1)S(1)}, bf16[128,2048]{1,0:T(8,128)(2,1)S(1)}, u32[]{:S(2)}, u32[]{:S(2)}) collective-permute-start(bf16[128,2048]{1,0:T(8,128)(2,1)S(1)} %collective-permute-done.7.refs_0_), channel_id=1, source_target_pairs={{0,1},{1,0},{2,3},{3,2},{4,5},{5,4},{6,7},{7,6},{8,9},{9,8},{10,11... | collective-permute-start | bytes 1572872 | tf_op jit(solution)/shard_map/ppermute | solution.py:295
  42.2 6.6 %copy-start.1 = (f32[2048]{0:T(1024)S(1)}, f32[2048]{0:T(1024)}, u32[]{:S(2)}) copy-start(f32[2048]{0:T(1024)} %param.14) | copy-start | bytes 24580
  45.2 6.8 %copy-start.2 = (bf16[31,512]{1,0:T(8,128)(2,1)S(1)}, bf16[31,512]{1,0:T(8,128)(2,1)}, u32[]{:S(2)}) copy-start(bf16[31,512]{1,0:T(8,128)(2,1)} %taps_ref.1) | copy-start | bytes 95236
  45.2 6.8 %copy-start.5 = (f32[2]{0:T(128)S(1)}, f32[2]{0:T(128)}, u32[]{:S(2)}) copy-start(f32[2]{0:T(128)} %sinks_ref.1) | copy-start | bytes 28
  45.2 6.8 %collective-permute-start = (bf16[160,128]{1,0:T(8,128)(2,1)S(1)}, bf16[160,128]{1,0:T(8,128)(2,1)S(1)}, u32[]{:S(2)}, u32[]{:S(2)}) collective-permute-start(bf16[160,128]{1,0:T(8,128)(2,1)S(1)} %get-tuple-element.22), channel_id=1, source_target_pairs={{0,4},{4,8},{8,12},{12,16},{16,20},{20,24},{24,28},{1,5},{5,9},{9,... | collective-permute-start | bytes 122888 | tf_op jit(solution)/shard_map/ppermute | solution.py:25
  48.9 18.3 %copy-start.3 = (f32[1024]{0:T(1024)S(1)}, f32[1024]{0:T(1024)}, u32[]{:S(2)}) copy-start(f32[1024]{0:T(1024)} %param.24) | copy-start | bytes 12292
  48.9 18.3 %copy-start.4 = (f32[512]{0:T(512)S(1)}, f32[512]{0:T(512)}, u32[]{:S(2)}) copy-start(f32[512]{0:T(512)} %param.22) | copy-start | bytes 6148
  51.2 17.7 %copy-start = (bf16[128,2048]{1,0:T(8,128)(2,1)S(1)}, bf16[128,2048]{1,0:T(8,128)(2,1)}, u32[]{:S(2)}) copy-start(bf16[128,2048]{1,0:T(8,128)(2,1)} %share_ref.1) | copy-start | bytes 1572868

commit v5 on v4

--- a/solution.py
+++ b/solution.py
@@ -110,14 +110,15 @@
         body,
         in_specs=[pl.BlockSpec(memory_space=pl.ANY)] * 7,
         out_specs=[vmem] * len(shapes),
-        out_shape=[jax.ShapeDtypeStruct(shape, jnp.bfloat16) for shape in shapes],
+        out_shape=[jax.ShapeDtypeStruct(shape, jnp.bfloat16) for shape in shapes[:4]]
+        + [pltpu.VMEM(shape, jnp.bfloat16) for shape in shapes[4:]],
         scratch_shapes=[
             pltpu.VMEM((BLOCK, width), jnp.bfloat16),
             pltpu.VMEM((pair_width, width), jnp.bfloat16),
             pltpu.VMEM((1, width), jnp.float32),
             pltpu.SemaphoreType.DMA((8,)),
         ],
-        compiler_params=pltpu.CompilerParams(vmem_limit_bytes=20 << 20),
+        compiler_params=pltpu.CompilerParams(vmem_limit_bytes=10 << 20),
         name="project_last",
     )(*in_hbm)
 
@@ -151,9 +152,13 @@
             for columns in (heads_width, pair_width, channels)
         ],
         scratch_shapes=[pltpu.VMEM((blocks, BLOCK, width), jnp.bfloat16)],
-        compiler_params=pltpu.CompilerParams(vmem_limit_bytes=24 << 20),
+        compiler_params=pltpu.CompilerParams(vmem_limit_bytes=12 << 20),
         name="project_rest",
-    )(norm_gain[None], tokens, joined)
+    )(
+        norm_gain[None],
+        pltpu.with_memory_space_constraint(tokens, pltpu.VMEM),
+        pltpu.with_memory_space_constraint(joined, pltpu.VMEM),
+    )
 
 
 def mix_rows(first_rows, last_rows, earlier, sinks, taps, shares):
@@ -300,35 +305,36 @@
             return to_line, side, lane
         return line, 1 - side, lane ^ 1
 
+    def relays(self, line, lane):
+        return line + (lane & 1) == 2
+
     def beyond(self, line, side, lane):
-        targets = far_lines(line, self.lines)
-        if lane % 2 >= len(targets):
-            return (line if lane % 2 else -1), 1 - side, lane
-        to_line = targets[lane % 2]
-        to_side = 1 - side if lane // 2 % 2 else side
-        to_lane = lane - lane % 2 + far_lines(to_line, self.lines).index(line)
-        return to_line, to_side, to_lane
+        last = self.lines - 1
+        row = lane - lane % 2
+        if self.relays(line, lane):
+            return (0 if line == 1 else last), side, row
+        if 0 < line < last:
+            return line, 1 - side, row + 1
+        if lane % 2 == (0 if line == 0 else 1):
+            return (2 if line == 0 else last - 2), side, row
+        return last - line, (1 - side if lane // 2 % 2 else side), row + 1
 
     def holders_across(self, line, side, lane):
         from_line = line - 1 if lane % 2 == 0 else line + 1
         return (line if 0 <= from_line < self.lines else -1), 1 - side, lane
 
     def to_neighbours(self, line, side, lane):
-        held = lane % 2 < len(far_lines(line, self.lines))
-        to = (1 - side, lane) if lane % 2 == 0 else (side, lane ^ 2)
-        return (line if held else -1), *to
+        if lane % 2 == 0:
+            return line, 1 - side, lane
+        return (line if line in (0, self.lines - 1) else -1), side, lane ^ 2
 
     def lanes(self, line, side, lane):
         return line, side, lane ^ 1
 
 
-def far_lines(line, lines):
-    return [other for other in range(lines) if abs(other - line) > 1]
-
-
 def place_of_device():
-    position, lane = lax.axis_index("sp"), lax.axis_index("tp") % 2
-    return position // 2, position % 2, lane
+    position = lax.axis_index("sp")
+    return position >> 1, position & 1, lax.axis_index("tp") & 1
 
 
 def columns_of(merged_ref, from_line, sides, share_rows):
@@ -340,9 +346,13 @@
 
 
 def far_line(line, at_lane, lines):
-    before = jnp.maximum(line - 1, 0)
-    found = jnp.where(at_lane < before, at_lane, line + 2 + at_lane - before)
-    return jnp.where(found < lines, found, -1)
+    two_away = jnp.where(line < 2, line + 2, line - 2)
+    at_end = (line == 0) | (line == lines - 1)
+    return jnp.where(at_lane == 0, two_away, jnp.where(at_end, lines - 1 - line, -1))
+
+
+def far_side(side, at_lane):
+    return jnp.where((at_lane == 1) & (odd_row() == 1), 1 - side, side)
 
 
 def odd_row():
@@ -385,13 +395,15 @@
                     from_line, both_sides, near_refs[which][...], near_refs[2 + which][...]
                 )
 
-        first_side = jnp.where(odd_row() == 1, 1 - side, side)
         for which in range(2):
-            from_line = far_line(line, (lane, 1 - lane)[which], lines)
+            at_lane = (lane, 1 - lane)[which]
+            from_line = far_line(line, at_lane, lines)
 
             @pl.when(from_line >= 0)
             def _():
-                out_ref[...] += product(from_line, (first_side,), far_refs[which][...])
+                out_ref[...] += product(
+                    from_line, (far_side(side, at_lane),), far_refs[which][...]
+                )
 
     vmem = pl.BlockSpec(memory_space=pltpu.VMEM)
     return pl.pallas_call(
@@ -412,13 +424,13 @@
     def body(merged_ref, early_ref, *refs):
         far_refs, out_hbm, rounded, sent = refs[:2], refs[2], refs[3], refs[4]
         line, side, lane = place_of_device()
-        last_side = jnp.where(odd_row() == 1, side, 1 - side)
         sources = [far_line(line, lane, lines), far_line(line, 1 - lane, lines)]
+        sides = [1 - far_side(side, lane), 1 - far_side(side, 1 - lane)]
 
         def finish(slots):
             if slots:
                 left = [
-                    columns_of(merged_ref, sources[slot], (last_side,), share_rows)
+                    columns_of(merged_ref, sources[slot], (sides[slot],), share_rows)
                     for slot in slots
                 ]
                 left = jnp.concatenate(left, axis=1)
@@ -484,7 +496,10 @@
     if by_shares:
         routes = ShareRoutes(lines, tp_size)
         near = routes.send(output_weight, routes.beside)
-        far = routes.send(output_weight, routes.beyond)
+        relays = routes.relays(lax.axis_index("sp") >> 1, lax.axis_index("tp"))
+        norm_gain, relays = lax.optimization_barrier((norm_gain, relays))
+        passed_on = jnp.where(relays, near, output_weight)
+        far = routes.send(passed_on, routes.beyond)
     *last_rows, tail, joined, other_tokens = project_last(
         tokens, norm_gain, query_weight, key_weight, value_weight, conv_in_weight, conv_gate_weight
     )
@@ -512,7 +527,7 @@
 
 
 def sends_shares(sp_size, tp_size):
-    return sp_size % 2 == 0 and tp_size % 4 == 0 and 3 <= sp_size // 2 <= 4
+    return sp_size == 2 * 4 and tp_size % 4 == 0
 
 
 def solution(mesh):

time: 72.3 us -> 67.1 us (0.928)
  the two profiles are of different devices: /device:TPU:16 before, /device:TPU:0 now
where the time goes in v5:
time: 67.1 us; the launch traced here: 66.8 us
  waiting for transfers between devices  21.5 us (32%)
  starting transfers between devices  18.7 us (28%)
  Pallas kernels  13.9 us (21%)
  blocking collectives  11.4 us (17%)
  other arithmetic  1.1 us (2%)
    ppermute x8, waiting for transfers between devices, send(): return lax.ppermute(block, PLACE, found)  21.5 us
    ppermute x8, starting transfers between devices, send(): return lax.ppermute(block, PLACE, found)  16.1 us
    all_to_all x1, blocking collectives, on_device(): lax.all_to_all(mixed, 'tp', split_axis=0, concat_axis=0, tiled=True)  11.4 us
    pallas_call x1, Pallas kernels, mix_rows(): pl.pallas_call(body, in_specs=[scalars] + [whole] * 8, out_specs=whole, o...  3.94 us
    pallas_call x1, Pallas kernels, project_last(): pl.pallas_call(body, in_specs=[pl.BlockSpec(memory_space=pl.ANY)] * 7, ou...  2.95 us
    ppermute x1, starting transfers between devices, from_behind(): return lax.ppermute(block, axis, route)  2.58 us
    pallas_call x1, Pallas kernels, project_rest(): pl.pallas_call(body, in_specs=[vmem] * 3, out_specs=[vmem] * 3, out_shape...  2.31 us
    pallas_call x1, Pallas kernels, early_product(): pl.pallas_call(body, in_specs=[vmem] * 8, out_specs=vmem, out_shape=jax.S...  1.75 us
  transfers between devices with their start and end apart: 9, of which 3 were waited for; matrix products, arithmetic and copies ran while one was open for 0% of the time, Pallas kernels for 19%

profile of v5, /device:TPU:0, one launch (start us, length us, event | category | flops | bytes accessed | tf_op | source)
XLA Modules:
  0.0 66.8 jit_solution(12202314604969908598)
XLA Ops:
  0.0 3.1 %collective-permute-start.1 = (bf16[128,2048]{1,0:T(8,128)(2,1)}, bf16[128,2048]{1,0:T(8,128)(2,1)S(1)}, u32[]{:S(2)}, u32[]{:S(2)}) collective-permute-start(bf16[128,2048]{1,0:T(8,128)(2,1)} %share_ref.1), channel_id=1, source_target_pairs={{0,8},{1,4},{2,10},{3,6},{4,12},{5,0},{6,14},{7,2},{8,16},{9,1},{1... | collective-permute-start | bytes 1572872 | tf_op jit(solution)/shard_map/ppermute | solution.py:300
  3.1 7.0 %collective-permute-done.1.refs_0_ = bf16[128,2048]{1,0:T(8,128)(2,1)S(1)} collective-permute-done((bf16[128,2048]{1,0:T(8,128)(2,1)}, bf16[128,2048]{1,0:T(8,128)(2,1)S(1)}, u32[]{:S(2)}, u32[]{:S(2)}) %collective-permute-start.1) | collective-permute-done | bytes 524320 | tf_op jit(solution)/shard_map/ppermute | solution.py:300
  10.1 1.1 %broadcast_select_fusion = bf16[128,2048]{1,0:T(8,128)(2,1)S(1)} fusion(bf16[128,2048]{1,0:T(8,128)(2,1)S(1)} %collective-permute-done.1.refs_0_, bf16[128,2048]{1,0:T(8,128)(2,1)} %share_ref.1, pred[]{:T(512)S(6)} %eq.3), kind=kLoop, calls=%fused_computation | loop fusion | flops 262144 | bytes 1572865 | tf_op jit(solution)/shard_map/jit(_where)/select_n | solution.py:501
  11.2 2.4 %collective-permute-start.5 = (bf16[128,2048]{1,0:T(8,128)(2,1)S(1)}, bf16[128,2048]{1,0:T(8,128)(2,1)S(1)}, u32[]{:S(2)}, u32[]{:S(2)}) collective-permute-start(bf16[128,2048]{1,0:T(8,128)(2,1)S(1)} %broadcast_select_fusion), channel_id=1, source_target_pairs={{0,16},{1,25},{2,18},{3,31},{4,20},{5,29},{6,22},{7,27},{8,13},{9,... | collective-permute-start | bytes 1572872 | tf_op jit(solution)/shard_map/ppermute | solution.py:300
  13.6 0.7 %collective-permute-start.3 = (bf16[128,2048]{1,0:T(8,128)(2,1)S(1)}, bf16[128,2048]{1,0:T(8,128)(2,1)S(1)}, u32[]{:S(2)}, u32[]{:S(2)}) collective-permute-start(bf16[128,2048]{1,0:T(8,128)(2,1)S(1)} %collective-permute-done.1.refs_0_), channel_id=1, source_target_pairs={{1,5},{3,7},{5,1},{7,3},{8,12},{9,13},{10,14},{11,15},{12,8},{13,9... | collective-permute-start | bytes 1572872 | tf_op jit(solution)/shard_map/ppermute | solution.py:300
  14.3 11.0 %collective-permute-done.5.refs_4_ = bf16[128,2048]{1,0:T(8,128)(2,1)S(1)} collective-permute-done((bf16[128,2048]{1,0:T(8,128)(2,1)S(1)}, bf16[128,2048]{1,0:T(8,128)(2,1)S(1)}, u32[]{:S(2)}, u32[]{:S(2)}) %collective-permute-start.5) | collective-permute-done | bytes 524320 | tf_op jit(solution)/shard_map/ppermute | solution.py:300
  25.2 3.4 %collective-permute-start.7 = (bf16[128,2048]{1,0:T(8,128)(2,1)S(1)}, bf16[128,2048]{1,0:T(8,128)(2,1)S(1)}, u32[]{:S(2)}, u32[]{:S(2)}) collective-permute-start(bf16[128,2048]{1,0:T(8,128)(2,1)S(1)} %collective-permute-done.5.refs_4_), channel_id=1, source_target_pairs={{0,4},{1,3},{2,6},{3,1},{4,0},{5,7},{6,2},{7,5},{8,12},{10,14},{12... | collective-permute-start | bytes 1572872 | tf_op jit(solution)/shard_map/ppermute | solution.py:300
  28.7 3.6 %collective-permute-start.2 = (bf16[128,2048]{1,0:T(8,128)(2,1)S(1)}, bf16[128,2048]{1,0:T(8,128)(2,1)S(1)}, u32[]{:S(2)}, u32[]{:S(2)}) collective-permute-start(bf16[128,2048]{1,0:T(8,128)(2,1)S(1)} %collective-permute-done.1.refs_0_), channel_id=1, source_target_pairs={{0,1},{1,0},{2,3},{3,2},{4,5},{5,4},{6,7},{7,6},{8,9},{9,8},{10,11... | collective-permute-start | bytes 1572872 | tf_op jit(solution)/shard_map/ppermute | solution.py:300
  32.2 0.1 collective-permute-start.6
  32.3 0.4 collective-permute-start.4
  32.7 3.5 %collective-permute-done.7.refs_0_ = bf16[128,2048]{1,0:T(8,128)(2,1)S(1)} collective-permute-done((bf16[128,2048]{1,0:T(8,128)(2,1)S(1)}, bf16[128,2048]{1,0:T(8,128)(2,1)S(1)}, u32[]{:S(2)}, u32[]{:S(2)}) %collective-permute-start.7) | collective-permute-done | bytes 524320 | tf_op jit(solution)/shard_map/ppermute | solution.py:300
  36.3 2.4 %collective-permute-start.8 = (bf16[128,2048]{1,0:T(8,128)(2,1)S(1)}, bf16[128,2048]{1,0:T(8,128)(2,1)S(1)}, u32[]{:S(2)}, u32[]{:S(2)}) collective-permute-start(bf16[128,2048]{1,0:T(8,128)(2,1)S(1)} %collective-permute-done.7.refs_0_), channel_id=1, source_target_pairs={{0,1},{1,0},{2,3},{3,2},{4,5},{5,4},{6,7},{7,6},{8,9},{9,8},{10,11... | collective-permute-start | bytes 1572872 | tf_op jit(solution)/shard_map/ppermute | solution.py:300
  38.7 2.9 %project_last.1 = (bf16[256,128]{1,0:T(8,128)(2,1)S(1)}, bf16[256,128]{1,0:T(8,128)(2,1)S(1)}, bf16[256,128]{1,0:T(8,128)(2,1)S(1)}, bf16[160,128]{1,0:T(8,128)(...) custom-call(f32[1,2048]{1,0:T(1,128)} %bitcast.5, bf16[1024,2048]{1,0:T(8,128)(2,1)} %tokens_hbm.1, ...), custom_call_target="tpu_custom_call" | custom-call | tf_op jit(solution)/shard_map/project_last/pallas_call | solution.py:109
  41.7 0.0 copy-start.2
  41.7 0.0 copy-start.5
  41.7 2.6 %collective-permute-start = (bf16[160,128]{1,0:T(8,128)(2,1)S(1)}, bf16[160,128]{1,0:T(8,128)(2,1)S(1)}, u32[]{:S(2)}, u32[]{:S(2)}) collective-permute-start(bf16[160,128]{1,0:T(8,128)(2,1)S(1)} %get-tuple-element.25), channel_id=1, source_target_pairs={{0,4},{4,8},{8,12},{12,16},{16,20},{20,24},{24,28},{1,5},{5,9},{9,... | collective-permute-start | bytes 122888 | tf_op jit(solution)/shard_map/ppermute | solution.py:25
  44.3 0.0 copy-start.4
  44.3 2.3 %project_rest.1 = (bf16[768,128]{1,0:T(8,128)(2,1)S(1)}, bf16[768,128]{1,0:T(8,128)(2,1)S(1)}, bf16[768,128]{1,0:T(8,128)(2,1)S(1)}) custom-call(f32[1,2048]{1,0:T(1,128)S(1)} %bitcast.6, bf16[768,2048]{1,0:T(8,128)(2,1)S(1)} %get-tuple-element.17.tokens_ref, bf16[2048,512]{1,0:T(8,128)(2,1)S(1)} %get-tuple-element.18.joined_ref), custom_call_target="tpu_custom_call" | custom-call | tf_op jit(solution)/shard_map/project_rest/pallas_call | solution.py:146
  46.6 0.0 copy-start
  46.7 3.9 %mix_rows.1 = bf16[4,256,256]{2,1,0:T(8,128)(2,1)S(1)} custom-call(f32[2]{0:T(128)S(1)} %copy-done.5, bf16[768,128]{1,0:T(8,128)(2,1)S(1)} %get-tuple-element.19.queries_ref, bf16[768,128]{1,0:T(8,128)(2,1)S(1)} %get-tuple-element.20.pairs_ref, bf16[768,128]{1,0:T(8,128)(2,1)S(1)} %get-tuple-element.21.gated_ref, ...), custom_call_target="tpu_custom_call" | custom-call | tf_op jit(solution)/shard_map/mix_rows/pallas_call | solution.py:219
  50.6 11.4 %all_to_all.5.exchanged_ref = bf16[4,256,256]{2,1,0:T(8,128)(2,1)S(1)} all-to-all(bf16[4,256,256]{2,1,0:T(8,128)(2,1)S(1)} %mix_rows.1), channel_id=1, replica_groups=mesh['sp'=8,'tp'=4] {'tp'}, dimensions={0} | all-to-all | bytes 1048576 | tf_op jit(solution)/shard_map/all_to_all | solution.py:510
  62.0 1.7 %merge_mixers.1.merged_ref = bf16[256,1024]{1,0:T(8,128)(2,1)S(1)} custom-call(bf16[4,256,256]{2,1,0:T(8,128)(2,1)S(1)} %all_to_all.5.exchanged_ref, f32[1,512]{1,0:T(1,128)S(1)} %bitcast.8, f32[1,1024]{1,0:T(1,128)S(1)} %bitcast.7, bf16[512,512]{1,0:T(8,128)(2,1)} %point_hbm.1), custom_call_target="tpu_custom_call" | custom-call | tf_op jit(solution)/shard_map/merge_mixers/pallas_call | solution.py:268
  63.8 1.8 %early_product.1.early_ref = f32[256,2048]{1,0:T(8,128)S(1)} custom-call(bf16[256,1024]{1,0:T(8,128)(2,1)S(1)} %merge_mixers.1.merged_ref, bf16[128,2048]{1,0:T(8,128)(2,1)S(1)} %copy-done, bf16[128,2048]{1,0:T(8,128)(2,1)S(1)} %collective-permute-done.1.refs_0_, bf16[128,2048]{1,0:T(8,128)(2,1)S(1)} %collective-permute-done.2.refs_1_, ...), custom_call_target="tpu_custom_call" | custom-call | tf_op jit(solution)/shard_map/early_product/pallas_call | solution.py:409
  65.5 1.3 %late_product.1 = bf16[256,2048]{1,0:T(8,128)(2,1)} custom-call(bf16[256,1024]{1,0:T(8,128)(2,1)S(1)} %merge_mixers.1.merged_ref, f32[256,2048]{1,0:T(8,128)S(1)} %early_product.1.early_ref, bf16[128,2048]{1,0:T(8,128)(2,1)S(1)} %collective-permute-done.7.refs_0_, bf16[128,2048]{1,0:T(8,128)(2,1)S(1)} %collective-permute-done.8.refs_1_), custom_call_target="tpu_custom_call" | custom-call | tf_op jit(solution)/shard_map/late_product/pallas_call | solution.py:464
  (14 shorter events, 0.0 us)
Async XLA Ops:
  0.0 10.1 %collective-permute-start.1 = (bf16[128,2048]{1,0:T(8,128)(2,1)}, bf16[128,2048]{1,0:T(8,128)(2,1)S(1)}, u32[]{:S(2)}, u32[]{:S(2)}) collective-permute-start(bf16[128,2048]{1,0:T(8,128)(2,1)} %share_ref.1), channel_id=1, source_target_pairs={{0,8},{1,4},{2,10},{3,6},{4,12},{5,0},{6,14},{7,2},{8,16},{9,1},{1... | collective-permute-start | bytes 1572872 | tf_op jit(solution)/shard_map/ppermute | solution.py:300
  11.2 14.1 %collective-permute-start.5 = (bf16[128,2048]{1,0:T(8,128)(2,1)S(1)}, bf16[128,2048]{1,0:T(8,128)(2,1)S(1)}, u32[]{:S(2)}, u32[]{:S(2)}) collective-permute-start(bf16[128,2048]{1,0:T(8,128)(2,1)S(1)} %broadcast_select_fusion), channel_id=1, source_target_pairs={{0,16},{1,25},{2,18},{3,31},{4,20},{5,29},{6,22},{7,27},{8,13},{9,... | collective-permute-start | bytes 1572872 | tf_op jit(solution)/shard_map/ppermute | solution.py:300
  13.6 18.7 %collective-permute-start.3 = (bf16[128,2048]{1,0:T(8,128)(2,1)S(1)}, bf16[128,2048]{1,0:T(8,128)(2,1)S(1)}, u32[]{:S(2)}, u32[]{:S(2)}) collective-permute-start(bf16[128,2048]{1,0:T(8,128)(2,1)S(1)} %collective-permute-done.1.refs_0_), channel_id=1, source_target_pairs={{1,5},{3,7},{5,1},{7,3},{8,12},{9,13},{10,14},{11,15},{12,8},{13,9... | collective-permute-start | bytes 1572872 | tf_op jit(solution)/shard_map/ppermute | solution.py:300
  25.2 11.1 %collective-permute-start.7 = (bf16[128,2048]{1,0:T(8,128)(2,1)S(1)}, bf16[128,2048]{1,0:T(8,128)(2,1)S(1)}, u32[]{:S(2)}, u32[]{:S(2)}) collective-permute-start(bf16[128,2048]{1,0:T(8,128)(2,1)S(1)} %collective-permute-done.5.refs_4_), channel_id=1, source_target_pairs={{0,4},{1,3},{2,6},{3,1},{4,0},{5,7},{6,2},{7,5},{8,12},{10,14},{12... | collective-permute-start | bytes 1572872 | tf_op jit(solution)/shard_map/ppermute | solution.py:300
  28.7 35.1 %collective-permute-start.2 = (bf16[128,2048]{1,0:T(8,128)(2,1)S(1)}, bf16[128,2048]{1,0:T(8,128)(2,1)S(1)}, u32[]{:S(2)}, u32[]{:S(2)}) collective-permute-start(bf16[128,2048]{1,0:T(8,128)(2,1)S(1)} %collective-permute-done.1.refs_0_), channel_id=1, source_target_pairs={{0,1},{1,0},{2,3},{3,2},{4,5},{5,4},{6,7},{7,6},{8,9},{9,8},{10,11... | collective-permute-start | bytes 1572872 | tf_op jit(solution)/shard_map/ppermute | solution.py:300
  32.2 31.5 %collective-permute-start.6 = (bf16[128,2048]{1,0:T(8,128)(2,1)S(1)}, bf16[128,2048]{1,0:T(8,128)(2,1)S(1)}, u32[]{:S(2)}, u32[]{:S(2)}) collective-permute-start(bf16[128,2048]{1,0:T(8,128)(2,1)S(1)} %collective-permute-done.5.refs_4_), channel_id=1, source_target_pairs={{0,1},{1,0},{2,3},{3,2},{4,5},{5,4},{6,7},{7,6},{8,9},{9,8},{10,11... | collective-permute-start | bytes 1572872 | tf_op jit(solution)/shard_map/ppermute | solution.py:300
  32.3 31.4 %collective-permute-start.4 = (bf16[128,2048]{1,0:T(8,128)(2,1)S(1)}, bf16[128,2048]{1,0:T(8,128)(2,1)S(1)}, u32[]{:S(2)}, u32[]{:S(2)}) collective-permute-start(bf16[128,2048]{1,0:T(8,128)(2,1)S(1)} %collective-permute-done.3.refs_2_), channel_id=1, source_target_pairs={{0,1},{1,0},{2,3},{3,2},{4,5},{5,4},{6,7},{7,6},{8,9},{9,8},{10,11... | collective-permute-start | bytes 1572872 | tf_op jit(solution)/shard_map/ppermute | solution.py:300
  36.3 29.2 %collective-permute-start.8 = (bf16[128,2048]{1,0:T(8,128)(2,1)S(1)}, bf16[128,2048]{1,0:T(8,128)(2,1)S(1)}, u32[]{:S(2)}, u32[]{:S(2)}) collective-permute-start(bf16[128,2048]{1,0:T(8,128)(2,1)S(1)} %collective-permute-done.7.refs_0_), channel_id=1, source_target_pairs={{0,1},{1,0},{2,3},{3,2},{4,5},{5,4},{6,7},{7,6},{8,9},{9,8},{10,11... | collective-permute-start | bytes 1572872 | tf_op jit(solution)/shard_map/ppermute | solution.py:300
  38.7 5.6 %copy-start.1 = (f32[2048]{0:T(1024)S(1)}, f32[2048]{0:T(1024)}, u32[]{:S(2)}) copy-start(f32[2048]{0:T(1024)} %param.14) | copy-start | bytes 24580
  41.7 5.0 %copy-start.2 = (bf16[31,512]{1,0:T(8,128)(2,1)S(1)}, bf16[31,512]{1,0:T(8,128)(2,1)}, u32[]{:S(2)}) copy-start(bf16[31,512]{1,0:T(8,128)(2,1)} %taps_ref.1) | copy-start | bytes 95236
  41.7 5.0 %copy-start.5 = (f32[2]{0:T(128)S(1)}, f32[2]{0:T(128)}, u32[]{:S(2)}) copy-start(f32[2]{0:T(128)} %sinks_ref.1) | copy-start | bytes 28
  41.7 5.0 %collective-permute-start = (bf16[160,128]{1,0:T(8,128)(2,1)S(1)}, bf16[160,128]{1,0:T(8,128)(2,1)S(1)}, u32[]{:S(2)}, u32[]{:S(2)}) collective-permute-start(bf16[160,128]{1,0:T(8,128)(2,1)S(1)} %get-tuple-element.25), channel_id=1, source_target_pairs={{0,4},{4,8},{8,12},{12,16},{16,20},{20,24},{24,28},{1,5},{5,9},{9,... | collective-permute-start | bytes 122888 | tf_op jit(solution)/shard_map/ppermute | solution.py:25
  44.3 17.7 %copy-start.3 = (f32[1024]{0:T(1024)S(1)}, f32[1024]{0:T(1024)}, u32[]{:S(2)}) copy-start(f32[1024]{0:T(1024)} %param.24) | copy-start | bytes 12292
  44.3 17.7 %copy-start.4 = (f32[512]{0:T(512)S(1)}, f32[512]{0:T(512)}, u32[]{:S(2)}) copy-start(f32[512]{0:T(512)} %param.22) | copy-start | bytes 6148
  46.6 17.1 %copy-start = (bf16[128,2048]{1,0:T(8,128)(2,1)S(1)}, bf16[128,2048]{1,0:T(8,128)(2,1)}, u32[]{:S(2)}) copy-start(bf16[128,2048]{1,0:T(8,128)(2,1)} %share_ref.1) | copy-start | bytes 1572868

commit v6 on v5

--- a/solution.py
+++ b/solution.py
@@ -170,19 +170,20 @@
 
     def body(
         sinks_ref, queries_ref, pairs_ref, gated_ref, last_queries, last_pairs, last_gated,
-        earlier_ref, taps_ref, out_ref, band, extended,
+        earlier_ref, taps_ref, out_hbm, out_ref, band, extended, sent,
     ):
+        copies = [
+            pltpu.make_async_copy(out_ref.at[i], out_hbm.at[i], sent.at[i]) for i in range(shares)
+        ]
         band[:WINDOW] = earlier_ref[:WINDOW]
         band[WINDOW : WINDOW + rest] = pairs_ref[...]
         band[WINDOW + rest :] = last_pairs[...]
         extended[:HALO] = earlier_ref[WINDOW:].astype(jnp.float32)
         extended[HALO : HALO + rest] = gated_ref[...].astype(jnp.float32)
         extended[HALO + rest :] = last_gated[...].astype(jnp.float32)
-        query_index = lax.broadcasted_iota(jnp.int32, (WINDOW, 2 * WINDOW), 0)
-        key_index = lax.broadcasted_iota(jnp.int32, (WINDOW, 2 * WINDOW), 1)
-        distance = WINDOW + query_index - key_index
-        in_window = (distance >= 0) & (distance < WINDOW)
-        not_before = in_window & ((lax.axis_index("sp") > 0) | (key_index >= WINDOW))
+        shape = (WINDOW, WINDOW)
+        before = lax.broadcasted_iota(jnp.int32, shape, 1) > lax.broadcasted_iota(jnp.int32, shape, 0)
+        nothing_before = before & (lax.axis_index("sp") == 0)
         own = pl.multiple_of(lax.axis_index("tp") * channels, channels)
         tap_rows = taps_ref[:, pl.ds(own, channels)].astype(jnp.float32)
         for block in range(rows // WINDOW):
@@ -190,22 +191,26 @@
             share, inner = start // share_rows, start % share_rows
             keys = band[start : start + 2 * WINDOW, :HEAD_DIM]
             values = band[start : start + 2 * WINDOW, HEAD_DIM : 2 * HEAD_DIM]
-            allowed = not_before if block == 0 else in_window
             found = []
             for head in range(head_count):
                 source, at = (queries_ref, start) if start < rest else (last_queries, start - rest)
                 here = source[at : at + WINDOW, head * HEAD_DIM : (head + 1) * HEAD_DIM]
-                scores = lax.dot_general(
+                both = lax.dot_general(
                     here, keys, (((1,), (1,)), ((), ())), preferred_element_type=jnp.float32
-                ) * HEAD_DIM ** (-0.5)
-                scores = jnp.where(allowed, scores, MASKED_SCORE)
+                )
+                scores = jnp.where(before, both[:, :WINDOW], both[:, WINDOW:]) * HEAD_DIM ** (-0.5)
+                if block == 0:
+                    scores = jnp.where(nothing_before, MASKED_SCORE, scores)
                 sink = sinks_ref[head]
                 peak = jnp.maximum(jnp.max(scores, axis=-1, keepdims=True), sink)
                 raised = jnp.exp(scores - peak)
                 denominator = jnp.sum(raised, axis=-1, keepdims=True) + jnp.exp(sink - peak)
-                weights = (raised * (1.0 / denominator)).astype(jnp.bfloat16)
+                weights = raised * (1.0 / denominator)
+                placed = jnp.concatenate(
+                    [jnp.where(before, weights, 0.0), jnp.where(before, 0.0, weights)], axis=1
+                ).astype(jnp.bfloat16)
                 found.append(
-                    jnp.dot(weights, values, preferred_element_type=jnp.float32).astype(jnp.bfloat16)
+                    jnp.dot(placed, values, preferred_element_type=jnp.float32).astype(jnp.bfloat16)
                 )
             out_ref[share, inner : inner + WINDOW, :heads_width] = jnp.concatenate(found, axis=1)
             total = jnp.zeros((WINDOW, channels), jnp.float32)
@@ -213,17 +218,23 @@
                 from_row = start + HALO - (CONV_WIDTH - 1) + tap
                 total = total + tap_rows[tap : tap + 1] * extended[from_row : from_row + WINDOW]
             out_ref[share, inner : inner + WINDOW, heads_width:] = total.astype(jnp.bfloat16)
+            if inner + WINDOW == share_rows:
+                copies[share].start()
+        for copy in copies:
+            copy.wait()
 
     whole = pl.BlockSpec(memory_space=pltpu.VMEM)
     scalars = pl.BlockSpec(memory_space=pltpu.SMEM)
     return pl.pallas_call(
         body,
         in_specs=[scalars] + [whole] * 8,
-        out_specs=whole,
-        out_shape=jax.ShapeDtypeStruct((shares, share_rows, heads_width + channels), jnp.bfloat16),
+        out_specs=pl.BlockSpec(memory_space=pl.ANY),
+        out_shape=pltpu.HBM((shares, share_rows, heads_width + channels), jnp.bfloat16),
         scratch_shapes=[
+            pltpu.VMEM((shares, share_rows, heads_width + channels), jnp.bfloat16),
             pltpu.VMEM((WINDOW + rows, pair_width), jnp.bfloat16),
             pltpu.VMEM((HALO + rows, channels), jnp.float32),
+            pltpu.SemaphoreType.DMA((shares,)),
         ],
         compiler_params=pltpu.CompilerParams(vmem_limit_bytes=12 << 20),
         name="mix_rows",
@@ -367,43 +378,40 @@
         near_refs, far_refs, out_ref = refs[:4], refs[4:6], refs[6]
         line, side, lane = place_of_device()
 
-        def product(from_line, sides, *parts):
-            return jnp.dot(
-                columns_of(merged_ref, from_line, sides, share_rows),
-                jnp.concatenate(parts, axis=0),
-                preferred_element_type=jnp.float32,
-            )
-
         both_sides = (side, 1 - side)
-        at_end = (line == 0) | (line == lines - 1)
-        holder = jnp.where(line == 0, 0, 1)
-        for which in range(2):
-            held = holder == (lane, 1 - lane)[which]
-            for ends, ref in ((True, near_refs[which]), (False, far_refs[which])):
-
-                @pl.when(held & (at_end == ends))
+
+        def pieces_of(at_line, at_lane):
+            at_end = at_line in (0, lines - 1)
+            which_of = {at_lane: 0, 1 - at_lane: 1}
+            holder = which_of[0 if at_line == 0 else 1]
+            opposite = (near_refs if at_end else far_refs)[holder]
+            found = [(at_line, both_sides, (share_ref, opposite))]
+            for held_by, which in which_of.items():
+                beside = at_line - 1 + 2 * held_by
+                if 0 <= beside < lines:
+                    found.append((beside, both_sides, (near_refs[which], near_refs[2 + which])))
+                if held_by == 0 or at_end:
+                    two_away = at_line + 2 if at_line < 2 else at_line - 2
+                    beyond = two_away if held_by == 0 else lines - 1 - at_line
+                    found.append((beyond, (far_side(side, held_by),), (far_refs[which],)))
+            return found
+
+        for at_line in range(lines):
+            for at_lane in range(2):
+
+                @pl.when((line == at_line) & (lane == at_lane))
                 def _():
-                    out_ref[...] = product(line, both_sides, share_ref[...], ref[...])
-
-        for which in range(2):
-            at_lane = (lane, 1 - lane)[which]
-            from_line = line - 1 + 2 * at_lane
-
-            @pl.when((from_line >= 0) & (from_line < lines))
-            def _():
-                out_ref[...] += product(
-                    from_line, both_sides, near_refs[which][...], near_refs[2 + which][...]
-                )
-
-        for which in range(2):
-            at_lane = (lane, 1 - lane)[which]
-            from_line = far_line(line, at_lane, lines)
-
-            @pl.when(from_line >= 0)
-            def _():
-                out_ref[...] += product(
-                    from_line, (far_side(side, at_lane),), far_refs[which][...]
-                )
+                    found = pieces_of(at_line, at_lane)
+                    left = [
+                        columns_of(merged_ref, from_line, sides, share_rows)
+                        for from_line, sides, _ in found
+                    ]
+                    right = [ref[...] for _, _, refs_here in found for ref in refs_here]
+                    out_ref[...] = jnp.dot(
+                        jnp.concatenate(left, axis=1),
+                        jnp.concatenate(right, axis=0),
+                        preferred_element_type=jnp.float32,
+                    )
 
     vmem = pl.BlockSpec(memory_space=pltpu.VMEM)
     return pl.pallas_call(

time: 67.1 us -> 68.3 us (1.018)
  blocking collectives: 11.4 us -> 12.3 us
    all_to_all x1, blocking collectives: 11.4 us -> 12.3 us  [on_device(): lax.all_to_all(mixed, 'tp', split_axis=0, concat_axis=0, tiled=True)]
where the time goes in v6:
time: 68.3 us; the launch traced here: 67.9 us
  waiting for transfers between devices  21.5 us (31%)
  starting transfers between devices  18.7 us (27%)
  Pallas kernels  14 us (20%)
  blocking collectives  12.3 us (18%)
  other arithmetic  1.1 us (2%)
    ppermute x8, waiting for transfers between devices, send(): return lax.ppermute(block, PLACE, found)  21.5 us
    ppermute x8, starting transfers between devices, send(): return lax.ppermute(block, PLACE, found)  16.1 us
    all_to_all x1, blocking collectives, on_device(): lax.all_to_all(mixed, 'tp', split_axis=0, concat_axis=0, tiled=True)  12.3 us
    pallas_call x1, Pallas kernels, mix_rows(): pl.pallas_call(body, in_specs=[scalars] + [whole] * 8, out_specs=pl.Block...  4.47 us
    pallas_call x1, Pallas kernels, project_last(): pl.pallas_call(body, in_specs=[pl.BlockSpec(memory_space=pl.ANY)] * 7, ou...  2.95 us
    ppermute x1, starting transfers between devices, from_behind(): return lax.ppermute(block, axis, route)  2.58 us
    pallas_call x1, Pallas kernels, project_rest(): pl.pallas_call(body, in_specs=[vmem] * 3, out_specs=[vmem] * 3, out_shape...  2.37 us
    pallas_call x1, Pallas kernels, merge_mixers(): pl.pallas_call(body, in_specs=[vmem] * 3 + [pl.BlockSpec(memory_space=pl....  1.72 us
  transfers between devices with their start and end apart: 9, of which 3 were waited for; matrix products, arithmetic and copies ran while one was open for 0% of the time, Pallas kernels for 19%

profile of v6, /device:TPU:0, one launch (start us, length us, event | category | flops | bytes accessed | tf_op | source)
XLA Modules:
  0.0 67.9 jit_solution(1176657866462349534)
XLA Ops:
  0.0 3.1 %collective-permute-start.1 = (bf16[128,2048]{1,0:T(8,128)(2,1)}, bf16[128,2048]{1,0:T(8,128)(2,1)S(1)}, u32[]{:S(2)}, u32[]{:S(2)}) collective-permute-start(bf16[128,2048]{1,0:T(8,128)(2,1)} %share_ref.1), channel_id=1, source_target_pairs={{0,8},{1,4},{2,10},{3,6},{4,12},{5,0},{6,14},{7,2},{8,16},{9,1},{1... | collective-permute-start | bytes 1572872 | tf_op jit(solution)/shard_map/ppermute | solution.py:311
  3.1 7.0 %collective-permute-done.1.refs_0_ = bf16[128,2048]{1,0:T(8,128)(2,1)S(1)} collective-permute-done((bf16[128,2048]{1,0:T(8,128)(2,1)}, bf16[128,2048]{1,0:T(8,128)(2,1)S(1)}, u32[]{:S(2)}, u32[]{:S(2)}) %collective-permute-start.1) | collective-permute-done | bytes 524320 | tf_op jit(solution)/shard_map/ppermute | solution.py:311
  10.1 1.1 %broadcast_select_fusion = bf16[128,2048]{1,0:T(8,128)(2,1)S(1)} fusion(bf16[128,2048]{1,0:T(8,128)(2,1)S(1)} %collective-permute-done.1.refs_0_, bf16[128,2048]{1,0:T(8,128)(2,1)} %share_ref.1, pred[]{:T(512)S(6)} %eq.3), kind=kLoop, calls=%fused_computation | loop fusion | flops 262144 | bytes 1572865 | tf_op jit(solution)/shard_map/jit(_where)/select_n | solution.py:509
  11.2 2.4 %collective-permute-start.5 = (bf16[128,2048]{1,0:T(8,128)(2,1)S(1)}, bf16[128,2048]{1,0:T(8,128)(2,1)S(1)}, u32[]{:S(2)}, u32[]{:S(2)}) collective-permute-start(bf16[128,2048]{1,0:T(8,128)(2,1)S(1)} %broadcast_select_fusion), channel_id=1, source_target_pairs={{0,16},{1,25},{2,18},{3,31},{4,20},{5,29},{6,22},{7,27},{8,13},{9,... | collective-permute-start | bytes 1572872 | tf_op jit(solution)/shard_map/ppermute | solution.py:311
  13.6 0.7 %collective-permute-start.3 = (bf16[128,2048]{1,0:T(8,128)(2,1)S(1)}, bf16[128,2048]{1,0:T(8,128)(2,1)S(1)}, u32[]{:S(2)}, u32[]{:S(2)}) collective-permute-start(bf16[128,2048]{1,0:T(8,128)(2,1)S(1)} %collective-permute-done.1.refs_0_), channel_id=1, source_target_pairs={{1,5},{3,7},{5,1},{7,3},{8,12},{9,13},{10,14},{11,15},{12,8},{13,9... | collective-permute-start | bytes 1572872 | tf_op jit(solution)/shard_map/ppermute | solution.py:311
  14.3 11.0 %collective-permute-done.5.refs_4_ = bf16[128,2048]{1,0:T(8,128)(2,1)S(1)} collective-permute-done((bf16[128,2048]{1,0:T(8,128)(2,1)S(1)}, bf16[128,2048]{1,0:T(8,128)(2,1)S(1)}, u32[]{:S(2)}, u32[]{:S(2)}) %collective-permute-start.5) | collective-permute-done | bytes 524320 | tf_op jit(solution)/shard_map/ppermute | solution.py:311
  25.2 3.4 %collective-permute-start.7 = (bf16[128,2048]{1,0:T(8,128)(2,1)S(1)}, bf16[128,2048]{1,0:T(8,128)(2,1)S(1)}, u32[]{:S(2)}, u32[]{:S(2)}) collective-permute-start(bf16[128,2048]{1,0:T(8,128)(2,1)S(1)} %collective-permute-done.5.refs_4_), channel_id=1, source_target_pairs={{0,4},{1,3},{2,6},{3,1},{4,0},{5,7},{6,2},{7,5},{8,12},{10,14},{12... | collective-permute-start | bytes 1572872 | tf_op jit(solution)/shard_map/ppermute | solution.py:311
  28.7 3.6 %collective-permute-start.2 = (bf16[128,2048]{1,0:T(8,128)(2,1)S(1)}, bf16[128,2048]{1,0:T(8,128)(2,1)S(1)}, u32[]{:S(2)}, u32[]{:S(2)}) collective-permute-start(bf16[128,2048]{1,0:T(8,128)(2,1)S(1)} %collective-permute-done.1.refs_0_), channel_id=1, source_target_pairs={{0,1},{1,0},{2,3},{3,2},{4,5},{5,4},{6,7},{7,6},{8,9},{9,8},{10,11... | collective-permute-start | bytes 1572872 | tf_op jit(solution)/shard_map/ppermute | solution.py:311
  32.2 0.1 collective-permute-start.6
  32.3 0.4 collective-permute-start.4
  32.7 3.5 %collective-permute-done.7.refs_0_ = bf16[128,2048]{1,0:T(8,128)(2,1)S(1)} collective-permute-done((bf16[128,2048]{1,0:T(8,128)(2,1)S(1)}, bf16[128,2048]{1,0:T(8,128)(2,1)S(1)}, u32[]{:S(2)}, u32[]{:S(2)}) %collective-permute-start.7) | collective-permute-done | bytes 524320 | tf_op jit(solution)/shard_map/ppermute | solution.py:311
  36.3 2.4 %collective-permute-start.8 = (bf16[128,2048]{1,0:T(8,128)(2,1)S(1)}, bf16[128,2048]{1,0:T(8,128)(2,1)S(1)}, u32[]{:S(2)}, u32[]{:S(2)}) collective-permute-start(bf16[128,2048]{1,0:T(8,128)(2,1)S(1)} %collective-permute-done.7.refs_0_), channel_id=1, source_target_pairs={{0,1},{1,0},{2,3},{3,2},{4,5},{5,4},{6,7},{7,6},{8,9},{9,8},{10,11... | collective-permute-start | bytes 1572872 | tf_op jit(solution)/shard_map/ppermute | solution.py:311
  38.7 2.9 %project_last.1 = (bf16[256,128]{1,0:T(8,128)(2,1)S(1)}, bf16[256,128]{1,0:T(8,128)(2,1)S(1)}, bf16[256,128]{1,0:T(8,128)(2,1)S(1)}, bf16[160,128]{1,0:T(8,128)(...) custom-call(f32[1,2048]{1,0:T(1,128)} %bitcast.5, bf16[1024,2048]{1,0:T(8,128)(2,1)} %tokens_hbm.1, ...), custom_call_target="tpu_custom_call" | custom-call | tf_op jit(solution)/shard_map/project_last/pallas_call | solution.py:109
  41.7 0.0 copy-start.2
  41.7 0.0 copy-start.5
  41.7 2.6 %collective-permute-start = (bf16[160,128]{1,0:T(8,128)(2,1)S(1)}, bf16[160,128]{1,0:T(8,128)(2,1)S(1)}, u32[]{:S(2)}, u32[]{:S(2)}) collective-permute-start(bf16[160,128]{1,0:T(8,128)(2,1)S(1)} %get-tuple-element.25), channel_id=1, source_target_pairs={{0,4},{4,8},{8,12},{12,16},{16,20},{20,24},{24,28},{1,5},{5,9},{9,... | collective-permute-start | bytes 122888 | tf_op jit(solution)/shard_map/ppermute | solution.py:25
  44.3 0.0 copy-start.3
  44.3 0.0 copy-start.4
  44.3 2.4 %project_rest.1 = (bf16[768,128]{1,0:T(8,128)(2,1)S(1)}, bf16[768,128]{1,0:T(8,128)(2,1)S(1)}, bf16[768,128]{1,0:T(8,128)(2,1)S(1)}) custom-call(f32[1,2048]{1,0:T(1,128)S(1)} %bitcast.6, bf16[768,2048]{1,0:T(8,128)(2,1)S(1)} %get-tuple-element.17.tokens_ref, bf16[2048,512]{1,0:T(8,128)(2,1)S(1)} %get-tuple-element.18.joined_ref), custom_call_target="tpu_custom_call" | custom-call | tf_op jit(solution)/shard_map/project_rest/pallas_call | solution.py:146
  46.7 4.5 %mix_rows.1 = bf16[4,256,256]{2,1,0:T(8,128)(2,1)} custom-call(f32[2]{0:T(128)S(1)} %copy-done.5, bf16[768,128]{1,0:T(8,128)(2,1)S(1)} %get-tuple-element.19.queries_ref, bf16[768,128]{1,0:T(8,128)(2,1)S(1)} %get-tuple-element.20.pairs_ref, bf16[768,128]{1,0:T(8,128)(2,1)S(1)} %get-tuple-element.21.gated_ref, ...), custom_call_target="tpu_custom_call" | custom-call | tf_op jit(solution)/shard_map/mix_rows/pallas_call | solution.py:228
  51.2 12.3 %all_to_all.5.exchanged_ref = bf16[4,256,256]{2,1,0:T(8,128)(2,1)S(1)} all-to-all(bf16[4,256,256]{2,1,0:T(8,128)(2,1)} %mix_rows.1), channel_id=1, replica_groups=mesh['sp'=8,'tp'=4] {'tp'}, dimensions={0} | all-to-all | bytes 1048576 | tf_op jit(solution)/shard_map/all_to_all | solution.py:518
  63.5 1.7 %merge_mixers.1.merged_ref = bf16[256,1024]{1,0:T(8,128)(2,1)S(1)} custom-call(bf16[4,256,256]{2,1,0:T(8,128)(2,1)S(1)} %all_to_all.5.exchanged_ref, f32[1,512]{1,0:T(1,128)S(1)} %bitcast.8, f32[1,1024]{1,0:T(1,128)S(1)} %bitcast.7, bf16[512,512]{1,0:T(8,128)(2,1)} %point_hbm.1), custom_call_target="tpu_custom_call" | custom-call | tf_op jit(solution)/shard_map/merge_mixers/pallas_call | solution.py:279
  65.3 1.2 %early_product.1.early_ref = f32[256,2048]{1,0:T(8,128)S(1)} custom-call(bf16[256,1024]{1,0:T(8,128)(2,1)S(1)} %merge_mixers.1.merged_ref, bf16[128,2048]{1,0:T(8,128)(2,1)S(1)} %copy-done, bf16[128,2048]{1,0:T(8,128)(2,1)S(1)} %collective-permute-done.1.refs_0_, bf16[128,2048]{1,0:T(8,128)(2,1)S(1)} %collective-permute-done.2.refs_1_, ...), custom_call_target="tpu_custom_call" | custom-call | tf_op jit(solution)/shard_map/early_product/pallas_call | solution.py:417
  66.5 1.3 %late_product.1 = bf16[256,2048]{1,0:T(8,128)(2,1)} custom-call(bf16[256,1024]{1,0:T(8,128)(2,1)S(1)} %merge_mixers.1.merged_ref, f32[256,2048]{1,0:T(8,128)S(1)} %early_product.1.early_ref, bf16[128,2048]{1,0:T(8,128)(2,1)S(1)} %collective-permute-done.7.refs_0_, bf16[128,2048]{1,0:T(8,128)(2,1)S(1)} %collective-permute-done.8.refs_1_), custom_call_target="tpu_custom_call" | custom-call | tf_op jit(solution)/shard_map/late_product/pallas_call | solution.py:472
  (14 shorter events, 0.0 us)
Async XLA Ops:
  0.0 10.1 %collective-permute-start.1 = (bf16[128,2048]{1,0:T(8,128)(2,1)}, bf16[128,2048]{1,0:T(8,128)(2,1)S(1)}, u32[]{:S(2)}, u32[]{:S(2)}) collective-permute-start(bf16[128,2048]{1,0:T(8,128)(2,1)} %share_ref.1), channel_id=1, source_target_pairs={{0,8},{1,4},{2,10},{3,6},{4,12},{5,0},{6,14},{7,2},{8,16},{9,1},{1... | collective-permute-start | bytes 1572872 | tf_op jit(solution)/shard_map/ppermute | solution.py:311
  11.2 14.1 %collective-permute-start.5 = (bf16[128,2048]{1,0:T(8,128)(2,1)S(1)}, bf16[128,2048]{1,0:T(8,128)(2,1)S(1)}, u32[]{:S(2)}, u32[]{:S(2)}) collective-permute-start(bf16[128,2048]{1,0:T(8,128)(2,1)S(1)} %broadcast_select_fusion), channel_id=1, source_target_pairs={{0,16},{1,25},{2,18},{3,31},{4,20},{5,29},{6,22},{7,27},{8,13},{9,... | collective-permute-start | bytes 1572872 | tf_op jit(solution)/shard_map/ppermute | solution.py:311
  13.6 18.7 %collective-permute-start.3 = (bf16[128,2048]{1,0:T(8,128)(2,1)S(1)}, bf16[128,2048]{1,0:T(8,128)(2,1)S(1)}, u32[]{:S(2)}, u32[]{:S(2)}) collective-permute-start(bf16[128,2048]{1,0:T(8,128)(2,1)S(1)} %collective-permute-done.1.refs_0_), channel_id=1, source_target_pairs={{1,5},{3,7},{5,1},{7,3},{8,12},{9,13},{10,14},{11,15},{12,8},{13,9... | collective-permute-start | bytes 1572872 | tf_op jit(solution)/shard_map/ppermute | solution.py:311
  25.2 11.1 %collective-permute-start.7 = (bf16[128,2048]{1,0:T(8,128)(2,1)S(1)}, bf16[128,2048]{1,0:T(8,128)(2,1)S(1)}, u32[]{:S(2)}, u32[]{:S(2)}) collective-permute-start(bf16[128,2048]{1,0:T(8,128)(2,1)S(1)} %collective-permute-done.5.refs_4_), channel_id=1, source_target_pairs={{0,4},{1,3},{2,6},{3,1},{4,0},{5,7},{6,2},{7,5},{8,12},{10,14},{12... | collective-permute-start | bytes 1572872 | tf_op jit(solution)/shard_map/ppermute | solution.py:311
  28.7 36.6 %collective-permute-start.2 = (bf16[128,2048]{1,0:T(8,128)(2,1)S(1)}, bf16[128,2048]{1,0:T(8,128)(2,1)S(1)}, u32[]{:S(2)}, u32[]{:S(2)}) collective-permute-start(bf16[128,2048]{1,0:T(8,128)(2,1)S(1)} %collective-permute-done.1.refs_0_), channel_id=1, source_target_pairs={{0,1},{1,0},{2,3},{3,2},{4,5},{5,4},{6,7},{7,6},{8,9},{9,8},{10,11... | collective-permute-start | bytes 1572872 | tf_op jit(solution)/shard_map/ppermute | solution.py:311
  32.2 33.0 %collective-permute-start.6 = (bf16[128,2048]{1,0:T(8,128)(2,1)S(1)}, bf16[128,2048]{1,0:T(8,128)(2,1)S(1)}, u32[]{:S(2)}, u32[]{:S(2)}) collective-permute-start(bf16[128,2048]{1,0:T(8,128)(2,1)S(1)} %collective-permute-done.5.refs_4_), channel_id=1, source_target_pairs={{0,1},{1,0},{2,3},{3,2},{4,5},{5,4},{6,7},{7,6},{8,9},{9,8},{10,11... | collective-permute-start | bytes 1572872 | tf_op jit(solution)/shard_map/ppermute | solution.py:311
  32.3 32.9 %collective-permute-start.4 = (bf16[128,2048]{1,0:T(8,128)(2,1)S(1)}, bf16[128,2048]{1,0:T(8,128)(2,1)S(1)}, u32[]{:S(2)}, u32[]{:S(2)}) collective-permute-start(bf16[128,2048]{1,0:T(8,128)(2,1)S(1)} %collective-permute-done.3.refs_2_), channel_id=1, source_target_pairs={{0,1},{1,0},{2,3},{3,2},{4,5},{5,4},{6,7},{7,6},{8,9},{9,8},{10,11... | collective-permute-start | bytes 1572872 | tf_op jit(solution)/shard_map/ppermute | solution.py:311
  36.3 30.2 %collective-permute-start.8 = (bf16[128,2048]{1,0:T(8,128)(2,1)S(1)}, bf16[128,2048]{1,0:T(8,128)(2,1)S(1)}, u32[]{:S(2)}, u32[]{:S(2)}) collective-permute-start(bf16[128,2048]{1,0:T(8,128)(2,1)S(1)} %collective-permute-done.7.refs_0_), channel_id=1, source_target_pairs={{0,1},{1,0},{2,3},{3,2},{4,5},{5,4},{6,7},{7,6},{8,9},{9,8},{10,11... | collective-permute-start | bytes 1572872 | tf_op jit(solution)/shard_map/ppermute | solution.py:311
  38.7 5.6 %copy-start.1 = (f32[2048]{0:T(1024)S(1)}, f32[2048]{0:T(1024)}, u32[]{:S(2)}) copy-start(f32[2048]{0:T(1024)} %param.14) | copy-start | bytes 24580
  41.7 5.0 %copy-start.2 = (bf16[31,512]{1,0:T(8,128)(2,1)S(1)}, bf16[31,512]{1,0:T(8,128)(2,1)}, u32[]{:S(2)}) copy-start(bf16[31,512]{1,0:T(8,128)(2,1)} %taps_ref.1) | copy-start | bytes 95236
  41.7 5.0 %copy-start.5 = (f32[2]{0:T(128)S(1)}, f32[2]{0:T(128)}, u32[]{:S(2)}) copy-start(f32[2]{0:T(128)} %sinks_ref.1) | copy-start | bytes 28
  41.7 5.0 %collective-permute-start = (bf16[160,128]{1,0:T(8,128)(2,1)S(1)}, bf16[160,128]{1,0:T(8,128)(2,1)S(1)}, u32[]{:S(2)}, u32[]{:S(2)}) collective-permute-start(bf16[160,128]{1,0:T(8,128)(2,1)S(1)} %get-tuple-element.25), channel_id=1, source_target_pairs={{0,4},{4,8},{8,12},{12,16},{16,20},{20,24},{24,28},{1,5},{5,9},{9,... | collective-permute-start | bytes 122888 | tf_op jit(solution)/shard_map/ppermute | solution.py:25
  44.3 19.2 %copy-start.3 = (f32[1024]{0:T(1024)S(1)}, f32[1024]{0:T(1024)}, u32[]{:S(2)}) copy-start(f32[1024]{0:T(1024)} %param.24) | copy-start | bytes 12292
  44.3 19.2 %copy-start.4 = (f32[512]{0:T(512)S(1)}, f32[512]{0:T(512)}, u32[]{:S(2)}) copy-start(f32[512]{0:T(512)} %param.22) | copy-start | bytes 6148
  46.7 18.6 %copy-start = (bf16[128,2048]{1,0:T(8,128)(2,1)S(1)}, bf16[128,2048]{1,0:T(8,128)(2,1)}, u32[]{:S(2)}) copy-start(bf16[128,2048]{1,0:T(8,128)(2,1)} %share_ref.1) | copy-start | bytes 1572868

commit v7 on v6

--- a/solution.py
+++ b/solution.py
@@ -241,14 +241,29 @@
     )(sinks, *first_rows, *last_rows, earlier, taps)
 
 
+def fetched(weight):
+    def body(weight_hbm, out_ref, moved):
+        copy = pltpu.make_async_copy(weight_hbm, out_ref, moved)
+        copy.start()
+        copy.wait()
+
+    return pl.pallas_call(
+        body,
+        in_specs=[pl.BlockSpec(memory_space=pl.ANY)],
+        out_specs=pl.BlockSpec(memory_space=pltpu.VMEM),
+        out_shape=jax.ShapeDtypeStruct(weight.shape, weight.dtype),
+        scratch_shapes=[pltpu.SemaphoreType.DMA(())],
+        compiler_params=pltpu.CompilerParams(vmem_limit_bytes=4 << 20),
+        name="fetched",
+    )(pltpu.with_memory_space_constraint(weight, pltpu.HBM))
+
+
 def merge_mixers(exchanged, conv_gain, point_weight, output_gain):
     shares, rows, joint = exchanged.shape
     heads_width = joint // 2
     width = shares * heads_width
 
-    def body(exchanged_ref, conv_gain_ref, gain_ref, point_hbm, out_ref, point_ref, fetched):
-        fetch = pltpu.make_async_copy(point_hbm, point_ref, fetched)
-        fetch.start()
+    def body(exchanged_ref, conv_gain_ref, gain_ref, point_ref, out_ref):
         attended = jnp.concatenate(
             [exchanged_ref[i, :, :heads_width] for i in range(shares)], axis=1
         ).astype(jnp.float32)
@@ -267,7 +282,6 @@
             * lax.rsqrt(jnp.mean(attended * attended, axis=-1, keepdims=True) + NORM_EPSILON)
             * gain_ref[:, :width]
         ).astype(jnp.bfloat16)
-        fetch.wait()
         pointwise = jnp.dot(activated, point_ref[...], preferred_element_type=jnp.float32)
         out_ref[:, width:] = (
             pointwise
@@ -278,19 +292,12 @@
     vmem = pl.BlockSpec(memory_space=pltpu.VMEM)
     return pl.pallas_call(
         body,
-        in_specs=[vmem] * 3 + [pl.BlockSpec(memory_space=pl.ANY)],
+        in_specs=[vmem] * 4,
         out_specs=vmem,
         out_shape=jax.ShapeDtypeStruct((rows, output_gain.shape[0]), jnp.bfloat16),
-        scratch_shapes=[
-            pltpu.VMEM(point_weight.shape, point_weight.dtype),
-            pltpu.SemaphoreType.DMA(()),
-        ],
         compiler_params=pltpu.CompilerParams(vmem_limit_bytes=12 << 20),
         name="merge_mixers",
-    )(
-        exchanged, conv_gain[None], output_gain[None],
-        pltpu.with_memory_space_constraint(point_weight, pltpu.HBM),
-    )
+    )(exchanged, conv_gain[None], output_gain[None], point_weight)
 
 
 class ShareRoutes:
@@ -516,7 +523,8 @@
     first_rows = project_rest(other_tokens, norm_gain, joined, query_weight.shape[1], pair_width)
     mixed = mix_rows(first_rows, last_rows, earlier, sink_logits, conv_taps, tp_size)
     exchanged = lax.all_to_all(mixed, "tp", split_axis=0, concat_axis=0, tiled=True)
-    merged = merge_mixers(exchanged, conv_gain, point_weight, output_gain)
+    point_here = fetched(point_weight)
+    merged = merge_mixers(exchanged, conv_gain, point_here, output_gain)
     if by_shares:
         near_across = routes.send(near, routes.holders_across)
         far_other = routes.send(far, routes.to_neighbours)

time: 68.3 us -> 69.9 us (1.023)
  blocking collectives: 12.3 us -> 0 us
  waiting for transfers between devices: 21.5 us -> 29.4 us
  starting transfers between devices: 18.7 us -> 22.1 us
  Pallas kernels: 14 us -> 16.5 us
    all_to_all x1 -> x0, blocking collectives: 12.3 us -> none  [on_device(): lax.all_to_all(mixed, 'tp', split_axis=0, concat_axis=0, tiled=True)]
    all_to_all x0 -> x1, waiting for transfers between devices: none -> 7.72 us  [on_device(): lax.all_to_all(mixed, 'tp', split_axis=0, concat_axis=0, tiled=True)]
    all_to_all x0 -> x1, starting transfers between devices: none -> 3.48 us  [on_device(): lax.all_to_all(mixed, 'tp', split_axis=0, concat_axis=0, tiled=True)]
    pallas_call x1, Pallas kernels: 1.21 us -> 2.56 us  [early_product(): pl.pallas_call(body, in_specs=[vmem] * 8, out_specs=vmem, out_shape=jax.S...]
    pallas_call x1, Pallas kernels: 1.27 us -> 2.44 us  [late_product(): pl.pallas_call(body, in_specs=[vmem] * 4, out_specs=pl.BlockSpec(memory_s...]
    pallas_call x1 -> x2, Pallas kernels: 1.72 us -> 1.67 us  [the longest x1 1.05 us: fetched(): pl.pallas_call(body, in_specs=[pl.BlockSpec(memory_space=pl.ANY)], out_sp...]
  transfers between devices with their start and end apart: 9 -> 10, of which waited for: 3 -> 4; matrix products, arithmetic and copies ran while one was open for 0% -> 0% of each run, Pallas kernels for 19% -> 20%
where the time goes in v7:
time: 69.9 us; the launch traced here: 69.5 us
  waiting for transfers between devices  29.4 us (42%)
  starting transfers between devices  22.1 us (32%)
  Pallas kernels  16.5 us (24%)
  other arithmetic  1.1 us (2%)
    ppermute x8, waiting for transfers between devices, send(): return lax.ppermute(block, PLACE, found)  21.6 us
    ppermute x8, starting transfers between devices, send(): return lax.ppermute(block, PLACE, found)  16.1 us
    all_to_all x1, waiting for transfers between devices, on_device(): lax.all_to_all(mixed, 'tp', split_axis=0, concat_axis=0, tiled=True)  7.72 us
    pallas_call x1, Pallas kernels, mix_rows(): pl.pallas_call(body, in_specs=[scalars] + [whole] * 8, out_specs=pl.Block...  4.48 us
    all_to_all x1, starting transfers between devices, on_device(): lax.all_to_all(mixed, 'tp', split_axis=0, concat_axis=0, tiled=True)  3.48 us
    pallas_call x1, Pallas kernels, project_last(): pl.pallas_call(body, in_specs=[pl.BlockSpec(memory_space=pl.ANY)] * 7, ou...  2.95 us
    ppermute x1, starting transfers between devices, from_behind(): return lax.ppermute(block, axis, route)  2.58 us
    pallas_call x1, Pallas kernels, early_product(): pl.pallas_call(body, in_specs=[vmem] * 8, out_specs=vmem, out_shape=jax.S...  2.56 us
  transfers between devices with their start and end apart: 10, of which 4 were waited for; matrix products, arithmetic and copies ran while one was open for 0% of the time, Pallas kernels for 20%

profile of v7, /device:TPU:0, one launch (start us, length us, event | category | flops | bytes accessed | tf_op | source)
XLA Modules:
  0.0 69.5 jit_solution(10101005657131805396)
XLA Ops:
  0.0 3.1 %collective-permute-start.1 = (bf16[128,2048]{1,0:T(8,128)(2,1)}, bf16[128,2048]{1,0:T(8,128)(2,1)S(1)}, u32[]{:S(2)}, u32[]{:S(2)}) collective-permute-start(bf16[128,2048]{1,0:T(8,128)(2,1)} %share_ref.1), channel_id=1, source_target_pairs={{0,8},{1,4},{2,10},{3,6},{4,12},{5,0},{6,14},{7,2},{8,16},{9,1},{1... | collective-permute-start | bytes 1572872 | tf_op jit(solution)/shard_map/ppermute | solution.py:318
  3.1 7.0 %collective-permute-done.1.refs_0_ = bf16[128,2048]{1,0:T(8,128)(2,1)S(1)} collective-permute-done((bf16[128,2048]{1,0:T(8,128)(2,1)}, bf16[128,2048]{1,0:T(8,128)(2,1)S(1)}, u32[]{:S(2)}, u32[]{:S(2)}) %collective-permute-start.1) | collective-permute-done | bytes 524320 | tf_op jit(solution)/shard_map/ppermute | solution.py:318
  10.1 1.1 %broadcast_select_fusion = bf16[128,2048]{1,0:T(8,128)(2,1)S(1)} fusion(bf16[128,2048]{1,0:T(8,128)(2,1)S(1)} %collective-permute-done.1.refs_0_, bf16[128,2048]{1,0:T(8,128)(2,1)} %share_ref.1, pred[]{:T(512)S(6)} %eq.3), kind=kLoop, calls=%fused_computation | loop fusion | flops 262144 | bytes 1572865 | tf_op jit(solution)/shard_map/jit(_where)/select_n | solution.py:516
  11.2 2.4 %collective-permute-start.5 = (bf16[128,2048]{1,0:T(8,128)(2,1)S(1)}, bf16[128,2048]{1,0:T(8,128)(2,1)S(1)}, u32[]{:S(2)}, u32[]{:S(2)}) collective-permute-start(bf16[128,2048]{1,0:T(8,128)(2,1)S(1)} %broadcast_select_fusion), channel_id=1, source_target_pairs={{0,16},{1,25},{2,18},{3,31},{4,20},{5,29},{6,22},{7,27},{8,13},{9,... | collective-permute-start | bytes 1572872 | tf_op jit(solution)/shard_map/ppermute | solution.py:318
  13.6 0.7 collective-permute-start.3
  14.3 11.0 %collective-permute-done.5.refs_4_ = bf16[128,2048]{1,0:T(8,128)(2,1)S(1)} collective-permute-done((bf16[128,2048]{1,0:T(8,128)(2,1)S(1)}, bf16[128,2048]{1,0:T(8,128)(2,1)S(1)}, u32[]{:S(2)}, u32[]{:S(2)}) %collective-permute-start.5) | collective-permute-done | bytes 524320 | tf_op jit(solution)/shard_map/ppermute | solution.py:318
  25.2 3.4 %collective-permute-start.7 = (bf16[128,2048]{1,0:T(8,128)(2,1)S(1)}, bf16[128,2048]{1,0:T(8,128)(2,1)}, u32[]{:S(2)}, u32[]{:S(2)}) collective-permute-start(bf16[128,2048]{1,0:T(8,128)(2,1)S(1)} %collective-permute-done.5.refs_4_), channel_id=1, source_target_pairs={{0,4},{1,3},{2,6},{3,1},{4,0},{5,7},{6,2},{7,5},{8,12},{10,14},{12... | collective-permute-start | bytes 1572872 | tf_op jit(solution)/shard_map/ppermute | solution.py:318
  28.7 3.6 %collective-permute-start.2 = (bf16[128,2048]{1,0:T(8,128)(2,1)S(1)}, bf16[128,2048]{1,0:T(8,128)(2,1)}, u32[]{:S(2)}, u32[]{:S(2)}) collective-permute-start(bf16[128,2048]{1,0:T(8,128)(2,1)S(1)} %collective-permute-done.1.refs_0_), channel_id=1, source_target_pairs={{0,1},{1,0},{2,3},{3,2},{4,5},{5,4},{6,7},{7,6},{8,9},{9,8},{10,11... | collective-permute-start | bytes 1572872 | tf_op jit(solution)/shard_map/ppermute | solution.py:318
  32.2 0.1 collective-permute-start.6
  32.3 0.4 collective-permute-start.4
  32.7 3.7 %collective-permute-done.7.refs_0_ = bf16[128,2048]{1,0:T(8,128)(2,1)} collective-permute-done((bf16[128,2048]{1,0:T(8,128)(2,1)S(1)}, bf16[128,2048]{1,0:T(8,128)(2,1)}, u32[]{:S(2)}, u32[]{:S(2)}) %collective-permute-start.7) | collective-permute-done | bytes 524320 | tf_op jit(solution)/shard_map/ppermute | solution.py:318
  36.4 2.4 %collective-permute-start.8 = (bf16[128,2048]{1,0:T(8,128)(2,1)}, bf16[128,2048]{1,0:T(8,128)(2,1)}, u32[]{:S(2)}, u32[]{:S(2)}) collective-permute-start(bf16[128,2048]{1,0:T(8,128)(2,1)} %collective-permute-done.7.refs_0_), channel_id=1, source_target_pairs={{0,1},{1,0},{2,3},{3,2},{4,5},{5,4},{6,7},{7,6},{8,9},{9,8},{10,11... | collective-permute-start | bytes 1572872 | tf_op jit(solution)/shard_map/ppermute | solution.py:318
  38.8 2.9 %project_last.1 = (bf16[256,128]{1,0:T(8,128)(2,1)S(1)}, bf16[256,128]{1,0:T(8,128)(2,1)S(1)}, bf16[256,128]{1,0:T(8,128)(2,1)S(1)}, bf16[160,128]{1,0:T(8,128)(...) custom-call(f32[1,2048]{1,0:T(1,128)} %bitcast.5, bf16[1024,2048]{1,0:T(8,128)(2,1)} %tokens_hbm.1, ...), custom_call_target="tpu_custom_call" | custom-call | tf_op jit(solution)/shard_map/project_last/pallas_call | solution.py:109
  41.8 0.0 copy-start.5
  41.8 2.6 %collective-permute-start = (bf16[160,128]{1,0:T(8,128)(2,1)S(1)}, bf16[160,128]{1,0:T(8,128)(2,1)S(1)}, u32[]{:S(2)}, u32[]{:S(2)}) collective-permute-start(bf16[160,128]{1,0:T(8,128)(2,1)S(1)} %get-tuple-element.25), channel_id=1, source_target_pairs={{0,4},{4,8},{8,12},{12,16},{16,20},{20,24},{24,28},{1,5},{5,9},{9,... | collective-permute-start | bytes 122888 | tf_op jit(solution)/shard_map/ppermute | solution.py:25
  44.4 2.4 %project_rest.1 = (bf16[768,128]{1,0:T(8,128)(2,1)S(1)}, bf16[768,128]{1,0:T(8,128)(2,1)S(1)}, bf16[768,128]{1,0:T(8,128)(2,1)S(1)}) custom-call(f32[1,2048]{1,0:T(1,128)S(1)} %bitcast.6, bf16[768,2048]{1,0:T(8,128)(2,1)S(1)} %get-tuple-element.17.tokens_ref, bf16[2048,512]{1,0:T(8,128)(2,1)S(1)} %get-tuple-element.18.joined_ref), custom_call_target="tpu_custom_call" | custom-call | tf_op jit(solution)/shard_map/project_rest/pallas_call | solution.py:146
  46.9 0.0 copy-start
  46.9 4.5 %mix_rows.1 = bf16[4,256,256]{2,1,0:T(8,128)(2,1)} custom-call(f32[2]{0:T(128)S(1)} %copy-done.5, bf16[768,128]{1,0:T(8,128)(2,1)S(1)} %get-tuple-element.19.queries_ref, bf16[768,128]{1,0:T(8,128)(2,1)S(1)} %get-tuple-element.20.pairs_ref, bf16[768,128]{1,0:T(8,128)(2,1)S(1)} %get-tuple-element.21.gated_ref, ...), custom_call_target="tpu_custom_call" | custom-call | tf_op jit(solution)/shard_map/mix_rows/pallas_call | solution.py:228
  51.4 3.5 %all-to-all-start = ((bf16[4,256,256]{2,1,0:T(8,128)(2,1)}), bf16[4,256,256]{2,1,0:T(8,128)(2,1)S(1)}, u32[]{:S(2)}, u32[]{:S(2)}) async-start(bf16[4,256,256]{2,1,0:T(8,128)(2,1)} %mix_rows.1), calls=%async_computation | async-start | bytes 1048576 | tf_op jit(solution)/shard_map/all_to_all | solution.py:525
  54.9 1.1 %fetched.1.point_ref = bf16[512,512]{1,0:T(8,128)(2,1)S(1)} custom-call(bf16[512,512]{1,0:T(8,128)(2,1)} %weight_hbm.1), custom_call_target="tpu_custom_call" | custom-call | tf_op jit(solution)/shard_map/fetched/pallas_call | solution.py:250
  55.9 7.7 %all-to-all-done.exchanged_ref = bf16[4,256,256]{2,1,0:T(8,128)(2,1)S(1)} async-done(((bf16[4,256,256]{2,1,0:T(8,128)(2,1)}), bf16[4,256,256]{2,1,0:T(8,128)(2,1)S(1)}, u32[]{:S(2)}, u32[]{:S(2)}) %all-to-all-start) | async-done | bytes 524320 | tf_op jit(solution)/shard_map/all_to_all | solution.py:525
  63.7 0.6 merge_mixers.1.merged_ref
  64.3 2.6 %early_product.1.early_ref = f32[256,2048]{1,0:T(8,128)S(1)} custom-call(bf16[256,1024]{1,0:T(8,128)(2,1)S(1)} %merge_mixers.1.merged_ref, bf16[128,2048]{1,0:T(8,128)(2,1)S(1)} %copy-done, bf16[128,2048]{1,0:T(8,128)(2,1)S(1)} %collective-permute-done.1.refs_0_, bf16[128,2048]{1,0:T(8,128)(2,1)} %collective-permute-done.2.refs_1_, ...), custom_call_target="tpu_custom_call" | custom-call | tf_op jit(solution)/shard_map/early_product/pallas_call | solution.py:424
  66.9 2.4 %late_product.1 = bf16[256,2048]{1,0:T(8,128)(2,1)} custom-call(bf16[256,1024]{1,0:T(8,128)(2,1)S(1)} %merge_mixers.1.merged_ref, f32[256,2048]{1,0:T(8,128)S(1)} %early_product.1.early_ref, bf16[128,2048]{1,0:T(8,128)(2,1)} %collective-permute-done.7.refs_0_, bf16[128,2048]{1,0:T(8,128)(2,1)} %collective-permute-done.8.refs_1_), custom_call_target="tpu_custom_call" | custom-call | tf_op jit(solution)/shard_map/late_product/pallas_call | solution.py:479
  (16 shorter events, 0.0 us)
Async XLA Ops:
  0.0 10.1 %collective-permute-start.1 = (bf16[128,2048]{1,0:T(8,128)(2,1)}, bf16[128,2048]{1,0:T(8,128)(2,1)S(1)}, u32[]{:S(2)}, u32[]{:S(2)}) collective-permute-start(bf16[128,2048]{1,0:T(8,128)(2,1)} %share_ref.1), channel_id=1, source_target_pairs={{0,8},{1,4},{2,10},{3,6},{4,12},{5,0},{6,14},{7,2},{8,16},{9,1},{1... | collective-permute-start | bytes 1572872 | tf_op jit(solution)/shard_map/ppermute | solution.py:318
  11.2 14.1 %collective-permute-start.5 = (bf16[128,2048]{1,0:T(8,128)(2,1)S(1)}, bf16[128,2048]{1,0:T(8,128)(2,1)S(1)}, u32[]{:S(2)}, u32[]{:S(2)}) collective-permute-start(bf16[128,2048]{1,0:T(8,128)(2,1)S(1)} %broadcast_select_fusion), channel_id=1, source_target_pairs={{0,16},{1,25},{2,18},{3,31},{4,20},{5,29},{6,22},{7,27},{8,13},{9,... | collective-permute-start | bytes 1572872 | tf_op jit(solution)/shard_map/ppermute | solution.py:318
  13.6 18.7 %collective-permute-start.3 = (bf16[128,2048]{1,0:T(8,128)(2,1)S(1)}, bf16[128,2048]{1,0:T(8,128)(2,1)S(1)}, u32[]{:S(2)}, u32[]{:S(2)}) collective-permute-start(bf16[128,2048]{1,0:T(8,128)(2,1)S(1)} %collective-permute-done.1.refs_0_), channel_id=1, source_target_pairs={{1,5},{3,7},{5,1},{7,3},{8,12},{9,13},{10,14},{11,15},{12,8},{13,9... | collective-permute-start | bytes 1572872 | tf_op jit(solution)/shard_map/ppermute | solution.py:318
  25.2 11.2 %collective-permute-start.7 = (bf16[128,2048]{1,0:T(8,128)(2,1)S(1)}, bf16[128,2048]{1,0:T(8,128)(2,1)}, u32[]{:S(2)}, u32[]{:S(2)}) collective-permute-start(bf16[128,2048]{1,0:T(8,128)(2,1)S(1)} %collective-permute-done.5.refs_4_), channel_id=1, source_target_pairs={{0,4},{1,3},{2,6},{3,1},{4,0},{5,7},{6,2},{7,5},{8,12},{10,14},{12... | collective-permute-start | bytes 1572872 | tf_op jit(solution)/shard_map/ppermute | solution.py:318
  28.7 35.6 %collective-permute-start.2 = (bf16[128,2048]{1,0:T(8,128)(2,1)S(1)}, bf16[128,2048]{1,0:T(8,128)(2,1)}, u32[]{:S(2)}, u32[]{:S(2)}) collective-permute-start(bf16[128,2048]{1,0:T(8,128)(2,1)S(1)} %collective-permute-done.1.refs_0_), channel_id=1, source_target_pairs={{0,1},{1,0},{2,3},{3,2},{4,5},{5,4},{6,7},{7,6},{8,9},{9,8},{10,11... | collective-permute-start | bytes 1572872 | tf_op jit(solution)/shard_map/ppermute | solution.py:318
  32.2 32.1 %collective-permute-start.6 = (bf16[128,2048]{1,0:T(8,128)(2,1)S(1)}, bf16[128,2048]{1,0:T(8,128)(2,1)}, u32[]{:S(2)}, u32[]{:S(2)}) collective-permute-start(bf16[128,2048]{1,0:T(8,128)(2,1)S(1)} %collective-permute-done.5.refs_4_), channel_id=1, source_target_pairs={{0,1},{1,0},{2,3},{3,2},{4,5},{5,4},{6,7},{7,6},{8,9},{9,8},{10,11... | collective-permute-start | bytes 1572872 | tf_op jit(solution)/shard_map/ppermute | solution.py:318
  32.3 32.0 %collective-permute-start.4 = (bf16[128,2048]{1,0:T(8,128)(2,1)S(1)}, bf16[128,2048]{1,0:T(8,128)(2,1)}, u32[]{:S(2)}, u32[]{:S(2)}) collective-permute-start(bf16[128,2048]{1,0:T(8,128)(2,1)S(1)} %collective-permute-done.3.refs_2_), channel_id=1, source_target_pairs={{0,1},{1,0},{2,3},{3,2},{4,5},{5,4},{6,7},{7,6},{8,9},{9,8},{10,11... | collective-permute-start | bytes 1572872 | tf_op jit(solution)/shard_map/ppermute | solution.py:318
  36.4 30.5 %collective-permute-start.8 = (bf16[128,2048]{1,0:T(8,128)(2,1)}, bf16[128,2048]{1,0:T(8,128)(2,1)}, u32[]{:S(2)}, u32[]{:S(2)}) collective-permute-start(bf16[128,2048]{1,0:T(8,128)(2,1)} %collective-permute-done.7.refs_0_), channel_id=1, source_target_pairs={{0,1},{1,0},{2,3},{3,2},{4,5},{5,4},{6,7},{7,6},{8,9},{9,8},{10,11... | collective-permute-start | bytes 1572872 | tf_op jit(solution)/shard_map/ppermute | solution.py:318
  38.8 5.6 %copy-start.1 = (f32[2048]{0:T(1024)S(1)}, f32[2048]{0:T(1024)}, u32[]{:S(2)}) copy-start(f32[2048]{0:T(1024)} %param.14) | copy-start | bytes 24580
  41.8 5.1 %copy-start.2 = (bf16[31,512]{1,0:T(8,128)(2,1)S(1)}, bf16[31,512]{1,0:T(8,128)(2,1)}, u32[]{:S(2)}) copy-start(bf16[31,512]{1,0:T(8,128)(2,1)} %taps_ref.1) | copy-start | bytes 95236
  41.8 5.1 %copy-start.5 = (f32[2]{0:T(128)S(1)}, f32[2]{0:T(128)}, u32[]{:S(2)}) copy-start(f32[2]{0:T(128)} %sinks_ref.1) | copy-start | bytes 28
  41.8 5.1 %collective-permute-start = (bf16[160,128]{1,0:T(8,128)(2,1)S(1)}, bf16[160,128]{1,0:T(8,128)(2,1)S(1)}, u32[]{:S(2)}, u32[]{:S(2)}) collective-permute-start(bf16[160,128]{1,0:T(8,128)(2,1)S(1)} %get-tuple-element.25), channel_id=1, source_target_pairs={{0,4},{4,8},{8,12},{12,16},{16,20},{20,24},{24,28},{1,5},{5,9},{9,... | collective-permute-start | bytes 122888 | tf_op jit(solution)/shard_map/ppermute | solution.py:25
  44.4 19.3 %copy-start.3 = (f32[1024]{0:T(1024)S(1)}, f32[1024]{0:T(1024)}, u32[]{:S(2)}) copy-start(f32[1024]{0:T(1024)} %param.24) | copy-start | bytes 12292
  44.4 19.3 %copy-start.4 = (f32[512]{0:T(512)S(1)}, f32[512]{0:T(512)}, u32[]{:S(2)}) copy-start(f32[512]{0:T(512)} %param.22) | copy-start | bytes 6148
  46.9 17.5 %copy-start = (bf16[128,2048]{1,0:T(8,128)(2,1)S(1)}, bf16[128,2048]{1,0:T(8,128)(2,1)}, u32[]{:S(2)}) copy-start(bf16[128,2048]{1,0:T(8,128)(2,1)} %share_ref.1) | copy-start | bytes 1572868
  51.4 12.3 %all-to-all-start = ((bf16[4,256,256]{2,1,0:T(8,128)(2,1)}), bf16[4,256,256]{2,1,0:T(8,128)(2,1)S(1)}, u32[]{:S(2)}, u32[]{:S(2)}) async-start(bf16[4,256,256]{2,1,0:T(8,128)(2,1)} %mix_rows.1), calls=%async_computation | async-start | bytes 1048576 | tf_op jit(solution)/shard_map/all_to_all | solution.py:525
